TPU v7x, 512 devices: a whole 4x4x16 slice. The times are simulated.
512 devices in a mesh: ep: 128 (over z, x, core), tp: 4 (over y).
Axes of the slice: x: 4, y: 4, z: 16, core: 2. Of those that a mesh axis runs over, the one named last changes fastest.
Arguments:
- tokens: bfloat16 [512, 2048], P('ep', 'tp'), may hold values from -6 to 6
- norm_gain: bfloat16 [2048], P('tp'), may hold values from 0.099609375 to 1.8984375
- w_query: bfloat16 [2048, 2048], P('tp', 'ep'), may hold values from -0.125 to 0.125
- w_forget: bfloat16 [2048, 2048], P('tp', 'ep'), may hold values from -0.125 to 0.125
- w_input: bfloat16 [2048, 2048], P('tp', 'ep'), may hold values from -0.125 to 0.125
- forget_floor: float32 [2048], P('tp'), may hold values from 0 to 0.9
- head_gain: bfloat16 [128], replicated, may hold values from 0.099609375 to 1.8984375
- w_output: bfloat16 [2048, 2048], P('tp', 'ep'), may hold values from -0.125 to 0.125
- state: float32 [512, 16, 128, 128], P('ep', 'tp'), may hold values from -6 to 6
- ffn_gain: bfloat16 [2048], P('tp'), may hold values from 0.099609375 to 1.8984375
- route_experts: int32 [512, 2], P('ep'), may hold values from 0 to 7, all different within a row; in each aligned block of 4 rows (0 to 3, 4 to 7, ...) at most 2 rows name the same one
- route_weights: float32 [512, 2], P('ep'), may hold values from 0.1 to 1
- w_gate: bfloat16 [128, 2048, 448], P('ep', None, 'tp'), may hold values from -0.125 to 0.125
- w_up: bfloat16 [128, 2048, 448], P('ep', None, 'tp'), may hold values from -0.125 to 0.125
- w_down: bfloat16 [128, 448, 2048], P('ep', 'tp'), may hold values from -0.0625 to 0.0625
Outputs:
- mixed: bfloat16 [512, 2048], P('ep', 'tp')
- new_state: float32 [512, 16, 128, 128], P('ep', 'tp')
Inputs may be any that keep to these rules, and one draw needn't show every extreme that they name: `route_experts`: each row names two different experts. Among the rows of one index of ep, no expert is named by more than 2 rows, and in every draw some expert is named by exactly 2 of them.
All inputs are finite; a program needn't handle non-finite values.
Results may differ from a plain program's by a relative error of at most 0.014.
Values may be sent and summed in bfloat16 or wider, within the bound.
No kernel may reach another device: no remote copies, remote signals or barrier semaphores. Data moves between devices by JAX's collectives and lax.ppermute only.
A program may use at most 64 MiB of HBM per device.

v0:
```python
import jax
import jax.numpy as jnp
from jax import lax
from jax.sharding import Mesh
from jax.sharding import PartitionSpec as P

EXPERTS = 8
EP = ("ep_0", "ep_1", "ep_2")


EPS = 1e-06


def laid_out(blocks, dim):
    blocks = jnp.moveaxis(blocks, 0, dim)
    dims = blocks.shape
    return blocks.reshape(*dims[:dim], dims[dim] * dims[dim + 1], *dims[dim + 2 :])


def all_blocks(shard, axes, sequence):
    blocks = shard
    for k in sequence:
        blocks = lax.all_gather(blocks, axes[k])
    done = sequence[::-1]
    back = [done.index(k) for k in range(len(axes))]
    blocks = blocks.transpose(*back, *range(len(axes), blocks.ndim))
    return blocks.reshape(-1, *shard.shape)


def whole_of(shard, axes, sequence, dim):
    return laid_out(all_blocks(shard, axes, sequence), dim)


def in_blocks(shard, dim, length):
    before, after = (shard.shape[:dim], shard.shape[dim + 1 :])
    return jnp.moveaxis(shard.reshape(*before, length, -1, *after), dim, 0)


def sent_and_summed(shard, axis, dim):
    length = lax.axis_size(axis)
    blocks = lax.all_to_all(in_blocks(shard, dim, length), axis, 0, 0, tiled=True)
    return jnp.sum(blocks, axis=0)


def summed_on_arrival(shard, axis, dim):
    blocks = in_blocks(shard, dim, lax.axis_size(axis))
    arrived = lax.all_to_all(blocks, axis, split_axis=0, concat_axis=0, tiled=True)
    return arrived.astype(jnp.float32).sum(axis=0)


def shards(
    tokens,
    norm_gain,
    w_query,
    w_forget,
    w_input,
    forget_floor,
    head_gain,
    w_output,
    state,
    ffn_gain,
    route_experts,
    route_weights,
    w_gate,
    w_up,
    w_down,
):
    ep_count = lax.axis_size(EP)
    tp_count = lax.axis_size("tp")
    seq_count = tokens.shape[0]
    model_width = tokens.shape[1] * tp_count
    head_size = state.shape[2]
    local_heads = state.shape[1]
    tok_f32 = tokens.astype(jnp.float32)
    sum_sq = lax.psum(jnp.sum(tok_f32 * tok_f32, axis=1), "tp")
    normed = (
        tok_f32 * lax.rsqrt(sum_sq / model_width + EPS)[:, None] * norm_gain.astype(jnp.float32)
    ).astype(jnp.bfloat16)
    w_joint = jnp.concatenate([w_query, w_forget, w_input], axis=1)
    partial_value = jnp.dot(
        whole_of(normed, EP, (1, 0, 2), 0), w_joint, preferred_element_type=jnp.float32
    )
    moved_in = lax.all_to_all(partial_value, EP, split_axis=0, concat_axis=1, tiled=True)
    summed = sent_and_summed(moved_in, "tp", 1)
    col_count = w_query.shape[1]
    blocks = summed.reshape(seq_count, -1, 3, col_count)
    queries = blocks[:, :, 0, :].reshape(seq_count, local_heads, head_size)
    fgate = blocks[:, :, 1, :].reshape(seq_count, local_heads, head_size)
    inputs = blocks[:, :, 2, :].reshape(seq_count, local_heads, head_size)
    floors = forget_floor.reshape(local_heads, head_size)
    forget = floors + (1.0 - floors) * jax.nn.sigmoid(fgate)
    new_state = forget[..., None] * state + (1.0 - forget)[..., None] * inputs[:, :, None, :]
    reads = jnp.einsum(
        "bhk,bhkv->bhv", jax.nn.silu(queries), new_state, precision=lax.Precision.HIGHEST
    )
    head_sq = jnp.mean(reads * reads, axis=-1, keepdims=True)
    heads_out = (
        (reads * lax.rsqrt(head_sq + EPS) * head_gain.astype(jnp.float32))
        .reshape(seq_count, local_heads * head_size)
        .astype(jnp.bfloat16)
    )
    part_out = jnp.dot(
        whole_of(heads_out, EP, (1, 0, 2), 0), w_output, preferred_element_type=jnp.float32
    )
    moved_out = lax.all_to_all(
        part_out.astype(jnp.bfloat16), EP, split_axis=0, concat_axis=1, tiled=True
    ).astype(part_out.dtype)
    mixer_slice = summed_on_arrival(moved_out.astype(jnp.bfloat16), "tp", 1).astype(jnp.bfloat16)
    middle = (tok_f32 + mixer_slice.astype(jnp.float32)).astype(jnp.bfloat16)
    middle_f32 = middle.astype(jnp.float32)
    span_count = ep_count // EXPERTS
    capacity = max(2, seq_count // 2)
    positions = jnp.arange(seq_count, dtype=jnp.int32)
    earlier = positions[None, :] < positions[:, None]
    same_expert = route_experts[:, :, None, None] == route_experts[None, None, :, :]
    slot_rank = jnp.sum(same_expert & earlier[:, None, :, None], axis=(2, 3))
    owners = jnp.arange(ep_count, dtype=jnp.int32) // span_count
    matched = route_experts[None, :, :] == owners[:, None, None]
    placed = slot_rank[:, :, None] == jnp.arange(capacity, dtype=jnp.int32)[None, None, :]
    slot_hits = matched[:, :, :, None] & placed[None, :, :, :]
    chosen = jnp.sum(slot_hits.astype(jnp.float32), axis=2).astype(jnp.bfloat16)
    weight_hits = jnp.sum(slot_hits.astype(jnp.float32) * route_weights[None, :, :, None], axis=2)
    row_stat = lax.psum(jnp.sum(middle_f32 * middle_f32, axis=1), "tp")
    second = (
        middle_f32 * lax.rsqrt(row_stat / model_width + EPS)[:, None] * ffn_gain.astype(jnp.float32)
    ).astype(jnp.bfloat16)
    outgoing = jnp.einsum("pts,td->psd", chosen, second, preferred_element_type=jnp.float32).astype(
        jnp.bfloat16
    )
    arrived_part = lax.all_to_all(outgoing, EP, split_axis=0, concat_axis=0, tiled=True)
    arrived = lax.all_gather(arrived_part, "tp", axis=2, tiled=True)
    expert_rows = arrived.reshape(ep_count * capacity, model_width)
    gate_act = jnp.dot(expert_rows, w_gate[0], preferred_element_type=jnp.float32)
    up_act = jnp.dot(expert_rows, w_up[0], preferred_element_type=jnp.float32)
    hidden = (jax.nn.silu(gate_act) * up_act).astype(jnp.bfloat16)
    piece_out = jnp.dot(hidden, w_down[0], preferred_element_type=jnp.float32)
    piece_total = summed_on_arrival(piece_out.astype(jnp.bfloat16), "tp", 1)
    returned = lax.all_to_all(
        piece_total.reshape(ep_count, capacity, -1).astype(jnp.bfloat16),
        EP,
        split_axis=0,
        concat_axis=0,
        tiled=True,
    ).astype(jnp.float32)
    routed = jnp.einsum("pts,psd->td", weight_hits, returned, precision=lax.Precision.HIGHEST)
    result = (middle_f32 + routed).astype(jnp.bfloat16)
    return (result, new_state)


def solution(mesh):
    torus = Mesh(mesh.devices.reshape(16, 4, 2, mesh.shape["tp"]), ("ep_0", "ep_1", "ep_2", "tp"))
    in_specs = (
        P(EP, "tp"),
        P("tp"),
        P("tp", EP),
        P("tp", EP),
        P("tp", EP),
        P("tp"),
        P(),
        P("tp", EP),
        P(EP, "tp", None, None),
        P("tp"),
        P(EP, None),
        P(EP, None),
        P(EP, None, "tp"),
        P(EP, None, "tp"),
        P(EP, "tp", None),
    )
    out_specs = (P(EP, "tp"), P(EP, "tp", None, None))
    return jax.shard_map(
        shards, mesh=torus, in_specs=in_specs, out_specs=out_specs, check_vma=False
    )
```

profile of v0, /device:TPU:1, one launch (start us, length us, event | category | flops | bytes accessed | tf_op | source)
XLA Modules:
  0.0 323.9 jit_solution(1485527307813868062)
XLA Ops:
  7.2 0.9 fusion.22
  8.0 9.5 %psum.14 = f32[4]{0:T(128)S(1)} all-reduce(f32[4]{0:T(128)S(1)} %fusion.22), channel_id=1, replica_groups=mesh['ep_0'=16,'ep_1'=4,'ep_2'=2,'tp'=4] {'tp'}, use_global_device_ids=true, to_apply=%region_1.0 | all-reduce | flops 4 | bytes 32 | tf_op jit(solution)/shard_map/psum | solution.py:75
  17.6 0.7 convert_element_type.76
  18.3 0.8 fusion.31
  19.0 9.5 %all-gather.5 = bf16[4,4,512]{2,1,0:T(4,128)(2,1)S(1)} all-gather(bf16[1,4,512]{2,1,0:T(4,128)(2,1)S(1)} %fusion.31), channel_id=2, replica_groups=mesh['ep_0'=16,'ep_1'=4,'ep_2'=2,'tp'=4] {'ep_1'}, dimensions={0}, use_global_device_ids=true | all-gather | bytes 20480 | tf_op jit(solution)/shard_map/all_gather | solution.py:23
  28.5 29.6 %all-gather.1 = bf16[64,4,512]{2,1,0:T(4,128)(2,1)S(1)} all-gather(bf16[4,4,512]{2,1,0:T(4,128)(2,1)S(1)} %all-gather.5), channel_id=3, replica_groups=mesh['ep_0'=16,'ep_1'=4,'ep_2'=2,'tp'=4] {'ep_0'}, dimensions={0}, use_global_device_ids=true | all-gather | bytes 278528 | tf_op jit(solution)/shard_map/all_gather | solution.py:23
  58.1 14.6 %all-gather.2 = bf16[32,4,4,512]{3,2,1,0:T(4,128)(2,1)S(1)} all-gather(bf16[16,4,4,512]{3,2,1,0:T(4,128)(2,1)S(1)} %bitcast.70), channel_id=4, replica_groups=mesh['ep_0'=16,'ep_1'=4,'ep_2'=2,'tp'=4] {'ep_2'}, dimensions={0}, use_global_device_ids=true | all-gather | bytes 786432 | tf_op jit(solution)/shard_map/all_gather | solution.py:23
  72.7 0.3 copy.120
  73.0 0.5 copy.121
  73.6 0.2 dot_general.26
  73.8 0.2 fusion.15
  74.1 0.2 copy.122
  74.3 1.0 reshape.148
  75.2 10.1 %all-to-all-start = ((f32[128,1,192]{2,1,0:T(1,128)}), f32[128,1,192]{2,1,0:T(1,128)S(1)}, u32[]{:S(2)}, u32[]{:S(2)}) async-start(f32[128,1,192]{2,1,0:T(1,128)} %reshape.148), calls=%async_computation | async-start | bytes 262144 | tf_op jit(solution)/shard_map/all_to_all | solution.py:83
  85.5 15.9 %all-to-all-done = f32[128,1,192]{2,1,0:T(1,128)S(1)} async-done(((f32[128,1,192]{2,1,0:T(1,128)}), f32[128,1,192]{2,1,0:T(1,128)S(1)}, u32[]{:S(2)}, u32[]{:S(2)}) %all-to-all-start) | async-done | bytes 98336 | tf_op jit(solution)/shard_map/all_to_all | solution.py:83
  101.4 0.5 broadcast.148
  101.9 1.0 reduce.10
  102.8 0.2 reshape.149
  103.1 0.2 reshape.118
  103.3 0.7 copy.124
  103.9 3.3 %all-to-all-start.1 = ((f32[4,4,1536]{2,1,0:T(4,128)}), f32[4,4,1536]{2,1,0:T(4,128)S(1)}, u32[]{:S(2)}, u32[]{:S(2)}) async-start(f32[4,4,1536]{2,1,0:T(4,128)} %copy.124), calls=%async_computation.1 | async-start | bytes 196608 | tf_op jit(solution)/shard_map/all_to_all | solution.py:41
  107.2 0.2 convert_reduce_fusion
  107.5 4.4 %all-to-all-done.1 = f32[4,4,1536]{2,1,0:T(4,128)S(1)} async-done(((f32[4,4,1536]{2,1,0:T(4,128)}), f32[4,4,1536]{2,1,0:T(4,128)S(1)}, u32[]{:S(2)}, u32[]{:S(2)}) %all-to-all-start.1) | async-done | bytes 98336 | tf_op jit(solution)/shard_map/all_to_all | solution.py:41
  111.9 0.2 reshape.119
  112.1 0.4 slice_reduce_fusion
  112.5 0.1 mul.125
  112.6 0.1 reshape_squeeze.4
  112.9 0.1 div.41
  113.0 0.6 multiply_add_fusion
  113.6 1.0 copy-done.1
  114.6 1.0 fusion.38
  115.6 0.1 multiply_reduce_fusion
  115.8 9.6 %all_gather.43 = bf16[4,4,512]{2,1,0:T(4,128)(2,1)S(1)} all-gather(bf16[1,4,512]{2,1,0:T(4,128)(2,1)S(1)} %convert_element_type.80), channel_id=1, replica_groups=mesh['ep_0'=16,'ep_1'=4,'ep_2'=2,'tp'=4] {'ep_1'}, dimensions={0}, use_global_device_ids=true | all-gather | bytes 20480 | tf_op jit(solution)/shard_map/all_gather | solution.py:23
  125.4 23.1 %all-gather.3 = bf16[64,4,512]{2,1,0:T(4,128)(2,1)S(1)} all-gather(bf16[4,4,512]{2,1,0:T(4,128)(2,1)S(1)} %all_gather.43), channel_id=5, replica_groups=mesh['ep_0'=16,'ep_1'=4,'ep_2'=2,'tp'=4] {'ep_0'}, dimensions={0}, use_global_device_ids=true | all-gather | bytes 278528 | tf_op jit(solution)/shard_map/all_gather | solution.py:23
  148.5 12.8 %all-gather.4 = bf16[32,4,4,512]{3,2,1,0:T(4,128)(2,1)S(1)} all-gather(bf16[16,4,4,512]{3,2,1,0:T(4,128)(2,1)S(1)} %bitcast.71), channel_id=6, replica_groups=mesh['ep_0'=16,'ep_1'=4,'ep_2'=2,'tp'=4] {'ep_2'}, dimensions={0}, use_global_device_ids=true | all-gather | bytes 786432 | tf_op jit(solution)/shard_map/all_gather | solution.py:23
  161.3 0.3 copy.127
  161.6 0.4 copy.128
  162.0 0.1 reshape_reshape.4
  162.2 0.1 copy-done.6
  162.3 0.2 convolution_convert_fusion.2
  162.5 0.8 copy.129
  163.3 7.2 %all-to-all-start.2 = ((bf16[128,4,16]{2,1,0:T(4,128)(2,1)}), bf16[128,4,16]{2,1,0:T(4,128)(2,1)S(1)}, u32[]{:S(2)}, u32[]{:S(2)}) async-start(bf16[128,4,16]{2,1,0:T(4,128)(2,1)} %bitcast.15), calls=%async_computation.2 | async-start | bytes 262144 | tf_op jit(solution)/shard_map/all_to_all | solution.py:105
  170.6 16.0 %all-to-all-done.2 = bf16[128,4,16]{2,1,0:T(4,128)(2,1)S(1)} async-done(((bf16[128,4,16]{2,1,0:T(4,128)(2,1)}), bf16[128,4,16]{2,1,0:T(4,128)(2,1)S(1)}, u32[]{:S(2)}, u32[]{:S(2)}) %all-to-all-start.2) | async-done | bytes 16416 | tf_op jit(solution)/shard_map/all_to_all | solution.py:105
  186.6 0.2 reshape.120
  186.7 0.6 copy.131
  187.3 3.2 %all-to-all-start.3 = ((bf16[4,4,512]{2,1,0:T(4,128)(2,1)}), bf16[4,4,512]{2,1,0:T(4,128)(2,1)S(1)}, u32[]{:S(2)}, u32[]{:S(2)}) async-start(bf16[4,4,512]{2,1,0:T(4,128)(2,1)} %copy.131), calls=%async_computation.3 | async-start | bytes 32768 | tf_op jit(solution)/shard_map/all_to_all | solution.py:47
  190.7 0.1 fusion.21
  190.7 4.0 %all-to-all-done.3 = bf16[4,4,512]{2,1,0:T(4,128)(2,1)S(1)} async-done(((bf16[4,4,512]{2,1,0:T(4,128)(2,1)}), bf16[4,4,512]{2,1,0:T(4,128)(2,1)S(1)}, u32[]{:S(2)}, u32[]{:S(2)}) %all-to-all-start.3) | async-done | bytes 16416 | tf_op jit(solution)/shard_map/all_to_all | solution.py:47
  194.8 0.1 fusion.26
  194.9 6.9 %psum.15 = f32[4]{0:T(128)S(1)} all-reduce(f32[4]{0:T(128)S(1)} %fusion.26), channel_id=1, replica_groups=mesh['ep_0'=16,'ep_1'=4,'ep_2'=2,'tp'=4] {'tp'}, use_global_device_ids=true, to_apply=%region_9.10 | all-reduce | flops 4 | bytes 32 | tf_op jit(solution)/shard_map/psum | solution.py:123
  201.8 0.3 convolution_convert_fusion.1
  202.1 0.3 copy.132
  202.4 30.9 %all_to_all.54 = bf16[128,2,512]{2,1,0:T(2,128)(2,1)} all-to-all(bf16[128,2,512]{2,1,0:T(2,128)(2,1)S(1)} %copy.132), channel_id=1, replica_groups=mesh['ep_0'=16,'ep_1'=4,'ep_2'=2,'tp'=4] {'ep_0','ep_1','ep_2'}, dimensions={0} | all-to-all | bytes 524288 | tf_op jit(solution)/shard_map/all_to_all | solution.py:130
  233.3 22.5 %all-gather.8.cloned.1.call-done = bf16[128,2,2048]{2,1,0:T(2,128)(2,1)} async-done(((bf16[128,2,512]{2,1,0:T(2,128)(2,1)}), bf16[128,2,2048]{2,1,0:T(2,128)(2,1)}) %all-gather.8.cloned.1.call-update) | async-done | bytes 1048592 | tf_op jit(solution)/shard_map/all_gather | solution.py:131
  255.9 1.5 reshape.121
  257.3 0.5 fusion.6
  257.8 0.5 copy-done.3
  258.4 1.4 convolution_convert_fusion
  259.8 0.1 copy.142
  259.9 16.5 %all_to_all.55 = bf16[4,256,512]{2,1,0:T(8,128)(2,1)S(1)} all-to-all(bf16[4,256,512]{2,1,0:T(8,128)(2,1)S(1)} %bitcast.67), channel_id=1, replica_groups=mesh['ep_0'=16,'ep_1'=4,'ep_2'=2,'tp'=4] {'tp'}, dimensions={0} | all-to-all | bytes 2097152 | tf_op jit(solution)/shard_map/all_to_all | solution.py:47
  276.4 0.2 reduce_sum.95
  276.6 0.1 convert_element_type.93
  276.7 39.5 %all_to_all.56 = bf16[128,2,512]{2,1,0:T(2,128)(2,1)S(1)} all-to-all(bf16[128,2,512]{2,1,0:T(2,128)(2,1)S(1)} %convert_element_type.93), channel_id=1, replica_groups=mesh['ep_0'=16,'ep_1'=4,'ep_2'=2,'tp'=4] {'ep_0','ep_1','ep_2'}, dimensions={0} | all-to-all | bytes 524288 | tf_op jit(solution)/shard_map/all_to_all | solution.py:138
  316.2 0.8 fusion.2
  (50 shorter events, 0.6 us)
Async XLA Ops:
  7.2 250.7 %copy-start = (bf16[1,112,2048]{2,1,0:T(8,128)(2,1)S(1)}, bf16[1,112,2048]{2,1,0:T(8,128)(2,1)}, u32[]{:S(2)}) copy-start(bf16[1,112,2048]{2,1,0:T(8,128)(2,1)} %param.29) | copy-start | bytes 1376260
  73.0 0.8 copy-start.7
  73.0 0.8 copy-start.8
  73.0 0.8 copy-start.9
  73.8 11.6 %copy-start.10 = (s32[4,2]{0,1:T(2,128)S(1)}, s32[4,2]{0,1:T(2,128)}, u32[]{:S(2)}) copy-start(s32[4,2]{0,1:T(2,128)} %param.25) | copy-start | bytes 100
  73.8 11.6 %copy-start.14 = (bf16[128]{0:T(256)(128)(2,1)S(1)}, bf16[128]{0:T(256)(128)(2,1)}, u32[]{:S(2)}) copy-start(bf16[128]{0:T(256)(128)(2,1)} %param.21) | copy-start | bytes 772
  73.8 11.6 %copy-start.11 = (f32[512]{0:T(512)S(1)}, f32[512]{0:T(512)}, u32[]{:S(2)}) copy-start(f32[512]{0:T(512)} %param.20) | copy-start | bytes 6148
  75.2 26.1 %all-to-all-start = ((f32[128,1,192]{2,1,0:T(1,128)}), f32[128,1,192]{2,1,0:T(1,128)S(1)}, u32[]{:S(2)}, u32[]{:S(2)}) async-start(f32[128,1,192]{2,1,0:T(1,128)} %reshape.148), calls=%async_computation | async-start | bytes 262144 | tf_op jit(solution)/shard_map/all_to_all | solution.py:83
  103.0 10.0 %copy-start.2 = (f32[4,4,128,128]{3,2,1,0:T(8,128)S(1)}, f32[4,4,128,128]{3,2,1,0:T(8,128)}, u32[]{:S(2)}) copy-start(f32[4,4,128,128]{3,2,1,0:T(8,128)} %param.23) | copy-start | bytes 3145732
  103.9 7.9 %all-to-all-start.1 = ((f32[4,4,1536]{2,1,0:T(4,128)}), f32[4,4,1536]{2,1,0:T(4,128)S(1)}, u32[]{:S(2)}, u32[]{:S(2)}) async-start(f32[4,4,1536]{2,1,0:T(4,128)} %copy.124), calls=%async_computation.1 | async-start | bytes 196608 | tf_op jit(solution)/shard_map/all_to_all | solution.py:41
  113.6 1.0 copy-start.1
  161.6 0.7 copy-start.6
  162.0 28.6 %copy-start.12 = (f32[4,2]{0,1:T(2,128)S(1)}, f32[4,2]{0,1:T(2,128)}, u32[]{:S(2)}) copy-start(f32[4,2]{0,1:T(2,128)} %param.26) | copy-start | bytes 100
  162.0 32.8 %copy-start.5 = (bf16[4,512]{1,0:T(4,128)(2,1)S(1)}, bf16[4,512]{1,0:T(4,128)(2,1)}, u32[]{:S(2)}) copy-start(bf16[4,512]{1,0:T(4,128)(2,1)} %param.15) | copy-start | bytes 12292
  162.0 32.9 %copy-start.13 = (bf16[512]{0:T(512)(128)(2,1)S(1)}, bf16[512]{0:T(512)(128)(2,1)}, u32[]{:S(2)}) copy-start(bf16[512]{0:T(512)(128)(2,1)} %param.24) | copy-start | bytes 3076
  163.3 23.2 %all-to-all-start.2 = ((bf16[128,4,16]{2,1,0:T(4,128)(2,1)}), bf16[128,4,16]{2,1,0:T(4,128)(2,1)S(1)}, u32[]{:S(2)}, u32[]{:S(2)}) async-start(bf16[128,4,16]{2,1,0:T(4,128)(2,1)} %bitcast.15), calls=%async_computation.2 | async-start | bytes 262144 | tf_op jit(solution)/shard_map/all_to_all | solution.py:105
  187.3 7.4 %all-to-all-start.3 = ((bf16[4,4,512]{2,1,0:T(4,128)(2,1)}), bf16[4,4,512]{2,1,0:T(4,128)(2,1)S(1)}, u32[]{:S(2)}, u32[]{:S(2)}) async-start(bf16[4,4,512]{2,1,0:T(4,128)(2,1)} %copy.131), calls=%async_computation.3 | async-start | bytes 32768 | tf_op jit(solution)/shard_map/all_to_all | solution.py:47
  190.6 65.3 %all-gather.8.cloned.1.call-start = ((), (), s32[]{:S(2)}) async-start(), calls=%async_computation.7 | async-start | bytes 1310720 | tf_op jit(solution)/shard_map/all_gather | solution.py:131
  233.3 24.0 %copy-start.4 = (bf16[1,2048,112]{1,2,0:T(8,128)(2,1)S(1)}, bf16[1,2048,112]{1,2,0:T(8,128)(2,1)}, u32[]{:S(2)}) copy-start(bf16[1,2048,112]{1,2,0:T(8,128)(2,1)} %param.27) | copy-start | bytes 1376260
  257.3 1.0 copy-start.3
Sparse Core Ops, SparseCore 0:
  233.4 22.3 all-gather.7
where the time goes:
time: 326 us; the launch traced here: 324 us
  blocking collectives  202 us (62%)
  waiting for transfers between devices  62.8 us (19%)
  starting transfers between devices  24 us (7%)
  between operations  14.5 us (4%)
  local copies, waits for them, and re-layouts  10.8 us (3%)
  other arithmetic  4.91 us (2%)
  matrix products  4.43 us (1%)
    all_gather x6, blocking collectives, all_blocks(): blocks = lax.all_gather(blocks, axes[k])  99.2 us
    all_to_all x1, blocking collectives, shards(): lax.all_to_all(piece_total.reshape(ep_count, capacity, -1).astype(jnp.bfl...  39.5 us
    all_to_all x1, blocking collectives, shards(): lax.all_to_all(outgoing, EP, split_axis=0, concat_axis=0, tiled=True)  30.9 us
    all_gather x1, waiting for transfers between devices, shards(): arrived = lax.all_gather(arrived_part, 'tp', axis=2, tiled=True)  22.5 us
    all_to_all x1, blocking collectives, summed_on_arrival(): lax.all_to_all(blocks, axis, split_axis=0, concat_axis=0, tiled=True)  16.5 us
    all_to_all x1, waiting for transfers between devices, shards(): lax.all_to_all(part_out.astype(jnp.bfloat16), EP, split_axis=0, concat_ax...  16 us
    all_to_all x1, waiting for transfers between devices, shards(): lax.all_to_all(partial_value, EP, split_axis=0, concat_axis=1, tiled=True)  15.9 us
    all_to_all x1, starting transfers between devices, shards(): lax.all_to_all(partial_value, EP, split_axis=0, concat_axis=1, tiled=True)  10.1 us
  transfers between devices with their start and end apart: 5, of which 5 were waited for; matrix products, arithmetic and copies ran while one was open for 0% of the time, Pallas kernels for 0%

commit v1 on v0

v1 whole, which is shorter than its diff:
```python
import jax
import jax.numpy as jnp
from jax import lax
from jax.sharding import Mesh
from jax.sharding import PartitionSpec as P

EXPERTS = 8
EPS = 1e-06
EP = ("zh", "zl", "x", "c")
ROW = ("zl", "x", "c")
PAIR = ("zl", "x", "c", "tp")
bf16 = jnp.bfloat16
f32 = jnp.float32


def exchange(blocks, axes):
    return lax.all_to_all(blocks, axes, split_axis=0, concat_axis=0, tiled=True)


def gathered(shard, axes, count):
    return exchange(jnp.broadcast_to(shard[None], (count, *shard.shape)), axes)


def shards(
    tokens,
    norm_gain,
    w_query,
    w_forget,
    w_input,
    forget_floor,
    head_gain,
    w_output,
    state,
    ffn_gain,
    route_experts,
    route_weights,
    w_gate,
    w_up,
    w_down,
):
    tp = lax.axis_size("tp")
    rows = lax.axis_size(ROW)
    zh = lax.axis_size("zh")
    seq, feat = tokens.shape
    width = feat * tp
    heads, head = state.shape[1], state.shape[2]
    col = w_query.shape[1]
    low = zh // tp
    here = lax.axis_index(ROW)

    w_joint = jnp.concatenate([w_query, w_forget, w_input, w_output], axis=1).T
    w_all = lax.all_gather(w_joint, "zh")
    w_in = w_all[:, : 3 * col].reshape(zh * 3 * col, feat)
    w_out = w_all[:, 3 * col :].reshape(zh * col, feat)

    tok_all = gathered(tokens, ROW, rows).reshape(rows * seq, feat).astype(f32)
    sum_sq = jnp.sum(tok_all * tok_all, axis=1)
    scaled = (tok_all * norm_gain.astype(f32)).astype(bf16)
    partial = lax.dot_general(
        scaled, w_in, (((1,), (1,)), ((), ())), preferred_element_type=f32
    )
    partial = partial.reshape(rows, seq, tp, low * 3 * col).transpose(0, 2, 1, 3)
    stat = jnp.broadcast_to(sum_sq.reshape(rows, 1, seq, 1), (rows, tp, seq, 1))
    sent = jnp.concatenate([partial, stat], axis=3).reshape(rows * tp, seq, -1)
    got = exchange(sent, PAIR).reshape(rows, tp, seq, -1).sum(axis=1)
    scale = lax.rsqrt(got[0, :, -1] / width + EPS)
    cols = got[:, :, :-1].reshape(rows, seq, low, 3, col).transpose(3, 1, 2, 0, 4)
    cols = cols.reshape(3, seq, heads, head) * scale[None, :, None, None]
    queries, fgate, inputs = cols[0], cols[1], cols[2]

    floors = forget_floor.reshape(heads, head)
    forget = floors + (1.0 - floors) * jax.nn.sigmoid(fgate)
    new_state = forget[..., None] * state + (1.0 - forget)[..., None] * inputs[:, :, None, :]
    reads = jnp.einsum(
        "bhk,bhkv->bhv", jax.nn.silu(queries), new_state, precision=lax.Precision.HIGHEST
    )
    head_sq = jnp.mean(reads * reads, axis=-1, keepdims=True)
    heads_out = (
        (reads * lax.rsqrt(head_sq + EPS) * head_gain.astype(f32))
        .reshape(seq, heads * head)
        .astype(bf16)
    )

    heads_all = gathered(heads_out, ROW, rows).reshape(rows * seq, feat)
    part_out = lax.dot_general(
        heads_all, w_out, (((1,), (1,)), ((), ())), preferred_element_type=f32
    )
    part_out = part_out.reshape(rows, seq, tp, low * col).transpose(0, 2, 1, 3)
    gain_here = lax.dynamic_index_in_dim(
        ffn_gain.astype(f32).reshape(rows, seq, feat // (rows * seq)), here, 0, False
    )
    gain_sent = jnp.broadcast_to(gain_here, (rows, tp, *gain_here.shape))
    sent = jnp.concatenate([part_out, gain_sent], axis=3).reshape(rows * tp, seq, -1)
    got = exchange(sent, PAIR).reshape(rows, tp, seq, -1)
    gain_all = got[:, :, :, low * col :].transpose(1, 0, 2, 3).reshape(tp, feat)
    mixer = got[:, :, :, : low * col].sum(axis=1).reshape(rows, seq, low, col)
    mixer = mixer.transpose(1, 2, 0, 3).reshape(seq, feat).astype(bf16)
    middle = (tokens.astype(f32) + mixer.astype(f32)).astype(bf16)

    cap = max(2, seq // 2)
    positions = jnp.arange(seq, dtype=jnp.int32)
    earlier = positions[None, :] < positions[:, None]
    same = route_experts[:, :, None, None] == route_experts[None, None, :, :]
    rank = jnp.sum(same & earlier[:, None, :, None], axis=(2, 3))
    matched = route_experts[None] == jnp.arange(EXPERTS, dtype=jnp.int32)[:, None, None]
    placed = rank[:, :, None] == jnp.arange(cap, dtype=jnp.int32)[None, None, :]
    hits = (matched[:, :, :, None] & placed[None]).astype(f32)
    chosen = jnp.sum(hits, axis=2).astype(bf16)
    weights = jnp.sum(hits * route_weights[None, :, :, None], axis=2)
    outgoing = jnp.einsum("ets,td->esd", chosen, middle, preferred_element_type=f32)
    arrived = exchange(outgoing.astype(bf16), "zh").reshape(zh * cap, feat)
    block = gathered(arrived, PAIR, rows * tp).reshape(rows, tp, zh * cap, feat)

    whole = block.transpose(0, 2, 1, 3).reshape(rows * zh * cap, width).astype(f32)
    mean_sq = jnp.mean(whole * whole, axis=1, keepdims=True)
    second = (whole * lax.rsqrt(mean_sq + EPS) * gain_all.reshape(width)).astype(bf16)
    gate = jnp.dot(second, w_gate[0], preferred_element_type=f32)
    up = jnp.dot(second, w_up[0], preferred_element_type=f32)
    hidden = (jax.nn.silu(gate) * up).astype(bf16)
    piece = jnp.dot(hidden, w_down[0], preferred_element_type=f32).astype(bf16)
    piece = piece.reshape(rows, zh * cap, tp, feat).transpose(0, 2, 1, 3)

    summed = exchange(piece.reshape(rows * tp, zh * cap, feat), PAIR)
    summed = summed.astype(f32).sum(axis=0).astype(bf16)
    returned = exchange(summed.reshape(zh, cap, feat), "zh").astype(f32)
    routed = jnp.einsum("ets,esd->td", weights, returned, precision=lax.Precision.HIGHEST)
    mixed = (middle.astype(f32) + routed).astype(bf16)
    return mixed, new_state


def solution(mesh):
    torus = Mesh(mesh.devices.reshape(8, 2, 4, 2, mesh.shape["tp"]), (*EP, "tp"))
    in_specs = (
        P(EP, "tp"),
        P("tp"),
        P("tp", EP),
        P("tp", EP),
        P("tp", EP),
        P("tp"),
        P(),
        P("tp", EP),
        P(EP, "tp", None, None),
        P("tp"),
        P(EP, None),
        P(EP, None),
        P(EP, None, "tp"),
        P(EP, None, "tp"),
        P(EP, "tp", None),
    )
    out_specs = (P(EP, "tp"), P(EP, "tp", None, None))
    return jax.shard_map(
        shards, mesh=torus, in_specs=in_specs, out_specs=out_specs, check_vma=False
    )
```

time: 326 us -> 183 us (0.56)
  blocking collectives: 202 us -> 82.3 us
  waiting for transfers between devices: 62.8 us -> 39.5 us
  starting transfers between devices: 24 us -> 39.5 us
  between operations: 14.5 us -> 1.09 us
    all_gather x6 -> x1, blocking collectives: 99.2 us -> 27.3 us  [shards(): w_all = lax.all_gather(w_joint, 'zh')]
    all_to_all x3, blocking collectives: 86.9 us -> 55 us  [exchange(): return lax.all_to_all(blocks, axes, split_axis=0, concat_axis=0, tiled=True)]
    all_gather x1 -> x0, waiting for transfers between devices: 22.5 us -> none  [shards(): arrived = lax.all_gather(arrived_part, 'tp', axis=2, tiled=True)]
    psum x2 -> x0, blocking collectives: 16.4 us -> none  [the longest x1 9.54 us: shards(): sum_sq = lax.psum(jnp.sum(tok_f32 * tok_f32, axis=1), 'tp')]
    all_to_all x4 -> x5, starting transfers between devices: 23.9 us -> 39.5 us  [exchange(): return lax.all_to_all(blocks, axes, split_axis=0, concat_axis=0, tiled=True)]
    broadcast_in_dim x0 -> x6, local copies, waits for them, and re-layouts: none -> 3.27 us  [the longest x4 3.18 us: gathered(): return exchange(jnp.broadcast_to(shard[None], (count, *shard.shape)), axes)]
    all_to_all x4 -> x5, waiting for transfers between devices: 40.3 us -> 39.5 us  [exchange(): return lax.all_to_all(blocks, axes, split_axis=0, concat_axis=0, tiled=True)]
  transfers between devices with their start and end apart: 5 -> 5, of which waited for: 5 -> 4; matrix products, arithmetic and copies ran while one was open for 0% -> 1% of each run, Pallas kernels for 0% -> 0%
where the time goes in v1:
time: 183 us; the launch traced here: 182 us
  blocking collectives  82.3 us (45%)
  starting transfers between devices  39.5 us (22%)
  waiting for transfers between devices  39.5 us (22%)
  local copies, waits for them, and re-layouts  10.7 us (6%)
  other arithmetic  4.78 us (3%)
  matrix products  4.32 us (2%)
    all_to_all x3, blocking collectives, exchange(): return lax.all_to_all(blocks, axes, split_axis=0, concat_axis=0, tiled=True)  55 us
    all_to_all x5, waiting for transfers between devices, exchange(): return lax.all_to_all(blocks, axes, split_axis=0, concat_axis=0, tiled=True)  39.5 us
    all_to_all x5, starting transfers between devices, exchange(): return lax.all_to_all(blocks, axes, split_axis=0, concat_axis=0, tiled=True)  39.5 us
    all_gather x1, blocking collectives, shards(): w_all = lax.all_gather(w_joint, 'zh')  27.3 us
  transfers between devices with their start and end apart: 5, of which 4 were waited for; matrix products, arithmetic and copies ran while one was open for 1% of the time, Pallas kernels for 0%

profile of v1, /device:TPU:1, one launch (start us, length us, event | category | flops | bytes accessed | tf_op | source)
XLA Modules:
  0.0 182.1 jit_solution(9374890429634816776)
XLA Ops:
  0.6 0.0 copy-start
  0.6 1.4 broadcast_in_dim.12
  2.0 10.1 %all-to-all-start = ((bf16[16,4,512]{2,1,0:T(4,128)(2,1)}), bf16[16,4,512]{2,1,0:T(4,128)(2,1)S(1)}, u32[]{:S(2)}, u32[]{:S(2)}) async-start(bf16[16,4,512]{2,1,0:T(4,128)(2,1)} %broadcast_in_dim.12), calls=%async_computation | async-start | bytes 131072 | tf_op jit(solution)/shard_map/all_to_all | solution.py:17
  12.2 0.8 maximum_bitcast_fusion
  12.9 0.7 convert_element_type.99
  13.6 27.3 %all-gather = bf16[512,512]{1,0:T(8,128)(2,1)S(1)} all-gather(bf16[64,512]{1,0:T(8,128)(2,1)S(1)} %maximum_bitcast_fusion), channel_id=2, replica_groups=mesh['zh'=8,'zl'=2,'x'=4,'c'=2,'tp'=4] {'zh'}, dimensions={0}, use_global_device_ids=true | all-gather | bytes 589824 | tf_op jit(solution)/shard_map/all_gather | solution.py:52
  41.0 0.0 copy-start.8
  41.0 0.1 fusion.13
  41.1 0.3 convolution_bitcast_fusion
  41.4 0.1 broadcast_in_dim.13
  41.4 0.1 pad_maximum_fusion
  41.6 0.1 copy.121
  41.6 0.7 copy.122
  42.4 15.0 %all-to-all-start.1 = ((f32[64,4,97]{2,1,0:T(4,128)}), f32[64,4,97]{2,1,0:T(4,128)S(1)}, u32[]{:S(2)}, u32[]{:S(2)}) async-start(f32[64,4,97]{2,1,0:T(4,128)} %copy.122), calls=%async_computation.1 | async-start | bytes 262144 | tf_op jit(solution)/shard_map/all_to_all | solution.py:17
  57.5 0.1 reshape.201
  57.6 0.2 convert_reduce_fusion
  57.8 8.1 %all-to-all-done.1 = f32[64,4,97]{2,1,0:T(4,128)S(1)} async-done(((f32[64,4,97]{2,1,0:T(4,128)}), f32[64,4,97]{2,1,0:T(4,128)S(1)}, u32[]{:S(2)}, u32[]{:S(2)}) %all-to-all-start.1) | async-done | bytes 99360 | tf_op jit(solution)/shard_map/all_to_all | solution.py:17
  66.0 0.1 slice.38
  66.1 0.1 rsqrt_reduce_fusion
  66.2 0.2 reshape.191
  66.4 0.1 reshape.192
  66.6 0.1 broadcast_multiply_fusion
  66.7 0.6 multiply_add_fusion
  67.3 1.0 copy-done.1
  68.3 1.0 fusion.39
  69.2 0.1 multiply_reduce_fusion
  69.3 0.1 fusion.34
  69.4 0.7 broadcast_in_dim.14
  70.1 3.9 %all-to-all-start.2 = ((bf16[16,4,512]{2,1,0:T(4,128)(2,1)}), bf16[16,4,512]{2,1,0:T(4,128)(2,1)S(1)}, u32[]{:S(2)}, u32[]{:S(2)}) async-start(bf16[16,4,512]{2,1,0:T(4,128)(2,1)} %broadcast_in_dim.14), calls=%async_computation.2 | async-start | bytes 131072 | tf_op jit(solution)/shard_map/all_to_all | solution.py:17
  74.0 0.1 iota_compare_fusion
  74.1 5.8 %all-to-all-done.2 = bf16[16,4,512]{2,1,0:T(4,128)(2,1)S(1)} async-done(((bf16[16,4,512]{2,1,0:T(4,128)(2,1)}), bf16[16,4,512]{2,1,0:T(4,128)(2,1)S(1)}, u32[]{:S(2)}, u32[]{:S(2)}) %all-to-all-start.2) | async-done | bytes 65568 | tf_op jit(solution)/shard_map/all_to_all | solution.py:17
  79.9 0.2 convolution_bitcast_fusion.1
  80.1 0.1 pad_maximum_fusion.1
  80.2 0.1 copy.126
  80.3 0.1 copy.127
  80.4 0.8 reshape.215
  81.2 4.5 %all-to-all-start.3 = ((f32[64,1,160]{2,1,0:T(1,128)}), f32[64,1,160]{2,1,0:T(1,128)S(1)}, u32[]{:S(2)}, u32[]{:S(2)}) async-start(f32[64,1,160]{2,1,0:T(1,128)} %reshape.215), calls=%async_computation.3 | async-start | bytes 131072 | tf_op jit(solution)/shard_map/all_to_all | solution.py:17
  85.7 0.1 fusion.27
  85.8 8.2 %all-to-all-done.3 = f32[64,1,160]{2,1,0:T(1,128)S(1)} async-done(((f32[64,1,160]{2,1,0:T(1,128)}), f32[64,1,160]{2,1,0:T(1,128)S(1)}, u32[]{:S(2)}, u32[]{:S(2)}) %all-to-all-start.3) | async-done | bytes 40992 | tf_op jit(solution)/shard_map/all_to_all | solution.py:17
  94.0 0.5 broadcast.153
  94.5 0.8 reduce.6
  95.3 0.1 reshape.216
  95.5 0.1 reshape.204
  95.6 0.1 reshape.202
  95.7 0.2 convolution_convert_fusion.1
  95.9 18.7 %all_to_all.40 = bf16[8,2,512]{2,1,0:T(2,128)(2,1)S(1)} all-to-all(bf16[8,2,512]{2,1,0:T(2,128)(2,1)S(1)} %copy.130), channel_id=1, replica_groups=mesh['zh'=8,'zl'=2,'x'=4,'c'=2,'tp'=4] {'zh'}, dimensions={0} | all-to-all | bytes 32768 | tf_op jit(solution)/shard_map/all_to_all | solution.py:17
  114.7 1.1 broadcast_in_dim.17
  115.8 5.9 %all-to-all-start.5 = ((bf16[64,16,512]{2,1,0:T(8,128)(2,1)}), bf16[64,16,512]{2,1,0:T(8,128)(2,1)S(1)}, u32[]{:S(2)}, u32[]{:S(2)}) async-start(bf16[64,16,512]{2,1,0:T(8,128)(2,1)} %broadcast_in_dim.17), calls=%async_computation.5 | async-start | bytes 2097152 | tf_op jit(solution)/shard_map/all_to_all | solution.py:17
  121.7 0.1 copy_bitcast_fusion
  121.9 0.2 mul.158
  122.0 17.4 %all-to-all-done.5 = bf16[64,16,512]{2,1,0:T(8,128)(2,1)S(1)} async-done(((bf16[64,16,512]{2,1,0:T(8,128)(2,1)}), bf16[64,16,512]{2,1,0:T(8,128)(2,1)S(1)}, u32[]{:S(2)}, u32[]{:S(2)}) %all-to-all-start.5) | async-done | bytes 1048608 | tf_op jit(solution)/shard_map/all_to_all | solution.py:17
  139.4 0.3 fusion
  139.7 0.3 fusion.6
  140.0 0.9 copy.132
  140.9 0.3 copy.147
  141.2 0.7 copy-done.4
  141.9 0.5 fusion.10
  142.4 1.4 convolution_convert_fusion
  143.8 0.8 reshape.197
  144.6 0.2 copy.133
  144.9 22.4 %all_to_all.41 = bf16[64,16,512]{2,1,0:T(8,128)(2,1)S(1)} all-to-all(bf16[64,16,512]{2,1,0:T(8,128)(2,1)S(1)} %bitcast.107), channel_id=1, replica_groups=mesh['zh'=8,'zl'=2,'x'=4,'c'=2,'tp'=4] {'zl','x','c','tp'}, dimensions={0} | all-to-all | bytes 2097152 | tf_op jit(solution)/shard_map/all_to_all | solution.py:17
  167.2 0.2 reduce_sum.92
  167.4 13.9 %all_to_all.42 = bf16[8,2,512]{2,1,0:T(2,128)(2,1)S(1)} all-to-all(bf16[8,2,512]{2,1,0:T(2,128)(2,1)S(1)} %reshape.199), channel_id=1, replica_groups=mesh['zh'=8,'zl'=2,'x'=4,'c'=2,'tp'=4] {'zh'}, dimensions={0} | all-to-all | bytes 32768 | tf_op jit(solution)/shard_map/all_to_all | solution.py:17
  181.3 0.8 fusion.5
  (41 shorter events, 0.3 us)
Async XLA Ops:
  0.6 141.8 %copy-start = (bf16[1,112,2048]{2,1,0:T(8,128)(2,1)S(1)}, bf16[1,112,2048]{2,1,0:T(8,128)(2,1)}, u32[]{:S(2)}) copy-start(bf16[1,112,2048]{2,1,0:T(8,128)(2,1)} %param.29) | copy-start | bytes 1376260
  2.0 39.0 %all-to-all-start = ((bf16[16,4,512]{2,1,0:T(4,128)(2,1)}), bf16[16,4,512]{2,1,0:T(4,128)(2,1)S(1)}, u32[]{:S(2)}, u32[]{:S(2)}) async-start(bf16[16,4,512]{2,1,0:T(4,128)(2,1)} %broadcast_in_dim.12), calls=%async_computation | async-start | bytes 131072 | tf_op jit(solution)/shard_map/all_to_all | solution.py:17
  40.9 16.5 %copy-start.10 = (bf16[128]{0:T(256)(128)(2,1)S(1)}, bf16[128]{0:T(256)(128)(2,1)}, u32[]{:S(2)}) copy-start(bf16[128]{0:T(256)(128)(2,1)} %param.21) | copy-start | bytes 772
  41.0 16.5 %copy-start.8 = (bf16[512]{0:T(512)(128)(2,1)S(1)}, bf16[512]{0:T(512)(128)(2,1)}, u32[]{:S(2)}) copy-start(bf16[512]{0:T(512)(128)(2,1)} %param.24) | copy-start | bytes 3076
  41.0 16.6 %copy-start.6 = (s32[4,2]{0,1:T(2,128)S(1)}, s32[4,2]{0,1:T(2,128)}, u32[]{:S(2)}) copy-start(s32[4,2]{0,1:T(2,128)} %param.25) | copy-start | bytes 100
  41.0 16.8 %copy-start.7 = (f32[512]{0:T(512)S(1)}, f32[512]{0:T(512)}, u32[]{:S(2)}) copy-start(f32[512]{0:T(512)} %param.20) | copy-start | bytes 6148
  41.6 25.1 %copy-start.2 = (f32[4,4,128,128]{3,2,1,0:T(8,128)S(1)}, f32[4,4,128,128]{3,2,1,0:T(8,128)}, u32[]{:S(2)}) copy-start(f32[4,4,128,128]{3,2,1,0:T(8,128)} %param.23) | copy-start | bytes 3145732
  42.4 23.6 %all-to-all-start.1 = ((f32[64,4,97]{2,1,0:T(4,128)}), f32[64,4,97]{2,1,0:T(4,128)S(1)}, u32[]{:S(2)}, u32[]{:S(2)}) async-start(f32[64,4,97]{2,1,0:T(4,128)} %copy.122), calls=%async_computation.1 | async-start | bytes 262144 | tf_op jit(solution)/shard_map/all_to_all | solution.py:17
  67.3 1.0 copy-start.1
  70.1 15.6 %copy-start.9 = (f32[4,2]{0,1:T(2,128)S(1)}, f32[4,2]{0,1:T(2,128)}, u32[]{:S(2)}) copy-start(f32[4,2]{0,1:T(2,128)} %param.26) | copy-start | bytes 100
  70.1 9.8 %all-to-all-start.2 = ((bf16[16,4,512]{2,1,0:T(4,128)(2,1)}), bf16[16,4,512]{2,1,0:T(4,128)(2,1)S(1)}, u32[]{:S(2)}, u32[]{:S(2)}) async-start(bf16[16,4,512]{2,1,0:T(4,128)(2,1)} %broadcast_in_dim.14), calls=%async_computation.2 | async-start | bytes 131072 | tf_op jit(solution)/shard_map/all_to_all | solution.py:17
  80.1 15.6 %copy-start.5 = (bf16[4,512]{1,0:T(4,128)(2,1)S(1)}, bf16[4,512]{1,0:T(4,128)(2,1)}, u32[]{:S(2)}) copy-start(bf16[4,512]{1,0:T(4,128)(2,1)} %param.15) | copy-start | bytes 12292
  81.2 12.8 %all-to-all-start.3 = ((f32[64,1,160]{2,1,0:T(1,128)}), f32[64,1,160]{2,1,0:T(1,128)S(1)}, u32[]{:S(2)}, u32[]{:S(2)}) async-start(f32[64,1,160]{2,1,0:T(1,128)} %reshape.215), calls=%async_computation.3 | async-start | bytes 131072 | tf_op jit(solution)/shard_map/all_to_all | solution.py:17
  115.8 23.6 %all-to-all-start.5 = ((bf16[64,16,512]{2,1,0:T(8,128)(2,1)}), bf16[64,16,512]{2,1,0:T(8,128)(2,1)S(1)}, u32[]{:S(2)}, u32[]{:S(2)}) async-start(bf16[64,16,512]{2,1,0:T(8,128)(2,1)} %broadcast_in_dim.17), calls=%async_computation.5 | async-start | bytes 2097152 | tf_op jit(solution)/shard_map/all_to_all | solution.py:17
  140.9 1.0 copy-start.4
  141.2 1.2 copy-start.3

commit v2 on v1

--- a/solution.py
+++ b/solution.py
@@ -6,6 +6,7 @@
 
 EXPERTS = 8
 EPS = 1e-06
+LANES = 128
 EP = ("zh", "zl", "x", "c")
 ROW = ("zl", "x", "c")
 PAIR = ("zl", "x", "c", "tp")
@@ -49,22 +50,28 @@
     here = lax.axis_index(ROW)
 
     w_joint = jnp.concatenate([w_query, w_forget, w_input, w_output], axis=1).T
-    w_all = lax.all_gather(w_joint, "zh")
-    w_in = w_all[:, : 3 * col].reshape(zh * 3 * col, feat)
-    w_out = w_all[:, 3 * col :].reshape(zh * col, feat)
+    w_all = gathered(w_joint, "zh", zh)
 
-    tok_all = gathered(tokens, ROW, rows).reshape(rows * seq, feat).astype(f32)
+    tok_all = tokens
+    for axis in reversed(ROW):
+        tok_all = lax.all_gather(tok_all, axis, tiled=True)
+    mine = jnp.concatenate([w_gate[0].T, w_up[0].T, w_down[0]], axis=0)
+    other = lax.ppermute(mine, "c", [(0, 1), (1, 0)])
+    w_all, tok_all, mine, other = lax.optimization_barrier((w_all, tok_all, mine, other))
+    w_in = w_all[:, : 3 * col].reshape(tp, low * 3 * col, feat)
+    w_out = w_all[:, 3 * col :].reshape(tp, low * col, feat)
+
+    tok_all = tok_all.astype(f32)
     sum_sq = jnp.sum(tok_all * tok_all, axis=1)
     scaled = (tok_all * norm_gain.astype(f32)).astype(bf16)
-    partial = lax.dot_general(
-        scaled, w_in, (((1,), (1,)), ((), ())), preferred_element_type=f32
-    )
+    partial = jnp.einsum("td,pcd->tpc", scaled, w_in, preferred_element_type=f32)
     partial = partial.reshape(rows, seq, tp, low * 3 * col).transpose(0, 2, 1, 3)
-    stat = jnp.broadcast_to(sum_sq.reshape(rows, 1, seq, 1), (rows, tp, seq, 1))
-    sent = jnp.concatenate([partial, stat], axis=3).reshape(rows * tp, seq, -1)
-    got = exchange(sent, PAIR).reshape(rows, tp, seq, -1).sum(axis=1)
-    scale = lax.rsqrt(got[0, :, -1] / width + EPS)
-    cols = got[:, :, :-1].reshape(rows, seq, low, 3, col).transpose(3, 1, 2, 0, 4)
+    used = low * 3 * col
+    stat = jnp.broadcast_to(sum_sq.reshape(rows, 1, seq, 1), (rows, tp, seq, LANES - used))
+    sent = jnp.concatenate([partial, stat], axis=3).reshape(rows * tp, seq, LANES)
+    got = exchange(sent, PAIR).reshape(rows, tp, seq, LANES).sum(axis=1)
+    scale = lax.rsqrt(got[0, :, LANES - 1] / width + EPS)
+    cols = got[:, :, :used].reshape(rows, seq, low, 3, col).transpose(3, 1, 2, 0, 4)
     cols = cols.reshape(3, seq, heads, head) * scale[None, :, None, None]
     queries, fgate, inputs = cols[0], cols[1], cols[2]
 
@@ -82,17 +89,17 @@
     )
 
     heads_all = gathered(heads_out, ROW, rows).reshape(rows * seq, feat)
-    part_out = lax.dot_general(
-        heads_all, w_out, (((1,), (1,)), ((), ())), preferred_element_type=f32
+    part_out = jnp.einsum("td,pcd->tpc", heads_all, w_out, preferred_element_type=f32)
+    part_out = part_out.reshape(rows, seq, tp, low * col).transpose(0, 2, 1, 3)
+    share = feat // (rows * seq)
+    gain_here = lax.dynamic_index_in_dim(
+        ffn_gain.astype(f32).reshape(rows, seq, share), here, 0, False
     )
-    part_out = part_out.reshape(rows, seq, tp, low * col).transpose(0, 2, 1, 3)
-    gain_here = lax.dynamic_index_in_dim(
-        ffn_gain.astype(f32).reshape(rows, seq, feat // (rows * seq)), here, 0, False
-    )
-    gain_sent = jnp.broadcast_to(gain_here, (rows, tp, *gain_here.shape))
-    sent = jnp.concatenate([part_out, gain_sent], axis=3).reshape(rows * tp, seq, -1)
-    got = exchange(sent, PAIR).reshape(rows, tp, seq, -1)
-    gain_all = got[:, :, :, low * col :].transpose(1, 0, 2, 3).reshape(tp, feat)
+    gain_sent = jnp.broadcast_to(gain_here, (rows, tp, seq, share))
+    rest = jnp.zeros((rows, tp, seq, LANES - low * col - share), f32)
+    sent = jnp.concatenate([part_out, gain_sent, rest], axis=3).reshape(rows * tp, seq, LANES)
+    got = exchange(sent, PAIR).reshape(rows, tp, seq, LANES)
+    gain_all = got[:, :, :, low * col : low * col + share].transpose(1, 0, 2, 3).reshape(width)
     mixer = got[:, :, :, : low * col].sum(axis=1).reshape(rows, seq, low, col)
     mixer = mixer.transpose(1, 2, 0, 3).reshape(seq, feat).astype(bf16)
     middle = (tokens.astype(f32) + mixer.astype(f32)).astype(bf16)
@@ -108,21 +115,26 @@
     chosen = jnp.sum(hits, axis=2).astype(bf16)
     weights = jnp.sum(hits * route_weights[None, :, :, None], axis=2)
     outgoing = jnp.einsum("ets,td->esd", chosen, middle, preferred_element_type=f32)
-    arrived = exchange(outgoing.astype(bf16), "zh").reshape(zh * cap, feat)
-    block = gathered(arrived, PAIR, rows * tp).reshape(rows, tp, zh * cap, feat)
+    arrived = exchange(outgoing.astype(bf16), "zh").transpose(1, 0, 2)
+    zl, x, c = (lax.axis_size(a) for a in ROW)
+    sent = jnp.broadcast_to(arrived[None, None, :, None], (zl, x, c, tp, zh, feat))
+    block = exchange(sent.reshape(rows * tp, zh, feat), PAIR).reshape(rows, tp, zh, feat)
 
-    whole = block.transpose(0, 2, 1, 3).reshape(rows * zh * cap, width).astype(f32)
+    whole = block.transpose(0, 2, 1, 3).reshape(rows * zh, width).astype(f32)
     mean_sq = jnp.mean(whole * whole, axis=1, keepdims=True)
-    second = (whole * lax.rsqrt(mean_sq + EPS) * gain_all.reshape(width)).astype(bf16)
-    gate = jnp.dot(second, w_gate[0], preferred_element_type=f32)
-    up = jnp.dot(second, w_up[0], preferred_element_type=f32)
-    hidden = (jax.nn.silu(gate) * up).astype(bf16)
-    piece = jnp.dot(hidden, w_down[0], preferred_element_type=f32).astype(bf16)
-    piece = piece.reshape(rows, zh * cap, tp, feat).transpose(0, 2, 1, 3)
+    second = (whole * lax.rsqrt(mean_sq + EPS) * gain_all).astype(bf16)
+    units = w_gate.shape[2]
+    piece = jnp.zeros((rows * zh, width), f32)
+    for w in (mine, other):
+        gate = jnp.einsum("rd,fd->rf", second, w[:units], preferred_element_type=f32)
+        up = jnp.einsum("rd,fd->rf", second, w[units : 2 * units], preferred_element_type=f32)
+        hidden = (jax.nn.silu(gate) * up).astype(bf16)
+        piece = piece + jnp.dot(hidden, w[2 * units :], preferred_element_type=f32)
+    piece = piece.astype(bf16).reshape(rows, zh, tp, feat).transpose(0, 2, 1, 3)
 
-    summed = exchange(piece.reshape(rows * tp, zh * cap, feat), PAIR)
-    summed = summed.astype(f32).sum(axis=0).astype(bf16)
-    returned = exchange(summed.reshape(zh, cap, feat), "zh").astype(f32)
+    summed = exchange(piece.reshape(rows * tp, zh, feat), PAIR).astype(f32)
+    summed = summed.reshape(zl, x, c, tp, zh, feat).sum(axis=(0, 1, 3)).astype(bf16)
+    returned = exchange(summed.transpose(1, 0, 2), "zh").astype(f32)
     routed = jnp.einsum("ets,esd->td", weights, returned, precision=lax.Precision.HIGHEST)
     mixed = (middle.astype(f32) + routed).astype(bf16)
     return mixed, new_state

time: 183 us -> 173 us (0.945)
  blocking collectives: 82.3 us -> 64.2 us
  starting transfers between devices: 39.5 us -> 47.7 us
    all_to_all x3, blocking collectives: 55 us -> 45.6 us  [exchange(): return lax.all_to_all(blocks, axes, split_axis=0, concat_axis=0, tiled=True)]
    all_gather x1 -> x3, blocking collectives: 27.3 us -> 18.6 us  [shards(): tok_all = lax.all_gather(tok_all, axis, tiled=True)]
    all_to_all x5, starting transfers between devices: 39.5 us -> 44.9 us  [exchange(): return lax.all_to_all(blocks, axes, split_axis=0, concat_axis=0, tiled=True)]
    ppermute x0 -> x1, starting transfers between devices: none -> 2.86 us  [shards(): other = lax.ppermute(mine, 'c', [(0, 1), (1, 0)])]
    dot_general x4 -> x6, matrix products: 2.35 us -> 3.95 us  [the longest x2 2.84 us: shards(): piece = piece + jnp.dot(hidden, w[2 * units:], preferred_element_type=f32)]
  transfers between devices with their start and end apart: 5 -> 6, of which waited for: 4 -> 5; matrix products, arithmetic and copies ran while one was open for 1% -> 1% of each run, Pallas kernels for 0% -> 0%
where the time goes in v2:
time: 173 us; the launch traced here: 172 us
  blocking collectives  64.2 us (37%)
  starting transfers between devices  47.7 us (28%)
  waiting for transfers between devices  38.3 us (22%)
  local copies, waits for them, and re-layouts  9.03 us (5%)
  matrix products  5.91 us (3%)
  other arithmetic  5.81 us (3%)
    all_to_all x3, blocking collectives, exchange(): return lax.all_to_all(blocks, axes, split_axis=0, concat_axis=0, tiled=True)  45.6 us
    all_to_all x5, starting transfers between devices, exchange(): return lax.all_to_all(blocks, axes, split_axis=0, concat_axis=0, tiled=True)  44.9 us
    all_to_all x5, waiting for transfers between devices, exchange(): return lax.all_to_all(blocks, axes, split_axis=0, concat_axis=0, tiled=True)  38.3 us
    all_gather x3, blocking collectives, shards(): tok_all = lax.all_gather(tok_all, axis, tiled=True)  18.6 us
  transfers between devices with their start and end apart: 6, of which 5 were waited for; matrix products, arithmetic and copies ran while one was open for 1% of the time, Pallas kernels for 0%

profile of v2, /device:TPU:1, one launch (start us, length us, event | category | flops | bytes accessed | tf_op | source)
XLA Modules:
  0.0 172.1 jit_solution(11702270478724123691)
XLA Ops:
  0.7 0.9 maximum_bitcast_fusion
  1.5 0.8 broadcast_in_dim.14
  2.4 15.6 %all-to-all-start = ((bf16[8,64,512]{2,1,0:T(8,128)(2,1)}), bf16[8,64,512]{2,1,0:T(8,128)(2,1)S(1)}, u32[]{:S(2)}, u32[]{:S(2)}) async-start(bf16[8,64,512]{2,1,0:T(8,128)(2,1)} %broadcast_in_dim.14), calls=%async_computation | async-start | bytes 1048576 | tf_op jit(solution)/shard_map/all_to_all | solution.py:18
  18.1 0.1 pad_maximum_fusion
  18.2 2.9 %collective-permute-start = (bf16[336,2048]{1,0:T(8,128)(2,1)S(1)}, bf16[336,2048]{1,0:T(8,128)(2,1)S(1)}, u32[]{:S(2)}, u32[]{:S(2)}) collective-permute-start(bf16[336,2048]{1,0:T(8,128)(2,1)S(1)} %pad_maximum_fusion), channel_id=1, source_target_pairs={{0,4},{4,0},{1,5},{5,1},{2,6},{6,2},{3,7},{7,3},{8,12},{12,8},{9,1... | collective-permute-start | bytes 4128776 | tf_op jit(solution)/shard_map/ppermute | solution.py:59
  21.1 2.7 %all-gather = bf16[2,4,512]{2,1,0:T(4,128)(2,1)S(1)} all-gather(bf16[1,4,512]{2,1,0:T(4,128)(2,1)S(1)} %bitcast.123), channel_id=1, replica_groups=mesh['zh'=8,'zl'=2,'x'=4,'c'=2,'tp'=4] {'c'}, dimensions={0}, use_global_device_ids=true | all-gather | bytes 12288 | tf_op jit(solution)/shard_map/all_gather | solution.py:57
  23.8 9.9 %all_gather.10 = bf16[32,512]{1,0:T(8,128)(2,1)S(1)} all-gather(bf16[8,512]{1,0:T(8,128)(2,1)S(1)} %reshape.196), channel_id=1, replica_groups=mesh['zh'=8,'zl'=2,'x'=4,'c'=2,'tp'=4] {'x'}, dimensions={0}, use_global_device_ids=true | all-gather | bytes 40960 | tf_op jit(solution)/shard_map/all_gather | solution.py:57
  33.7 6.0 %all_gather.11 = bf16[64,512]{1,0:T(8,128)(2,1)S(1)} all-gather(bf16[32,512]{1,0:T(8,128)(2,1)S(1)} %all_gather.10), channel_id=1, replica_groups=mesh['zh'=8,'zl'=2,'x'=4,'c'=2,'tp'=4] {'zl'}, dimensions={0}, use_global_device_ids=true | all-gather | bytes 98304 | tf_op jit(solution)/shard_map/all_gather | solution.py:57
  39.7 4.1 %all-to-all-done = bf16[8,64,512]{2,1,0:T(8,128)(2,1)S(1)} async-done(((bf16[8,64,512]{2,1,0:T(8,128)(2,1)}), bf16[8,64,512]{2,1,0:T(8,128)(2,1)S(1)}, u32[]{:S(2)}, u32[]{:S(2)}) %all-to-all-start) | async-done | bytes 524320 | tf_op jit(solution)/shard_map/all_to_all | solution.py:18
  43.9 0.1 fusion.16
  44.0 0.1 broadcast_in_dim.15
  44.1 0.1 copy.100
  44.2 0.3 convolution_bitcast_fusion
  44.6 0.1 pad_maximum_fusion.1
  44.7 0.7 copy.102
  45.5 15.0 %all-to-all-start.1 = ((f32[64,4,128]{2,1,0:T(4,128)}), f32[64,4,128]{2,1,0:T(4,128)S(1)}, u32[]{:S(2)}, u32[]{:S(2)}) async-start(f32[64,4,128]{2,1,0:T(4,128)} %copy.102), calls=%async_computation.1 | async-start | bytes 262144 | tf_op jit(solution)/shard_map/all_to_all | solution.py:18
  60.5 0.5 convert_element_type.107
  61.0 8.0 %all-to-all-done.1 = f32[64,4,128]{2,1,0:T(4,128)S(1)} async-done(((f32[64,4,128]{2,1,0:T(4,128)}), f32[64,4,128]{2,1,0:T(4,128)S(1)}, u32[]{:S(2)}, u32[]{:S(2)}) %all-to-all-start.1) | async-done | bytes 131104 | tf_op jit(solution)/shard_map/all_to_all | solution.py:18
  69.1 0.1 rsqrt_reduce_fusion
  69.3 0.6 copy.126
  69.9 0.9 reshape.177
  70.8 0.7 copy.104
  71.5 1.0 reshape.178
  72.6 0.1 broadcast_multiply_fusion
  72.7 1.8 %multiply_add_fusion = f32[4,4,128,128]{3,2,1,0:T(8,128)S(1)} fusion(f32[4,4,128,128]{3,2,1,0:T(8,128)} %param.23, f32[4,4,128]{2,1,0:T(4,128)S(1)} %slice_bitcast_fusion.1, f32[4,4,128]{2,1,0:T(4,128)S(1)} %get-tuple-element.12, f32[4,4,128]{2,1,0:T(4,128)S(1)} %get-tuple-element.13), kind=kLoop, calls=%fused_computation.16 | loop fusion | flops 786432 | bytes 2121728 | tf_op jit(solution)/shard_map/add | solution.py:80
  74.6 1.0 copy-done
  75.6 1.0 fusion.47
  76.5 0.1 multiply_reduce_fusion.1
  76.6 0.1 fusion.41
  76.7 0.7 broadcast_in_dim.17
  77.4 3.8 %all-to-all-start.2 = ((bf16[16,4,512]{2,1,0:T(4,128)(2,1)}), bf16[16,4,512]{2,1,0:T(4,128)(2,1)S(1)}, u32[]{:S(2)}, u32[]{:S(2)}) async-start(bf16[16,4,512]{2,1,0:T(4,128)(2,1)} %broadcast_in_dim.17), calls=%async_computation.2 | async-start | bytes 131072 | tf_op jit(solution)/shard_map/all_to_all | solution.py:18
  81.2 0.1 reshape.190
  81.3 0.2 convert_reduce_fusion
  81.6 5.4 %all-to-all-done.2 = bf16[16,4,512]{2,1,0:T(4,128)(2,1)S(1)} async-done(((bf16[16,4,512]{2,1,0:T(4,128)(2,1)}), bf16[16,4,512]{2,1,0:T(4,128)(2,1)S(1)}, u32[]{:S(2)}, u32[]{:S(2)}) %all-to-all-start.2) | async-done | bytes 65568 | tf_op jit(solution)/shard_map/all_to_all | solution.py:18
  87.0 0.2 convolution_bitcast_fusion.1
  87.2 0.1 copy.106
  87.4 0.8 maximum_maximum_fusion
  88.2 4.5 %all-to-all-start.3 = ((f32[64,4,128]{2,1,0:T(4,128)}), f32[64,4,128]{2,1,0:T(4,128)S(1)}, u32[]{:S(2)}, u32[]{:S(2)}) async-start(f32[64,4,128]{2,1,0:T(4,128)} %bitcast.27), calls=%async_computation.3 | async-start | bytes 262144 | tf_op jit(solution)/shard_map/all_to_all | solution.py:18
  92.8 0.1 fusion.34
  92.8 8.5 %all-to-all-done.3 = f32[64,4,128]{2,1,0:T(4,128)S(1)} async-done(((f32[64,4,128]{2,1,0:T(4,128)}), f32[64,4,128]{2,1,0:T(4,128)S(1)}, u32[]{:S(2)}, u32[]{:S(2)}) %all-to-all-start.3) | async-done | bytes 131104 | tf_op jit(solution)/shard_map/all_to_all | solution.py:18
  101.3 0.1 slice_reduce_fusion
  101.4 0.1 reshape.193
  101.5 0.1 reshape.191
  101.6 0.2 convolution_convert_fusion
  101.8 15.1 %all_to_all.40 = bf16[8,2,512]{2,1,0:T(2,128)(2,1)S(1)} all-to-all(bf16[8,2,512]{2,1,0:T(2,128)(2,1)S(1)} %copy.109), channel_id=1, replica_groups=mesh['zh'=8,'zl'=2,'x'=4,'c'=2,'tp'=4] {'zh'}, dimensions={0} | all-to-all | bytes 32768 | tf_op jit(solution)/shard_map/all_to_all | solution.py:18
  116.9 0.9 broadcast_in_dim.20
  117.8 6.0 %all-to-all-start.5 = ((bf16[64,8,512]{2,1,0:T(8,128)(2,1)}), bf16[64,8,512]{2,1,0:T(8,128)(2,1)S(1)}, u32[]{:S(2)}, u32[]{:S(2)}) async-start(bf16[64,8,512]{2,1,0:T(8,128)(2,1)} %bitcast.32), calls=%async_computation.5 | async-start | bytes 1048576 | tf_op jit(solution)/shard_map/all_to_all | solution.py:18
  123.8 0.1 slice_bitcast_fusion
  123.9 0.1 copy.113
  124.0 0.2 mul.157
  124.2 12.2 %all-to-all-done.5 = bf16[64,8,512]{2,1,0:T(8,128)(2,1)S(1)} async-done(((bf16[64,8,512]{2,1,0:T(8,128)(2,1)}), bf16[64,8,512]{2,1,0:T(8,128)(2,1)S(1)}, u32[]{:S(2)}, u32[]{:S(2)}) %all-to-all-start.5) | async-done | bytes 524320 | tf_op jit(solution)/shard_map/all_to_all | solution.py:18
  136.4 0.2 multiply_reduce_fusion
  136.7 0.1 copy.112
  136.7 0.1 rsqrt.33
  136.8 0.1 convert_element_type.138
  137.0 0.2 multiply_convert_fusion
  137.1 0.3 fusion.9
  137.5 2.0 %fusion.3 = f32[128,2048]{1,0:T(8,128)S(1)} fusion(bf16[128,2048]{1,0:T(8,128)(2,1)S(1)} %multiply_convert_fusion, bf16[336,2048]{1,0:T(8,128)(2,1)} %copy-done.1, f32[128,112]{0,1:T(8,128)S(1)} %fusion.9), kind=kOutput, calls=%fused_computation.9 | convolution fusion | flops 117526528 | bytes 2547712 | tf_op jit(solution)/shard_map/dot_general | solution.py:132
  139.5 0.3 fusion.14
  139.8 0.8 fusion
  140.6 16.7 %all_to_all.41 = bf16[64,8,512]{2,1,0:T(8,128)(2,1)S(1)} all-to-all(bf16[64,8,512]{2,1,0:T(8,128)(2,1)S(1)} %bitcast.104), channel_id=1, replica_groups=mesh['zh'=8,'zl'=2,'x'=4,'c'=2,'tp'=4] {'zl','x','c','tp'}, dimensions={0} | all-to-all | bytes 1048576 | tf_op jit(solution)/shard_map/all_to_all | solution.py:18
  157.3 0.1 reduce.4
  157.4 13.9 %all_to_all.42 = bf16[8,2,512]{2,1,0:T(2,128)(2,1)S(1)} all-to-all(bf16[8,2,512]{2,1,0:T(2,128)(2,1)S(1)} %copy.114), channel_id=1, replica_groups=mesh['zh'=8,'zl'=2,'x'=4,'c'=2,'tp'=4] {'zh'}, dimensions={0} | all-to-all | bytes 32768 | tf_op jit(solution)/shard_map/all_to_all | solution.py:18
  171.3 0.8 fusion.5
  (55 shorter events, 0.8 us)
Async XLA Ops:
  0.6 17.4 %copy-start.2 = (bf16[1,112,2048]{2,1,0:T(8,128)(2,1)S(1)}, bf16[1,112,2048]{2,1,0:T(8,128)(2,1)}, u32[]{:S(2)}) copy-start(bf16[1,112,2048]{2,1,0:T(8,128)(2,1)} %param.29) | copy-start | bytes 1376260
  0.6 17.4 %copy-start.3 = (bf16[1,2048,112]{1,2,0:T(8,128)(2,1)S(1)}, bf16[1,2048,112]{1,2,0:T(8,128)(2,1)}, u32[]{:S(2)}) copy-start(bf16[1,2048,112]{1,2,0:T(8,128)(2,1)} %param.28) | copy-start | bytes 1376260
  0.7 17.4 %copy-start.4 = (bf16[1,2048,112]{1,2,0:T(8,128)(2,1)S(1)}, bf16[1,2048,112]{1,2,0:T(8,128)(2,1)}, u32[]{:S(2)}) copy-start(bf16[1,2048,112]{1,2,0:T(8,128)(2,1)} %param.27) | copy-start | bytes 1376260
  2.4 41.5 %all-to-all-start = ((bf16[8,64,512]{2,1,0:T(8,128)(2,1)}), bf16[8,64,512]{2,1,0:T(8,128)(2,1)S(1)}, u32[]{:S(2)}, u32[]{:S(2)}) async-start(bf16[8,64,512]{2,1,0:T(8,128)(2,1)} %broadcast_in_dim.14), calls=%async_computation | async-start | bytes 1048576 | tf_op jit(solution)/shard_map/all_to_all | solution.py:18
  18.0 3.0 %copy-start.8 = (bf16[512]{0:T(512)(128)(2,1)S(1)}, bf16[512]{0:T(512)(128)(2,1)}, u32[]{:S(2)}) copy-start(bf16[512]{0:T(512)(128)(2,1)} %param.16) | copy-start | bytes 3076
  18.0 3.0 %copy-start.5 = (bf16[4,512]{1,0:T(4,128)(2,1)S(1)}, bf16[4,512]{1,0:T(4,128)(2,1)}, u32[]{:S(2)}) copy-start(bf16[4,512]{1,0:T(4,128)(2,1)} %param.15) | copy-start | bytes 12292
  18.2 21.6 %collective-permute-start = (bf16[336,2048]{1,0:T(8,128)(2,1)S(1)}, bf16[336,2048]{1,0:T(8,128)(2,1)S(1)}, u32[]{:S(2)}, u32[]{:S(2)}) collective-permute-start(bf16[336,2048]{1,0:T(8,128)(2,1)S(1)} %pad_maximum_fusion), channel_id=1, source_target_pairs={{0,4},{4,0},{1,5},{5,1},{2,6},{6,2},{3,7},{7,3},{8,12},{12,8},{9,1... | collective-permute-start | bytes 4128776 | tf_op jit(solution)/shard_map/ppermute | solution.py:59
  39.7 97.4 %copy-start.1 = (bf16[336,2048]{1,0:T(8,128)(2,1)}, bf16[336,2048]{1,0:T(8,128)(2,1)S(1)}, u32[]{:S(2)}) copy-start(bf16[336,2048]{1,0:T(8,128)(2,1)S(1)} %collective-permute-done) | copy-start | bytes 4128772
  44.0 16.5 %copy-start.12 = (bf16[128]{0:T(256)(128)(2,1)S(1)}, bf16[128]{0:T(256)(128)(2,1)}, u32[]{:S(2)}) copy-start(bf16[128]{0:T(256)(128)(2,1)} %param.21) | copy-start | bytes 772
  44.0 17.0 %copy-start.7 = (f32[512]{0:T(512)S(1)}, f32[512]{0:T(512)}, u32[]{:S(2)}) copy-start(f32[512]{0:T(512)} %param.20) | copy-start | bytes 6148
  45.5 23.6 %all-to-all-start.1 = ((f32[64,4,128]{2,1,0:T(4,128)}), f32[64,4,128]{2,1,0:T(4,128)S(1)}, u32[]{:S(2)}, u32[]{:S(2)}) async-start(f32[64,4,128]{2,1,0:T(4,128)} %copy.102), calls=%async_computation.1 | async-start | bytes 262144 | tf_op jit(solution)/shard_map/all_to_all | solution.py:18
  72.7 3.9 %copy-start.11 = (f32[128]{0:T(128)S(1)}, f32[128]{0:T(128)}, u32[]{:S(2)}) copy-start(f32[128]{0:T(128)} %convert_element_type.107) | copy-start | bytes 1540
  72.7 8.4 %copy-start.9 = (bf16[512]{0:T(512)(128)(2,1)S(1)}, bf16[512]{0:T(512)(128)(2,1)}, u32[]{:S(2)}) copy-start(bf16[512]{0:T(512)(128)(2,1)} %param.24) | copy-start | bytes 3076
  72.7 8.6 %copy-start.6 = (s32[4,2]{0,1:T(2,128)S(1)}, s32[4,2]{0,1:T(2,128)}, u32[]{:S(2)}) copy-start(s32[4,2]{0,1:T(2,128)} %param.25) | copy-start | bytes 100
  74.6 1.0 copy-start
  75.6 17.2 %copy-start.10 = (f32[4,2]{0,1:T(2,128)S(1)}, f32[4,2]{0,1:T(2,128)}, u32[]{:S(2)}) copy-start(f32[4,2]{0,1:T(2,128)} %param.26) | copy-start | bytes 100
  77.4 9.7 %all-to-all-start.2 = ((bf16[16,4,512]{2,1,0:T(4,128)(2,1)}), bf16[16,4,512]{2,1,0:T(4,128)(2,1)S(1)}, u32[]{:S(2)}, u32[]{:S(2)}) async-start(bf16[16,4,512]{2,1,0:T(4,128)(2,1)} %broadcast_in_dim.17), calls=%async_computation.2 | async-start | bytes 131072 | tf_op jit(solution)/shard_map/all_to_all | solution.py:18
  88.2 13.1 %all-to-all-start.3 = ((f32[64,4,128]{2,1,0:T(4,128)}), f32[64,4,128]{2,1,0:T(4,128)S(1)}, u32[]{:S(2)}, u32[]{:S(2)}) async-start(f32[64,4,128]{2,1,0:T(4,128)} %bitcast.27), calls=%async_computation.3 | async-start | bytes 262144 | tf_op jit(solution)/shard_map/all_to_all | solution.py:18
  117.8 18.6 %all-to-all-start.5 = ((bf16[64,8,512]{2,1,0:T(8,128)(2,1)}), bf16[64,8,512]{2,1,0:T(8,128)(2,1)S(1)}, u32[]{:S(2)}, u32[]{:S(2)}) async-start(bf16[64,8,512]{2,1,0:T(8,128)(2,1)} %bitcast.32), calls=%async_computation.5 | async-start | bytes 1048576 | tf_op jit(solution)/shard_map/all_to_all | solution.py:18

commit v3 on v2

v3 whole, which is shorter than its diff:
```python
import jax
import jax.numpy as jnp
from jax import lax
from jax.experimental import pallas as pl
from jax.experimental.pallas import tpu as pltpu
from jax.sharding import Mesh
from jax.sharding import PartitionSpec as P

EXPERTS = 8
EPS = 1e-06
LANES = 128
EP = ("zh", "zl", "x", "c")
ROW = ("zl", "x", "c")
PAIR = ("zl", "x", "c", "tp")
bf16 = jnp.bfloat16
f32 = jnp.float32


def exchange(blocks, axes):
    return lax.all_to_all(blocks, axes, split_axis=0, concat_axis=0, tiled=True)


def gathered(shard, axes, count):
    return exchange(jnp.broadcast_to(shard[None], (count, *shard.shape)), axes)


def slot_hits(experts, cap):
    positions = jnp.arange(experts.shape[1], dtype=jnp.int32)
    earlier = positions[None, :] < positions[:, None]
    same = experts[:, :, :, None, None] == experts[:, None, None, :, :]
    rank = jnp.sum(same & earlier[None, :, None, :, None], axis=(3, 4))
    matched = experts[None] == jnp.arange(EXPERTS, dtype=jnp.int32)[:, None, None, None]
    placed = rank[..., None] == jnp.arange(cap, dtype=jnp.int32)
    return (matched[..., None] & placed[None]).astype(f32)


def chosen_slots(experts, cap):
    return jnp.sum(slot_hits(experts, cap), axis=3)


def recurrence_kernel(
    width, got_ref, state_ref, floor_ref, gain_ref, out_ref, forget_ref, input_ref, held, sem
):
    copy = pltpu.make_async_copy(state_ref, held, sem)
    copy.start()
    sources, parts, seq, lanes = got_ref.shape
    heads = forget_ref.shape[0]
    half = sources // 2
    col = lanes // half
    summed = []
    for s in range(half):
        both = []
        for source in (s, s + half):
            block = got_ref[source, 0]
            for part in range(1, parts):
                block = block + got_ref[source, part]
            both.append(block)
        summed.append(jnp.concatenate(both, axis=0))
    stat = summed[0][:seq, lanes - 1 :]
    scale = lax.rsqrt(stat / width + EPS)
    scale = jnp.concatenate([scale, scale], axis=0)
    lane = lax.broadcasted_iota(jnp.int32, (2 * seq, lanes), 1) // col
    first = lax.broadcasted_iota(jnp.int32, (2 * seq, lanes), 0) < seq

    def columns(low, which):
        total = jnp.zeros((2 * seq, lanes), f32)
        at = (low * 3 + which) * col
        for s in range(half):
            moved = pltpu.roll(summed[s], (s * col - at) % lanes, 1)
            total = jnp.where(lane == s, moved, total)
        return total * scale

    rows = []
    for low in range(heads // 2):
        query, gate, value = (columns(low, which) for which in range(3))
        floor = jnp.where(first, floor_ref[2 * low][None, :], floor_ref[2 * low + 1][None, :])
        forget = floor + (1.0 - floor) / (1.0 + jnp.exp(-gate))
        query = query / (1.0 + jnp.exp(-query))
        for k in range(2):
            forget_ref[2 * low + k] = forget[k * seq : (k + 1) * seq]
            input_ref[2 * low + k] = value[k * seq : (k + 1) * seq]
        fresh = jnp.sum(query * (1.0 - forget), axis=1, keepdims=True)
        rows.append((fresh * value, (query * forget).T))
    copy.wait()
    gain = gain_ref[...].astype(f32)
    for low in range(heads // 2):
        fresh, kept = rows[low]
        old = []
        for k in range(2):
            for t in range(seq):
                r = k * seq + t
                old.append(
                    jnp.sum(kept[:, r : r + 1] * held[t, 2 * low + k], axis=0, keepdims=True)
                )
        reads = fresh + jnp.concatenate(old, axis=0)
        mean_sq = jnp.mean(reads * reads, axis=1, keepdims=True)
        normed = (reads * lax.rsqrt(mean_sq + EPS) * gain).astype(bf16)
        for k in range(2):
            head = 2 * low + k
            block = normed[k * seq : (k + 1) * seq]
            for n in range(out_ref.shape[0]):
                out_ref[n, :, head * lanes : (head + 1) * lanes] = block


def recurrence(width, got, state, floors, gain):
    sources, _, seq, lanes = got.shape
    heads = state.shape[1]
    return pl.pallas_call(
        lambda *refs: recurrence_kernel(width, *refs),
        out_shape=(
            jax.ShapeDtypeStruct((sources, seq, heads * lanes), bf16),
            jax.ShapeDtypeStruct((heads, seq, lanes), f32),
            jax.ShapeDtypeStruct((heads, seq, lanes), f32),
        ),
        in_specs=[
            pl.BlockSpec(memory_space=pltpu.VMEM),
            pl.BlockSpec(memory_space=pl.ANY),
            pl.BlockSpec(memory_space=pltpu.VMEM),
            pl.BlockSpec(memory_space=pltpu.VMEM),
        ],
        out_specs=tuple(pl.BlockSpec(memory_space=pltpu.VMEM) for _ in range(3)),
        scratch_shapes=[pltpu.VMEM(state.shape, f32), pltpu.SemaphoreType.DMA],
        name="recurrence",
    )(got, state, floors, gain)


def shards(
    tokens,
    norm_gain,
    w_query,
    w_forget,
    w_input,
    forget_floor,
    head_gain,
    w_output,
    state,
    ffn_gain,
    route_experts,
    route_weights,
    w_gate,
    w_up,
    w_down,
):
    tp = lax.axis_size("tp")
    rows = lax.axis_size(ROW)
    zh = lax.axis_size("zh")
    seq, feat = tokens.shape
    width = feat * tp
    heads, head = state.shape[1], state.shape[2]
    col = w_query.shape[1]
    low = zh // tp
    here = lax.axis_index(ROW)
    zl, x, c = (lax.axis_size(a) for a in ROW)
    cap = max(2, seq // 2)

    w_joint = jnp.concatenate([w_query, w_forget, w_input, w_output], axis=1).T
    w_all = gathered(w_joint, "zh", zh)

    routes = jnp.pad(route_experts.astype(bf16), ((0, 0), (0, feat - route_experts.shape[1])))
    all_rows = jnp.concatenate([tokens, routes], axis=0)
    for axis in reversed(ROW):
        all_rows = lax.all_gather(all_rows, axis, tiled=True)
    w_all, all_rows = lax.optimization_barrier((w_all, all_rows))
    all_rows = all_rows.reshape(rows, 2, seq, feat)
    tok_all = all_rows[:, 0].reshape(rows * seq, feat)
    experts_all = all_rows[:, 1, :, : route_experts.shape[1]].astype(jnp.int32)
    w_in = w_all[:, : 3 * col].reshape(tp, low * 3 * col, feat)
    w_out = w_all[:, 3 * col :].reshape(tp, low * col, feat)

    tok_all = tok_all.astype(f32)
    sum_sq = jnp.sum(tok_all * tok_all, axis=1)
    scaled = (tok_all * norm_gain.astype(f32)).astype(bf16)
    partial = jnp.einsum("td,pcd->tpc", scaled, w_in, preferred_element_type=f32)
    partial = partial.reshape(rows, seq, tp, low * 3 * col).transpose(0, 2, 1, 3)
    used = low * 3 * col
    share = feat // (rows * seq)
    gain_here = lax.dynamic_index_in_dim(
        ffn_gain.astype(f32).reshape(rows, seq, share), here, 0, False
    )
    gain_sent = jnp.broadcast_to(gain_here, (rows, tp, seq, share))
    stat = jnp.broadcast_to(sum_sq.reshape(rows, 1, seq, 1), (rows, tp, seq, LANES - used - share))
    sent = jnp.concatenate([partial, gain_sent, stat], axis=3).reshape(rows * tp, seq, LANES)
    got = exchange(sent, PAIR).reshape(rows, tp, seq, LANES)

    heads_sent, forget, inputs = recurrence(
        width, got, state, forget_floor.reshape(heads, head), head_gain.reshape(1, head)
    )
    forget, inputs = forget.transpose(1, 0, 2), inputs.transpose(1, 0, 2)
    new_state = forget[..., None] * state + (1.0 - forget)[..., None] * inputs[:, :, None, :]

    quarter = rows // tp
    sel = chosen_slots(experts_all, cap).reshape(EXPERTS, tp, quarter, seq, cap)
    sel = sel.transpose(0, 1, 4, 2, 3)
    eye = jnp.eye(rows, dtype=f32).reshape(tp, quarter, rows)
    sel = sel[:, :, :, :, None, :] * eye[None, :, None, :, :, None]
    sel = sel.reshape(EXPERTS * rows * cap, rows * seq).astype(bf16)

    heads_all = exchange(heads_sent, ROW).reshape(rows * seq, feat)
    part_out = jnp.einsum("td,pcd->tpc", heads_all, w_out, preferred_element_type=f32)
    residual = lax.dynamic_index_in_dim(
        tok_all.reshape(rows * seq, low, rows, col), here, 2, False
    ).reshape(rows * seq, 1, low * col)
    own = (jnp.arange(tp) == lax.axis_index("tp"))[None, :, None]
    with_tok = (part_out + jnp.where(own, residual, 0.0)).reshape(rows * seq, tp * low * col)

    outgoing = jnp.dot(sel, with_tok.astype(bf16), preferred_element_type=f32).astype(bf16)
    arrived = exchange(outgoing.reshape(zh * tp, cap * quarter, LANES), ("zh", "tp"))
    arrived = arrived.astype(f32).reshape(zh, tp, cap, quarter, LANES).sum(axis=1).astype(bf16)
    arrived = arrived.transpose(1, 2, 0, 3).reshape(cap, quarter * zh, LANES)
    sent = jnp.broadcast_to(
        arrived[None, None, :, None], (zl, x, c, tp, quarter * zh, LANES)
    ).reshape(rows * tp, quarter * zh, LANES)
    block = exchange(sent, PAIR).reshape(rows, tp, quarter * zh, LANES)

    def ordered(w):
        return w.reshape(zh, rows, col, -1).transpose(1, 0, 2, 3).reshape(width, -1)

    pair = lambda w: lax.ppermute(w, "c", [(0, 1), (1, 0)])
    gate_up = jnp.concatenate([ordered(w_gate[0]), ordered(w_up[0])], axis=1)
    down = w_down[0]
    gain_all = got[:, :, :, used : used + share].transpose(1, 0, 2, 3)
    gain_all = ordered(gain_all.reshape(width, 1)).reshape(width)

    whole = block.transpose(1, 2, 0, 3).reshape(rows * zh, width).astype(f32)
    mean_sq = jnp.mean(whole * whole, axis=1, keepdims=True)
    second = (whole * lax.rsqrt(mean_sq + EPS) * gain_all).astype(bf16)
    units = w_gate.shape[2]
    piece = jnp.zeros((rows * zh, width), f32)
    for w, w_d in ((gate_up, down), (pair(gate_up), pair(down))):
        both = jnp.dot(second, w, preferred_element_type=f32)
        hidden = (jax.nn.silu(both[:, :units]) * both[:, units:]).astype(bf16)
        piece = piece + jnp.dot(hidden, w_d, preferred_element_type=f32)
    piece = piece.astype(bf16).reshape(rows, zh, tp, feat).transpose(0, 2, 1, 3)

    rider = part_out.reshape(rows, seq, tp, low * col).transpose(0, 2, 1, 3)
    rider = jnp.pad(rider.astype(bf16), ((0, 0), (0, 0), (0, zh - seq), (0, LANES - low * col)))
    back = jnp.concatenate([piece, rider], axis=3).reshape(rows * tp, zh, feat + LANES)
    back = exchange(back, PAIR).astype(f32)
    summed = back[:, :, :feat].reshape(zl, x, c, tp, zh, feat).sum(axis=(0, 1, 3)).astype(bf16)
    returned = exchange(summed.transpose(1, 0, 2), "zh").astype(f32)
    mixer = back[:, :seq, feat : feat + low * col].reshape(rows, tp, seq, low, col).sum(axis=1)
    mixer = mixer.transpose(1, 2, 0, 3).reshape(seq, feat).astype(bf16)
    middle = (tokens.astype(f32) + mixer.astype(f32)).astype(bf16)

    hits = slot_hits(route_experts[None], cap)[:, 0]
    weights = jnp.sum(hits * route_weights[None, :, :, None], axis=2)
    routed = jnp.einsum("ets,esd->td", weights, returned, precision=lax.Precision.HIGHEST)
    mixed = (middle.astype(f32) + routed).astype(bf16)
    return mixed, new_state


def solution(mesh):
    torus = Mesh(mesh.devices.reshape(8, 2, 4, 2, mesh.shape["tp"]), (*EP, "tp"))
    in_specs = (
        P(EP, "tp"),
        P("tp"),
        P("tp", EP),
        P("tp", EP),
        P("tp", EP),
        P("tp"),
        P(),
        P("tp", EP),
        P(EP, "tp", None, None),
        P("tp"),
        P(EP, None),
        P(EP, None),
        P(EP, None, "tp"),
        P(EP, None, "tp"),
        P(EP, "tp", None),
    )
    out_specs = (P(EP, "tp"), P(EP, "tp", None, None))
    return jax.shard_map(
        shards, mesh=torus, in_specs=in_specs, out_specs=out_specs, check_vma=False
    )
```

time: 173 us -> 165 us (0.954)
  blocking collectives: 64.2 us -> 42 us
  starting transfers between devices: 47.7 us -> 54.6 us
  waiting for transfers between devices: 38.3 us -> 42 us
  Pallas kernels: 0 us -> 3.34 us
    all_to_all x3 -> x1, blocking collectives: 45.6 us -> 18.3 us  [exchange(): return lax.all_to_all(blocks, axes, split_axis=0, concat_axis=0, tiled=True)]
    all_to_all x5 -> x6, starting transfers between devices: 44.9 us -> 50.1 us  [exchange(): return lax.all_to_all(blocks, axes, split_axis=0, concat_axis=0, tiled=True)]
    all_gather x3, blocking collectives: 18.6 us -> 23.7 us  [shards(): all_rows = lax.all_gather(all_rows, axis, tiled=True)]
    all_to_all x5 -> x6, waiting for transfers between devices: 38.3 us -> 42 us  [exchange(): return lax.all_to_all(blocks, axes, split_axis=0, concat_axis=0, tiled=True)]
    pallas_call x0 -> x1, Pallas kernels: none -> 3.34 us  [recurrence(): pl.pallas_call(lambda *refs: recurrence_kernel(width, *refs), out_shape=(...]
    convert_element_type x2 -> x6, local copies, waits for them, and re-layouts: 0.03 us -> 2.16 us  [the longest x1 1.06 us: shards(): sel = sel.reshape(EXPERTS * rows * cap, rows * seq).astype(bf16)]
    reshape x3 -> x4, local copies, waits for them, and re-layouts: 2.72 us -> 0.98 us  [the longest x1 0.73 us: shards(): jnp.concatenate([partial, gain_sent, stat], axis=3)]
    ppermute x1 -> x2, starting transfers between devices: 2.86 us -> 4.45 us  [shards(): pair = lambda w: lax.ppermute(w, 'c', [(0, 1), (1, 0)])]
  transfers between devices with their start and end apart: 6 -> 8, of which waited for: 5 -> 6; matrix products, arithmetic and copies ran while one was open for 1% -> 7% of each run, Pallas kernels for 0% -> 0%
where the time goes in v3:
time: 165 us; the launch traced here: 164 us
  starting transfers between devices  54.6 us (33%)
  blocking collectives  42 us (25%)
  waiting for transfers between devices  42 us (25%)
  local copies, waits for them, and re-layouts  9.9 us (6%)
  other arithmetic  5.8 us (4%)
  matrix products  4.83 us (3%)
  Pallas kernels  3.34 us (2%)
    all_to_all x6, starting transfers between devices, exchange(): return lax.all_to_all(blocks, axes, split_axis=0, concat_axis=0, tiled=True)  50.1 us
    all_to_all x6, waiting for transfers between devices, exchange(): return lax.all_to_all(blocks, axes, split_axis=0, concat_axis=0, tiled=True)  42 us
    all_gather x3, blocking collectives, shards(): all_rows = lax.all_gather(all_rows, axis, tiled=True)  23.7 us
    all_to_all x1, blocking collectives, exchange(): return lax.all_to_all(blocks, axes, split_axis=0, concat_axis=0, tiled=True)  18.3 us
    ppermute x2, starting transfers between devices, shards(): pair = lambda w: lax.ppermute(w, 'c', [(0, 1), (1, 0)])  4.45 us
    pallas_call x1, Pallas kernels, recurrence(): pl.pallas_call(lambda *refs: recurrence_kernel(width, *refs), out_shape=(...  3.34 us
  transfers between devices with their start and end apart: 8, of which 6 were waited for; matrix products, arithmetic and copies ran while one was open for 7% of the time, Pallas kernels for 0%

profile of v3, /device:TPU:1, one launch (start us, length us, event | category | flops | bytes accessed | tf_op | source)
XLA Modules:
  0.0 163.7 jit_solution(10975908870607486552)
XLA Ops:
  0.7 0.8 maximum_bitcast_fusion
  1.5 0.8 broadcast_in_dim.25
  2.3 15.6 %all-to-all-start = ((bf16[8,64,512]{2,1,0:T(8,128)(2,1)}), bf16[8,64,512]{2,1,0:T(8,128)(2,1)S(1)}, u32[]{:S(2)}, u32[]{:S(2)}) async-start(bf16[8,64,512]{2,1,0:T(8,128)(2,1)} %broadcast_in_dim.25), calls=%async_computation | async-start | bytes 1048576 | tf_op jit(solution)/shard_map/all_to_all | solution.py:20
  18.0 0.1 copy.216
  18.1 0.1 reshape.268
  18.2 2.4 %all_gather.9 = bf16[16,512]{1,0:T(8,128)(2,1)S(1)} all-gather(bf16[8,512]{1,0:T(8,128)(2,1)S(1)} %fusion.19), channel_id=1, replica_groups=mesh['zh'=8,'zl'=2,'x'=4,'c'=2,'tp'=4] {'c'}, dimensions={0}, use_global_device_ids=true | all-gather | bytes 24576 | tf_op jit(solution)/shard_map/all_gather | solution.py:162
  20.6 9.9 %all_gather.10 = bf16[64,512]{1,0:T(8,128)(2,1)S(1)} all-gather(bf16[16,512]{1,0:T(8,128)(2,1)S(1)} %all_gather.9), channel_id=1, replica_groups=mesh['zh'=8,'zl'=2,'x'=4,'c'=2,'tp'=4] {'x'}, dimensions={0}, use_global_device_ids=true | all-gather | bytes 81920 | tf_op jit(solution)/shard_map/all_gather | solution.py:162
  30.5 11.4 %all_gather.11 = bf16[128,512]{1,0:T(8,128)(2,1)S(1)} all-gather(bf16[64,512]{1,0:T(8,128)(2,1)S(1)} %all_gather.10), channel_id=1, replica_groups=mesh['zh'=8,'zl'=2,'x'=4,'c'=2,'tp'=4] {'zl'}, dimensions={0}, use_global_device_ids=true | all-gather | bytes 196608 | tf_op jit(solution)/shard_map/all_gather | solution.py:162
  42.0 1.7 %all-to-all-done = bf16[8,64,512]{2,1,0:T(8,128)(2,1)S(1)} async-done(((bf16[8,64,512]{2,1,0:T(8,128)(2,1)}), bf16[8,64,512]{2,1,0:T(8,128)(2,1)S(1)}, u32[]{:S(2)}, u32[]{:S(2)}) %all-to-all-start) | async-done | bytes 524320 | tf_op jit(solution)/shard_map/all_to_all | solution.py:20
  43.8 0.1 copy.215
  43.9 0.1 convert_reduce_fusion.1
  44.0 0.1 fusion.8
  44.2 0.1 copy.184
  44.2 0.3 convolution_bitcast_fusion
  44.6 0.1 pad_maximum_fusion.1
  44.8 0.7 copy.186
  45.5 16.5 %all-to-all-start.1 = ((f32[64,4,128]{2,1,0:T(4,128)}), f32[64,4,128]{2,1,0:T(4,128)S(1)}, u32[]{:S(2)}, u32[]{:S(2)}) async-start(f32[64,4,128]{2,1,0:T(4,128)} %copy.186), calls=%async_computation.1 | async-start | bytes 262144 | tf_op jit(solution)/shard_map/all_to_all | solution.py:20
  62.2 0.3 copy.182
  62.5 0.3 multiply_convert_fusion
  62.8 1.1 convert_element_type.188
  63.9 6.7 %all-to-all-done.1 = f32[64,4,128]{2,1,0:T(4,128)S(1)} async-done(((f32[64,4,128]{2,1,0:T(4,128)}), f32[64,4,128]{2,1,0:T(4,128)S(1)}, u32[]{:S(2)}, u32[]{:S(2)}) %all-to-all-start.1) | async-done | bytes 131104 | tf_op jit(solution)/shard_map/all_to_all | solution.py:20
  70.6 0.6 copy-done.2
  71.2 3.3 %recurrence.1 = (bf16[16,4,512]{2,1,0:T(4,128)(2,1)}, f32[4,4,128]{2,1,0:T(4,128)}, f32[4,4,128]{2,1,0:T(4,128)}) custom-call(f32[16,4,4,128]{3,2,1,0:T(4,128)} %bitcast.122, f32[4,4,128,128]{3,2,1,0:T(8,128)} %refs_1_.1, f32[4,128]{1,0:T(4,128)} %bitcast.137, bf16[1,128]{1,0:T(2,128)(2,1)} %bitcast.138), custom_call_target="tpu_custom_call" | custom-call | tf_op jit(solution)/shard_map/recurrence/pallas_call | solution.py:108
  74.6 3.9 %all-to-all-start.2 = ((bf16[16,4,512]{2,1,0:T(4,128)(2,1)}), bf16[16,4,512]{2,1,0:T(4,128)(2,1)S(1)}, u32[]{:S(2)}, u32[]{:S(2)}) async-start(bf16[16,4,512]{2,1,0:T(4,128)(2,1)} %get-tuple-element.9), calls=%async_computation.2 | async-start | bytes 131072 | tf_op jit(solution)/shard_map/all_to_all | solution.py:20
  78.5 0.4 reshape.269
  79.1 5.4 %all-to-all-done.2 = bf16[16,4,512]{2,1,0:T(4,128)(2,1)S(1)} async-done(((bf16[16,4,512]{2,1,0:T(4,128)(2,1)}), bf16[16,4,512]{2,1,0:T(4,128)(2,1)S(1)}, u32[]{:S(2)}, u32[]{:S(2)}) %all-to-all-start.2) | async-done | bytes 65568 | tf_op jit(solution)/shard_map/all_to_all | solution.py:20
  84.4 0.2 add_convert_fusion
  84.6 0.2 fusion.2
  84.8 18.3 %all_to_all.35 = bf16[32,8,128]{2,1,0:T(8,128)(2,1)S(1)} all-to-all(bf16[32,8,128]{2,1,0:T(8,128)(2,1)S(1)} %fusion.2), channel_id=1, replica_groups=mesh['zh'=8,'zl'=2,'x'=4,'c'=2,'tp'=4] {'zh','tp'}, dimensions={0} | all-to-all | bytes 131072 | tf_op jit(solution)/shard_map/all_to_all | solution.py:20
  103.2 0.9 broadcast_in_dim.40
  104.1 6.1 %all-to-all-start.4 = ((bf16[64,32,128]{2,1,0:T(8,128)(2,1)}), bf16[64,32,128]{2,1,0:T(8,128)(2,1)S(1)}, u32[]{:S(2)}, u32[]{:S(2)}) async-start(bf16[64,32,128]{2,1,0:T(8,128)(2,1)} %bitcast.22), calls=%async_computation.4 | async-start | bytes 1048576 | tf_op jit(solution)/shard_map/all_to_all | solution.py:20
  110.1 2.5 %collective-permute-start.1 = (bf16[112,2048]{1,0:T(8,128)(2,1)S(1)}, bf16[112,2048]{1,0:T(8,128)(2,1)}, u32[]{:S(2)}, u32[]{:S(2)}) collective-permute-start(bf16[112,2048]{1,0:T(8,128)(2,1)S(1)} %bitcast.125), channel_id=1, source_target_pairs={{0,4},{4,0},{1,5},{5,1},{2,6},{6,2},{3,7},{7,3},{8,12},{12,8},{9,1... | collective-permute-start | bytes 1376264 | tf_op jit(solution)/shard_map/ppermute | solution.py:218
  112.7 0.3 copy.193
  113.0 0.3 copy.195
  113.3 0.4 pad_maximum_fusion
  113.8 1.3 copy.197
  115.1 2.0 %collective-permute-start = (bf16[2048,224]{0,1:T(8,128)(2,1)}, bf16[2048,224]{0,1:T(8,128)(2,1)S(1)}, u32[]{:S(2)}, u32[]{:S(2)}) collective-permute-start(bf16[2048,224]{0,1:T(8,128)(2,1)} %copy.197), channel_id=1, source_target_pairs={{0,4},{4,0},{1,5},{5,1},{2,6},{6,2},{3,7},{7,3},{8,12},{12,8},{9,1... | collective-permute-start | bytes 2752520 | tf_op jit(solution)/shard_map/ppermute | solution.py:218
  117.0 0.1 slice_bitcast_fusion
  117.2 0.1 reshape_reshape.3
  117.3 0.1 mul.118
  117.4 0.1 copy.198
  117.5 5.1 %all-to-all-done.4 = bf16[64,32,128]{2,1,0:T(8,128)(2,1)S(1)} async-done(((bf16[64,32,128]{2,1,0:T(8,128)(2,1)}), bf16[64,32,128]{2,1,0:T(8,128)(2,1)S(1)}, u32[]{:S(2)}, u32[]{:S(2)}) %all-to-all-start.4) | async-done | bytes 524320 | tf_op jit(solution)/shard_map/all_to_all | solution.py:20
  122.6 0.3 multiply_reduce_fusion
  123.0 0.1 rsqrt.12
  123.1 0.1 convert_element_type.229
  123.2 0.6 copy.189
  123.8 1.1 fusion.26
  125.0 0.3 fusion.12
  125.3 0.6 fusion.24
  125.9 1.4 fusion
  127.3 0.9 fusion.7
  128.2 4.7 %all-to-all-start.5 = ((bf16[64,8,640]{2,1,0:T(8,128)(2,1)}), bf16[64,8,640]{2,1,0:T(8,128)(2,1)S(1)}, u32[]{:S(2)}, u32[]{:S(2)}) async-start(bf16[64,8,640]{2,1,0:T(8,128)(2,1)} %bitcast.39), calls=%async_computation.5 | async-start | bytes 1310720 | tf_op jit(solution)/shard_map/all_to_all | solution.py:20
  133.0 0.2 convert_reduce_fusion.2
  133.3 0.1 select_reduce_fusion
  133.4 1.6 multiply_add_fusion
  135.0 11.9 %all-to-all-done.5 = bf16[64,8,640]{2,1,0:T(8,128)(2,1)S(1)} async-done(((bf16[64,8,640]{2,1,0:T(8,128)(2,1)}), bf16[64,8,640]{2,1,0:T(8,128)(2,1)S(1)}, u32[]{:S(2)}, u32[]{:S(2)}) %all-to-all-start.5) | async-done | bytes 655392 | tf_op jit(solution)/shard_map/all_to_all | solution.py:20
  147.0 0.2 reshape.264
  147.2 0.2 reduce_sum.95
  147.3 0.1 slice.52
  147.5 0.6 copy.235
  148.2 3.3 %all-to-all-start.6 = ((bf16[8,2,512]{2,1,0:T(2,128)(2,1)}), bf16[8,2,512]{2,1,0:T(2,128)(2,1)S(1)}, u32[]{:S(2)}, u32[]{:S(2)}) async-start(bf16[8,2,512]{2,1,0:T(2,128)(2,1)} %bitcast.107), calls=%async_computation.6 | async-start | bytes 32768 | tf_op jit(solution)/shard_map/all_to_all | solution.py:20
  151.5 0.1 reshape.271
  151.6 11.3 %all-to-all-done.6 = bf16[8,2,512]{2,1,0:T(2,128)(2,1)S(1)} async-done(((bf16[8,2,512]{2,1,0:T(2,128)(2,1)}), bf16[8,2,512]{2,1,0:T(2,128)(2,1)S(1)}, u32[]{:S(2)}, u32[]{:S(2)}) %all-to-all-start.6) | async-done | bytes 16416 | tf_op jit(solution)/shard_map/all_to_all | solution.py:20
  162.9 0.8 fusion.4
  (74 shorter events, 1.2 us)
Async XLA Ops:
  0.6 17.3 %copy-start.9 = (s32[4,2]{0,1:T(2,128)S(1)}, s32[4,2]{0,1:T(2,128)}, u32[]{:S(2)}) copy-start(s32[4,2]{0,1:T(2,128)} %param.25) | copy-start | bytes 100
  0.6 17.4 %copy-start.11 = (bf16[512]{0:T(512)(128)(2,1)S(1)}, bf16[512]{0:T(512)(128)(2,1)}, u32[]{:S(2)}) copy-start(bf16[512]{0:T(512)(128)(2,1)} %param.16) | copy-start | bytes 3076
  0.7 17.4 %copy-start.12 = (bf16[512]{0:T(512)(128)(2,1)S(1)}, bf16[512]{0:T(512)(128)(2,1)}, u32[]{:S(2)}) copy-start(bf16[512]{0:T(512)(128)(2,1)} %param.24) | copy-start | bytes 3076
  0.7 17.5 %copy-start.8 = (bf16[4,512]{1,0:T(4,128)(2,1)S(1)}, bf16[4,512]{1,0:T(4,128)(2,1)}, u32[]{:S(2)}) copy-start(bf16[4,512]{1,0:T(4,128)(2,1)} %param.15) | copy-start | bytes 12292
  2.3 41.4 %all-to-all-start = ((bf16[8,64,512]{2,1,0:T(8,128)(2,1)}), bf16[8,64,512]{2,1,0:T(8,128)(2,1)S(1)}, u32[]{:S(2)}, u32[]{:S(2)}) async-start(bf16[8,64,512]{2,1,0:T(8,128)(2,1)} %broadcast_in_dim.25), calls=%async_computation | async-start | bytes 1048576 | tf_op jit(solution)/shard_map/all_to_all | solution.py:20
  43.7 0.8 copy-start.1
  45.5 25.1 %all-to-all-start.1 = ((f32[64,4,128]{2,1,0:T(4,128)}), f32[64,4,128]{2,1,0:T(4,128)S(1)}, u32[]{:S(2)}, u32[]{:S(2)}) async-start(f32[64,4,128]{2,1,0:T(4,128)} %copy.186), calls=%async_computation.1 | async-start | bytes 262144 | tf_op jit(solution)/shard_map/all_to_all | solution.py:20
  70.6 0.6 copy-start.2
  74.6 9.8 %slice-start = ((bf16[8,64,512]{2,1,0:T(8,128)(2,1)}), bf16[8,16,512]{2,1,0:T(8,128)(2,1)S(1)}, s32[]{:S(2)}) async-start(bf16[8,64,512]{2,1,0:T(8,128)(2,1)} %copy-done.1), calls=%async_computation.7 | async-start | bytes 262144 | tf_op jit(solution)/shard_map/slice | solution.py:168
  74.6 9.8 %all-to-all-start.2 = ((bf16[16,4,512]{2,1,0:T(4,128)(2,1)}), bf16[16,4,512]{2,1,0:T(4,128)(2,1)S(1)}, u32[]{:S(2)}, u32[]{:S(2)}) async-start(bf16[16,4,512]{2,1,0:T(4,128)(2,1)} %get-tuple-element.9), calls=%async_computation.2 | async-start | bytes 131072 | tf_op jit(solution)/shard_map/all_to_all | solution.py:20
  84.6 25.5 %copy-start.6 = (bf16[1,112,2048]{2,1,0:T(8,128)(2,1)S(1)}, bf16[1,112,2048]{2,1,0:T(8,128)(2,1)}, u32[]{:S(2)}) copy-start(bf16[1,112,2048]{2,1,0:T(8,128)(2,1)} %param.29) | copy-start | bytes 1376260
  84.6 28.0 %copy-start.4 = (bf16[1,2048,112]{1,2,0:T(8,128)(2,1)S(1)}, bf16[1,2048,112]{1,2,0:T(8,128)(2,1)}, u32[]{:S(2)}) copy-start(bf16[1,2048,112]{1,2,0:T(8,128)(2,1)} %param.27) | copy-start | bytes 1376260
  104.1 18.5 %all-to-all-start.4 = ((bf16[64,32,128]{2,1,0:T(8,128)(2,1)}), bf16[64,32,128]{2,1,0:T(8,128)(2,1)S(1)}, u32[]{:S(2)}, u32[]{:S(2)}) async-start(bf16[64,32,128]{2,1,0:T(8,128)(2,1)} %bitcast.22), calls=%async_computation.4 | async-start | bytes 1048576 | tf_op jit(solution)/shard_map/all_to_all | solution.py:20
  110.1 2.9 %copy-start.5 = (bf16[1,2048,112]{1,2,0:T(8,128)(2,1)S(1)}, bf16[1,2048,112]{1,2,0:T(8,128)(2,1)}, u32[]{:S(2)}) copy-start(bf16[1,2048,112]{1,2,0:T(8,128)(2,1)} %param.28) | copy-start | bytes 1376260
  110.1 15.8 %collective-permute-start.1 = (bf16[112,2048]{1,0:T(8,128)(2,1)S(1)}, bf16[112,2048]{1,0:T(8,128)(2,1)}, u32[]{:S(2)}, u32[]{:S(2)}) collective-permute-start(bf16[112,2048]{1,0:T(8,128)(2,1)S(1)} %bitcast.125), channel_id=1, source_target_pairs={{0,4},{4,0},{1,5},{5,1},{2,6},{6,2},{3,7},{7,3},{8,12},{12,8},{9,1... | collective-permute-start | bytes 1376264 | tf_op jit(solution)/shard_map/ppermute | solution.py:218
  113.8 3.2 %copy-start.3 = (f32[64,4,128]{2,1,0:T(4,128)S(1)}, f32[64,4,128]{2,1,0:T(4,128)}, u32[]{:S(2)}) copy-start(f32[64,4,128]{2,1,0:T(4,128)} %copy-done.2) | copy-start | bytes 393220
  115.1 10.2 %collective-permute-start = (bf16[2048,224]{0,1:T(8,128)(2,1)}, bf16[2048,224]{0,1:T(8,128)(2,1)S(1)}, u32[]{:S(2)}, u32[]{:S(2)}) collective-permute-start(bf16[2048,224]{0,1:T(8,128)(2,1)} %copy.197), channel_id=1, source_target_pairs={{0,4},{4,0},{1,5},{5,1},{2,6},{6,2},{3,7},{7,3},{8,12},{12,8},{9,1... | collective-permute-start | bytes 2752520 | tf_op jit(solution)/shard_map/ppermute | solution.py:218
  127.3 6.0 %copy-start.13 = (f32[4,2]{0,1:T(2,128)S(1)}, f32[4,2]{0,1:T(2,128)}, u32[]{:S(2)}) copy-start(f32[4,2]{0,1:T(2,128)} %param.26) | copy-start | bytes 100
  127.3 6.1 %copy-start.10 = (f32[4,4,128]{2,1,0:T(4,128)S(1)}, f32[4,4,128]{2,1,0:T(4,128)}, u32[]{:S(2)}) copy-start(f32[4,4,128]{2,1,0:T(4,128)} %get-tuple-element.11) | copy-start | bytes 24580
  127.3 6.1 %copy-start.7 = (f32[4,4,128]{2,1,0:T(4,128)S(1)}, f32[4,4,128]{2,1,0:T(4,128)}, u32[]{:S(2)}) copy-start(f32[4,4,128]{2,1,0:T(4,128)} %get-tuple-element.10) | copy-start | bytes 24580
  127.3 6.1 %copy-start = (f32[4,4,128,128]{3,2,1,0:T(8,128)S(1)}, f32[4,4,128,128]{3,2,1,0:T(8,128)}, u32[]{:S(2)}) copy-start(f32[4,4,128,128]{3,2,1,0:T(8,128)} %refs_1_.1) | copy-start | bytes 3145732
  128.2 18.7 %all-to-all-start.5 = ((bf16[64,8,640]{2,1,0:T(8,128)(2,1)}), bf16[64,8,640]{2,1,0:T(8,128)(2,1)S(1)}, u32[]{:S(2)}, u32[]{:S(2)}) async-start(bf16[64,8,640]{2,1,0:T(8,128)(2,1)} %bitcast.39), calls=%async_computation.5 | async-start | bytes 1310720 | tf_op jit(solution)/shard_map/all_to_all | solution.py:20
  148.2 14.7 %all-to-all-start.6 = ((bf16[8,2,512]{2,1,0:T(2,128)(2,1)}), bf16[8,2,512]{2,1,0:T(2,128)(2,1)S(1)}, u32[]{:S(2)}, u32[]{:S(2)}) async-start(bf16[8,2,512]{2,1,0:T(2,128)(2,1)} %bitcast.107), calls=%async_computation.6 | async-start | bytes 32768 | tf_op jit(solution)/shard_map/all_to_all | solution.py:20

commit v4 on v3

--- a/solution.py
+++ b/solution.py
@@ -9,9 +9,10 @@
 EXPERTS = 8
 EPS = 1e-06
 LANES = 128
-EP = ("zh", "zl", "x", "c")
-ROW = ("zl", "x", "c")
-PAIR = ("zl", "x", "c", "tp")
+EP = ("zh", "zl", "xh", "xl", "c")
+ROW = ("zl", "xh", "xl", "c")
+PAIR = (*ROW, "tp")
+GATHER = ("zl", "xl", "xh", "c")
 bf16 = jnp.bfloat16
 f32 = jnp.float32
 
@@ -36,6 +37,10 @@
 
 def chosen_slots(experts, cap):
     return jnp.sum(slot_hits(experts, cap), axis=3)
+
+
+def resident(value):
+    return pltpu.with_memory_space_constraint(value, pltpu.VMEM)
 
 
 def recurrence_kernel(
@@ -121,7 +126,83 @@
         out_specs=tuple(pl.BlockSpec(memory_space=pltpu.VMEM) for _ in range(3)),
         scratch_shapes=[pltpu.VMEM(state.shape, f32), pltpu.SemaphoreType.DMA],
         name="recurrence",
-    )(got, state, floors, gain)
+    )(resident(got), state, floors, gain)
+
+
+def experts_kernel(
+    rows_v, gain_ref, gu0_ref, down0_ref, gu1_ref, down1_ref, rider_ref, out_ref,
+    second, gu_v, down_v, out_v, sems, out_sems,
+):
+    copies = [
+        pltpu.make_async_copy(src, dst, sems.at[n])
+        for n, (src, dst) in enumerate(
+            (
+                (gu0_ref, gu_v.at[0]),
+                (gu1_ref, gu_v.at[1]),
+                (down0_ref, down_v.at[0]),
+                (down1_ref, down_v.at[1]),
+            )
+        )
+    ]
+    for copy in copies:
+        copy.start()
+    sources, parts, height, lanes = rows_v.shape
+    count = parts * height
+    zh, feat = out_v.shape[2], out_v.shape[3] - lanes
+    out_v[:, :, :, feat:] = rider_ref[...]
+    total = jnp.zeros((count, lanes), f32)
+    for n in range(sources):
+        block = rows_v[n].reshape(count, lanes).astype(f32)
+        total = total + block * block
+    scale = lax.rsqrt(jnp.sum(total, axis=1, keepdims=True) / (sources * lanes) + EPS)
+    for n in range(sources):
+        block = rows_v[n].reshape(count, lanes).astype(f32)
+        second[:, n * lanes : (n + 1) * lanes] = (block * scale * gain_ref[n]).astype(bf16)
+    copies[0].wait()
+    copies[1].wait()
+    hidden = []
+    for k in range(2):
+        both = jnp.dot(second[...], gu_v[k], preferred_element_type=f32)
+        gate = both[:, :lanes]
+        hidden.append((gate / (1.0 + jnp.exp(-gate)) * both[:, lanes:]).astype(bf16))
+    copies[2].wait()
+    copies[3].wait()
+    outs = []
+    for part in range(parts):
+        at = slice(part * feat, (part + 1) * feat)
+        piece = jnp.dot(hidden[0], down_v[0, :, at], preferred_element_type=f32)
+        piece = piece + jnp.dot(hidden[1], down_v[1, :, at], preferred_element_type=f32)
+        out_v[:, part, :, :feat] = piece.astype(bf16).reshape(count // zh, zh, feat)
+        outs.append(pltpu.make_async_copy(out_v.at[:, part], out_ref.at[:, part], out_sems.at[part]))
+        outs[-1].start()
+    for copy in outs:
+        copy.wait()
+
+
+def experts(block, gain, weights_of, rider):
+    sources, parts, height, lanes = block.shape
+    (gate_up, down), (gate_up_1, down_1) = weights_of
+    zh = rider.shape[2]
+    feat = gate_up.shape[0] // parts
+    count = parts * height
+    whole = (count // zh, parts, zh, feat + lanes)
+    anywhere = pl.BlockSpec(memory_space=pl.ANY)
+    vmem = pl.BlockSpec(memory_space=pltpu.VMEM)
+    return pl.pallas_call(
+        experts_kernel,
+        out_shape=jax.ShapeDtypeStruct(whole, bf16),
+        in_specs=[vmem, vmem, anywhere, anywhere, anywhere, anywhere, vmem],
+        out_specs=anywhere,
+        scratch_shapes=[
+            pltpu.VMEM((count, gate_up.shape[0]), bf16),
+            pltpu.VMEM((2, *gate_up.shape), bf16),
+            pltpu.VMEM((2, *down.shape), bf16),
+            pltpu.VMEM(whole, bf16),
+            pltpu.SemaphoreType.DMA((4,)),
+            pltpu.SemaphoreType.DMA((parts,)),
+        ],
+        name="experts",
+    )(resident(block), gain, gate_up, down, gate_up_1, down_1, rider)
 
 
 def shards(
@@ -150,7 +231,8 @@
     col = w_query.shape[1]
     low = zh // tp
     here = lax.axis_index(ROW)
-    zl, x, c = (lax.axis_size(a) for a in ROW)
+    c = lax.axis_size("c")
+    chips = rows // c
     cap = max(2, seq // 2)
 
     w_joint = jnp.concatenate([w_query, w_forget, w_input, w_output], axis=1).T
@@ -158,12 +240,14 @@
 
     routes = jnp.pad(route_experts.astype(bf16), ((0, 0), (0, feat - route_experts.shape[1])))
     all_rows = jnp.concatenate([tokens, routes], axis=0)
-    for axis in reversed(ROW):
+    for axis in GATHER:
         all_rows = lax.all_gather(all_rows, axis, tiled=True)
-    w_all, all_rows = lax.optimization_barrier((w_all, all_rows))
-    all_rows = all_rows.reshape(rows, 2, seq, feat)
-    tok_all = all_rows[:, 0].reshape(rows * seq, feat)
+
+    all_rows = all_rows.reshape(2, 2, 2, 2, 2, seq, feat)
+    order = tuple(GATHER[::-1].index(axis) for axis in ROW)
+    all_rows = all_rows.transpose(*order, 4, 5, 6).reshape(rows, 2, seq, feat)
     experts_all = all_rows[:, 1, :, : route_experts.shape[1]].astype(jnp.int32)
+    w_all, tok_all = lax.optimization_barrier((w_all, all_rows[:, 0].reshape(rows * seq, feat)))
     w_in = w_all[:, : 3 * col].reshape(tp, low * 3 * col, feat)
     w_out = w_all[:, 3 * col :].reshape(tp, low * col, feat)
 
@@ -208,35 +292,29 @@
     arrived = arrived.astype(f32).reshape(zh, tp, cap, quarter, LANES).sum(axis=1).astype(bf16)
     arrived = arrived.transpose(1, 2, 0, 3).reshape(cap, quarter * zh, LANES)
     sent = jnp.broadcast_to(
-        arrived[None, None, :, None], (zl, x, c, tp, quarter * zh, LANES)
+        arrived[None, :, None], (chips, c, tp, quarter * zh, LANES)
     ).reshape(rows * tp, quarter * zh, LANES)
     block = exchange(sent, PAIR).reshape(rows, tp, quarter * zh, LANES)
 
     def ordered(w):
         return w.reshape(zh, rows, col, -1).transpose(1, 0, 2, 3).reshape(width, -1)
 
-    pair = lambda w: lax.ppermute(w, "c", [(0, 1), (1, 0)])
-    gate_up = jnp.concatenate([ordered(w_gate[0]), ordered(w_up[0])], axis=1)
-    down = w_down[0]
+    units = w_gate.shape[2]
+    fill = ((0, 0), (0, LANES - units))
+    gate_up = jnp.concatenate(
+        [jnp.pad(ordered(w_gate[0]), fill), jnp.pad(ordered(w_up[0]), fill)], axis=1
+    )
+    down = jnp.pad(w_down[0], fill[::-1])
+    weights_of = [(gate_up, down), tuple(lax.ppermute(w, "c", [(0, 1), (1, 0)]) for w in (gate_up, down))]
+
     gain_all = got[:, :, :, used : used + share].transpose(1, 0, 2, 3)
-    gain_all = ordered(gain_all.reshape(width, 1)).reshape(width)
-
-    whole = block.transpose(1, 2, 0, 3).reshape(rows * zh, width).astype(f32)
-    mean_sq = jnp.mean(whole * whole, axis=1, keepdims=True)
-    second = (whole * lax.rsqrt(mean_sq + EPS) * gain_all).astype(bf16)
-    units = w_gate.shape[2]
-    piece = jnp.zeros((rows * zh, width), f32)
-    for w, w_d in ((gate_up, down), (pair(gate_up), pair(down))):
-        both = jnp.dot(second, w, preferred_element_type=f32)
-        hidden = (jax.nn.silu(both[:, :units]) * both[:, units:]).astype(bf16)
-        piece = piece + jnp.dot(hidden, w_d, preferred_element_type=f32)
-    piece = piece.astype(bf16).reshape(rows, zh, tp, feat).transpose(0, 2, 1, 3)
-
+    gain_all = ordered(gain_all.reshape(width, 1)).reshape(rows, 1, LANES)
     rider = part_out.reshape(rows, seq, tp, low * col).transpose(0, 2, 1, 3)
     rider = jnp.pad(rider.astype(bf16), ((0, 0), (0, 0), (0, zh - seq), (0, LANES - low * col)))
-    back = jnp.concatenate([piece, rider], axis=3).reshape(rows * tp, zh, feat + LANES)
+    back = experts(block, gain_all, weights_of, rider)
+    back = back.reshape(rows * tp, zh, feat + LANES)
     back = exchange(back, PAIR).astype(f32)
-    summed = back[:, :, :feat].reshape(zl, x, c, tp, zh, feat).sum(axis=(0, 1, 3)).astype(bf16)
+    summed = back[:, :, :feat].reshape(chips, c, tp, zh, feat).sum(axis=(0, 2)).astype(bf16)
     returned = exchange(summed.transpose(1, 0, 2), "zh").astype(f32)
     mixer = back[:, :seq, feat : feat + low * col].reshape(rows, tp, seq, low, col).sum(axis=1)
     mixer = mixer.transpose(1, 2, 0, 3).reshape(seq, feat).astype(bf16)
@@ -250,7 +328,7 @@
 
 
 def solution(mesh):
-    torus = Mesh(mesh.devices.reshape(8, 2, 4, 2, mesh.shape["tp"]), (*EP, "tp"))
+    torus = Mesh(mesh.devices.reshape(8, 2, 2, 2, 2, mesh.shape["tp"]), (*EP, "tp"))
     in_specs = (
         P(EP, "tp"),
         P("tp"),

time: 165 us -> 174 us (1.055)
  blocking collectives: 42 us -> 61.2 us
  starting transfers between devices: 54.6 us -> 48.7 us
  Pallas kernels: 3.34 us -> 7.27 us
  matrix products: 4.83 us -> 1.41 us
  waiting for transfers between devices: 42 us -> 39.7 us
    all_to_all x1, blocking collectives: 18.3 us -> 30.5 us  [exchange(): return lax.all_to_all(blocks, axes, split_axis=0, concat_axis=0, tiled=True)]
    all_gather x3 -> x4, blocking collectives: 23.7 us -> 30.8 us  [shards(): all_rows = lax.all_gather(all_rows, axis, tiled=True)]
    all_to_all x6, starting transfers between devices: 50.1 us -> 44.4 us  [exchange(): return lax.all_to_all(blocks, axes, split_axis=0, concat_axis=0, tiled=True)]
    pallas_call x0 -> x1, Pallas kernels: none -> 4.12 us  [experts(): pl.pallas_call(experts_kernel, out_shape=jax.ShapeDtypeStruct(whole, bf16...]
    dot_general x4 -> x0, matrix products: 3.42 us -> none  [the longest x2 1.74 us: shards(): both = jnp.dot(second, w, preferred_element_type=f32)]
    all_to_all x6, waiting for transfers between devices: 42 us -> 39.6 us  [exchange(): return lax.all_to_all(blocks, axes, split_axis=0, concat_axis=0, tiled=True)]
  transfers between devices with their start and end apart: 8 -> 8, of which waited for: 6 -> 6; matrix products, arithmetic and copies ran while one was open for 7% -> 4% of each run, Pallas kernels for 0% -> 0%
where the time goes in v4:
time: 174 us; the launch traced here: 173 us
  blocking collectives  61.2 us (35%)
  starting transfers between devices  48.7 us (28%)
  waiting for transfers between devices  39.7 us (23%)
  local copies, waits for them, and re-layouts  9.16 us (5%)
  Pallas kernels  7.27 us (4%)
  other arithmetic  4.11 us (2%)
    all_to_all x6, starting transfers between devices, exchange(): return lax.all_to_all(blocks, axes, split_axis=0, concat_axis=0, tiled=True)  44.4 us
    all_to_all x6, waiting for transfers between devices, exchange(): return lax.all_to_all(blocks, axes, split_axis=0, concat_axis=0, tiled=True)  39.6 us
    all_gather x4, blocking collectives, shards(): all_rows = lax.all_gather(all_rows, axis, tiled=True)  30.8 us
    all_to_all x1, blocking collectives, exchange(): return lax.all_to_all(blocks, axes, split_axis=0, concat_axis=0, tiled=True)  30.5 us
    ppermute x2, starting transfers between devices, shards(): lax.ppermute(w, 'c', [(0, 1), (1, 0)])  4.33 us
    pallas_call x1, Pallas kernels, experts(): pl.pallas_call(experts_kernel, out_shape=jax.ShapeDtypeStruct(whole, bf16...  4.12 us
  transfers between devices with their start and end apart: 8, of which 6 were waited for; matrix products, arithmetic and copies ran while one was open for 4% of the time, Pallas kernels for 0%

profile of v4, /device:TPU:1, one launch (start us, length us, event | category | flops | bytes accessed | tf_op | source)
XLA Modules:
  0.0 172.8 jit_solution(337223758604925110)
XLA Ops:
  0.7 0.8 maximum_bitcast_fusion
  1.4 0.8 broadcast_in_dim.27
  2.3 15.8 %all-to-all-start = ((bf16[8,64,512]{2,1,0:T(8,128)(2,1)}), bf16[8,64,512]{2,1,0:T(8,128)(2,1)S(1)}, u32[]{:S(2)}, u32[]{:S(2)}) async-start(bf16[8,64,512]{2,1,0:T(8,128)(2,1)} %broadcast_in_dim.27), calls=%async_computation | async-start | bytes 1048576 | tf_op jit(solution)/shard_map/all_to_all | solution.py:21
  18.1 0.1 copy.217
  18.2 13.7 %all_gather.12 = bf16[16,512]{1,0:T(8,128)(2,1)S(1)} all-gather(bf16[8,512]{1,0:T(8,128)(2,1)S(1)} %fusion.9), channel_id=1, replica_groups=mesh['zh'=8,'zl'=2,'xh'=2,'xl'=2,'c'=2,'tp'=4] {'zl'}, dimensions={0}, use_global_device_ids=true | all-gather | bytes 24576 | tf_op jit(solution)/shard_map/all_gather | solution.py:244
  31.9 3.5 %all_gather.13 = bf16[32,512]{1,0:T(8,128)(2,1)S(1)} all-gather(bf16[16,512]{1,0:T(8,128)(2,1)S(1)} %all_gather.12), channel_id=1, replica_groups=mesh['zh'=8,'zl'=2,'xh'=2,'xl'=2,'c'=2,'tp'=4] {'xl'}, dimensions={0}, use_global_device_ids=true | all-gather | bytes 49152 | tf_op jit(solution)/shard_map/all_gather | solution.py:244
  35.5 5.2 %all_gather.14 = bf16[64,512]{1,0:T(8,128)(2,1)S(1)} all-gather(bf16[32,512]{1,0:T(8,128)(2,1)S(1)} %all_gather.13), channel_id=1, replica_groups=mesh['zh'=8,'zl'=2,'xh'=2,'xl'=2,'c'=2,'tp'=4] {'xh'}, dimensions={0}, use_global_device_ids=true | all-gather | bytes 98304 | tf_op jit(solution)/shard_map/all_gather | solution.py:244
  40.7 8.3 %all_gather.15 = bf16[128,512]{1,0:T(8,128)(2,1)S(1)} all-gather(bf16[64,512]{1,0:T(8,128)(2,1)S(1)} %all_gather.14), channel_id=1, replica_groups=mesh['zh'=8,'zl'=2,'xh'=2,'xl'=2,'c'=2,'tp'=4] {'c'}, dimensions={0}, use_global_device_ids=true | all-gather | bytes 196608 | tf_op jit(solution)/shard_map/all_gather | solution.py:244
  49.1 0.1 copy.216
  49.3 0.1 reshape.234
  49.4 0.1 convert_reduce_fusion.1
  49.5 0.1 multiply_convert_fusion.1
  49.7 0.1 broadcast_in_dim.29
  49.8 0.1 copy.189
  49.9 0.3 convolution_bitcast_fusion
  50.2 0.1 broadcast_in_dim.30
  50.3 0.1 pad_maximum_fusion
  50.4 0.1 copy.190
  50.5 0.7 copy.191
  51.2 10.1 %all-to-all-start.1 = ((f32[64,4,128]{2,1,0:T(4,128)}), f32[64,4,128]{2,1,0:T(4,128)S(1)}, u32[]{:S(2)}, u32[]{:S(2)}) async-start(f32[64,4,128]{2,1,0:T(4,128)} %copy.191), calls=%async_computation.1 | async-start | bytes 262144 | tf_op jit(solution)/shard_map/all_to_all | solution.py:21
  61.4 0.1 copy.186
  61.4 0.3 copy.187
  61.7 0.1 fusion.10
  61.8 8.1 %all-to-all-done.1 = f32[64,4,128]{2,1,0:T(4,128)S(1)} async-done(((f32[64,4,128]{2,1,0:T(4,128)}), f32[64,4,128]{2,1,0:T(4,128)S(1)}, u32[]{:S(2)}, u32[]{:S(2)}) %all-to-all-start.1) | async-done | bytes 131104 | tf_op jit(solution)/shard_map/all_to_all | solution.py:21
  69.9 3.2 %recurrence.1 = (bf16[16,4,512]{2,1,0:T(4,128)(2,1)}, f32[4,4,128]{2,1,0:T(4,128)}, f32[4,4,128]{2,1,0:T(4,128)}) custom-call(f32[16,4,4,128]{3,2,1,0:T(4,128)S(1)} %bitcast.90, f32[4,4,128,128]{3,2,1,0:T(8,128)} %refs_1_.1, f32[4,128]{1,0:T(4,128)} %bitcast.118, bf16[1,128]{1,0:T(2,128)(2,1)} %bitcast.119), custom_call_target="tpu_custom_call" | custom-call | tf_op jit(solution)/shard_map/recurrence/pallas_call | solution.py:113
  73.0 3.8 %all-to-all-start.2 = ((bf16[16,4,512]{2,1,0:T(4,128)(2,1)}), bf16[16,4,512]{2,1,0:T(4,128)(2,1)S(1)}, u32[]{:S(2)}, u32[]{:S(2)}) async-start(bf16[16,4,512]{2,1,0:T(4,128)(2,1)} %get-tuple-element.9), calls=%async_computation.2 | async-start | bytes 131072 | tf_op jit(solution)/shard_map/all_to_all | solution.py:21
  76.8 0.3 multiply_convert_fusion
  77.2 1.1 convert_element_type.151
  78.2 0.1 copy.192
  78.4 4.3 %all-to-all-done.2 = bf16[16,4,512]{2,1,0:T(4,128)(2,1)S(1)} async-done(((bf16[16,4,512]{2,1,0:T(4,128)(2,1)}), bf16[16,4,512]{2,1,0:T(4,128)(2,1)S(1)}, u32[]{:S(2)}, u32[]{:S(2)}) %all-to-all-start.2) | async-done | bytes 65568 | tf_op jit(solution)/shard_map/all_to_all | solution.py:21
  82.7 0.2 fusion.11
  82.9 0.2 fusion.2
  83.1 30.5 %all_to_all.35 = bf16[32,8,128]{2,1,0:T(8,128)(2,1)S(1)} all-to-all(bf16[32,8,128]{2,1,0:T(8,128)(2,1)S(1)} %fusion.2), channel_id=1, replica_groups=mesh['zh'=8,'zl'=2,'xh'=2,'xl'=2,'c'=2,'tp'=4] {'zh','tp'}, dimensions={0} | all-to-all | bytes 131072 | tf_op jit(solution)/shard_map/all_to_all | solution.py:21
  113.6 0.9 broadcast_in_dim.43
  114.5 6.0 %all-to-all-start.4 = ((bf16[64,32,128]{2,1,0:T(8,128)(2,1)}), bf16[64,32,128]{2,1,0:T(8,128)(2,1)S(1)}, u32[]{:S(2)}, u32[]{:S(2)}) async-start(bf16[64,32,128]{2,1,0:T(8,128)(2,1)} %bitcast.24), calls=%async_computation.4 | async-start | bytes 1048576 | tf_op jit(solution)/shard_map/all_to_all | solution.py:21
  120.6 0.3 copy.198
  121.0 0.7 copy-done.6
  121.6 0.3 copy.196
  122.0 0.2 fusion.5.gu0_ref
  122.2 2.4 %collective-permute-start = (bf16[2048,256]{1,0:T(8,128)(2,1)S(1)}, bf16[2048,256]{1,0:T(8,128)(2,1)S(1)}, u32[]{:S(2)}, u32[]{:S(2)}) collective-permute-start(bf16[2048,256]{1,0:T(8,128)(2,1)S(1)} %fusion.5.gu0_ref), channel_id=1, source_target_pairs={{0,4},{4,0},{1,5},{5,1},{2,6},{6,2},{3,7},{7,3},{8,12},{12,8},{9,1... | collective-permute-start | bytes 3145736 | tf_op jit(solution)/shard_map/ppermute | solution.py:308
  124.6 2.0 %collective-permute-start.1 = (bf16[128,2048]{1,0:T(8,128)(2,1)S(1)}, bf16[128,2048]{1,0:T(8,128)(2,1)}, u32[]{:S(2)}, u32[]{:S(2)}) collective-permute-start(bf16[128,2048]{1,0:T(8,128)(2,1)S(1)} %pad.22.down0_ref), channel_id=1, source_target_pairs={{0,4},{4,0},{1,5},{5,1},{2,6},{6,2},{3,7},{7,3},{8,12},{12,8},{9,1... | collective-permute-start | bytes 1572872 | tf_op jit(solution)/shard_map/ppermute | solution.py:308
  126.6 0.1 slice_bitcast_fusion
  126.8 0.1 reshape_reshape.6
  126.9 0.7 reshape_reshape.7.gain_ref
  127.6 0.1 copy.200
  127.7 0.7 pad.23.rider_ref
  128.4 0.1 collective-permute-done.1.down1_ref
  128.6 4.5 %all-to-all-done.4 = bf16[64,32,128]{2,1,0:T(8,128)(2,1)S(1)} async-done(((bf16[64,32,128]{2,1,0:T(8,128)(2,1)}), bf16[64,32,128]{2,1,0:T(8,128)(2,1)S(1)}, u32[]{:S(2)}, u32[]{:S(2)}) %all-to-all-start.4) | async-done | bytes 524320 | tf_op jit(solution)/shard_map/all_to_all | solution.py:21
  133.1 4.1 %experts.1 = bf16[16,4,8,640]{3,2,1,0:T(8,128)(2,1)} custom-call(bf16[16,4,32,128]{3,2,1,0:T(8,128)(2,1)S(1)} %bitcast.89, f32[16,1,128]{2,1,0:T(1,128)} %reshape_reshape.7.gain_ref, bf16[2048,256]{1,0:T(8,128)(2,1)} %copy-done, bf16[128,2048]{1,0:T(8,128)(2,1)} %copy-done.2, bf16[2048,256]{1,0:T(8,128)(2,1)} %copy-done.3, ...), custom_call_target="tpu_custom_call" | custom-call | tf_op jit(solution)/shard_map/experts/pallas_call | solution.py:191
  137.3 5.3 %all-to-all-start.5 = ((bf16[64,8,640]{2,1,0:T(8,128)(2,1)}), bf16[64,8,640]{2,1,0:T(8,128)(2,1)S(1)}, u32[]{:S(2)}, u32[]{:S(2)}) async-start(bf16[64,8,640]{2,1,0:T(8,128)(2,1)} %bitcast.93), calls=%async_computation.5 | async-start | bytes 1310720 | tf_op jit(solution)/shard_map/all_to_all | solution.py:21
  142.6 0.2 convert_reduce_fusion.2
  142.8 0.1 iota_compare_fusion.6
  142.9 0.1 select_reduce_fusion
  143.1 1.6 multiply_add_fusion
  144.7 11.8 %all-to-all-done.5 = bf16[64,8,640]{2,1,0:T(8,128)(2,1)S(1)} async-done(((bf16[64,8,640]{2,1,0:T(8,128)(2,1)}), bf16[64,8,640]{2,1,0:T(8,128)(2,1)S(1)}, u32[]{:S(2)}, u32[]{:S(2)}) %all-to-all-start.5) | async-done | bytes 655392 | tf_op jit(solution)/shard_map/all_to_all | solution.py:21
  156.5 0.1 slice.32
  156.6 0.1 reduce_sum.79
  156.7 0.6 copy.230
  157.3 3.3 %all-to-all-start.6 = ((bf16[8,2,512]{2,1,0:T(2,128)(2,1)}), bf16[8,2,512]{2,1,0:T(2,128)(2,1)S(1)}, u32[]{:S(2)}, u32[]{:S(2)}) async-start(bf16[8,2,512]{2,1,0:T(2,128)(2,1)} %bitcast.87), calls=%async_computation.6 | async-start | bytes 32768 | tf_op jit(solution)/shard_map/all_to_all | solution.py:21
  160.7 0.2 reshape.230
  160.9 0.2 reduce_sum.76
  161.1 0.1 reshape.235
  161.2 10.8 %all-to-all-done.6 = bf16[8,2,512]{2,1,0:T(2,128)(2,1)S(1)} async-done(((bf16[8,2,512]{2,1,0:T(2,128)(2,1)}), bf16[8,2,512]{2,1,0:T(2,128)(2,1)S(1)}, u32[]{:S(2)}, u32[]{:S(2)}) %all-to-all-start.6) | async-done | bytes 16416 | tf_op jit(solution)/shard_map/all_to_all | solution.py:21
  172.0 0.8 fusion.4
  (69 shorter events, 0.8 us)
Async XLA Ops:
  0.6 17.4 %copy-start.9 = (s32[4,2]{0,1:T(2,128)S(1)}, s32[4,2]{0,1:T(2,128)}, u32[]{:S(2)}) copy-start(s32[4,2]{0,1:T(2,128)} %param.25) | copy-start | bytes 100
  0.6 17.5 %copy-start.8 = (bf16[4,512]{1,0:T(4,128)(2,1)S(1)}, bf16[4,512]{1,0:T(4,128)(2,1)}, u32[]{:S(2)}) copy-start(bf16[4,512]{1,0:T(4,128)(2,1)} %param.15) | copy-start | bytes 12292
  2.3 47.0 %copy-start.11 = (bf16[512]{0:T(512)(128)(2,1)S(1)}, bf16[512]{0:T(512)(128)(2,1)}, u32[]{:S(2)}) copy-start(bf16[512]{0:T(512)(128)(2,1)} %param.16) | copy-start | bytes 3076
  2.3 47.0 %copy-start.12 = (bf16[512]{0:T(512)(128)(2,1)S(1)}, bf16[512]{0:T(512)(128)(2,1)}, u32[]{:S(2)}) copy-start(bf16[512]{0:T(512)(128)(2,1)} %param.24) | copy-start | bytes 3076
  2.3 47.3 %all-to-all-start = ((bf16[8,64,512]{2,1,0:T(8,128)(2,1)}), bf16[8,64,512]{2,1,0:T(8,128)(2,1)S(1)}, u32[]{:S(2)}, u32[]{:S(2)}) async-start(bf16[8,64,512]{2,1,0:T(8,128)(2,1)} %broadcast_in_dim.27), calls=%async_computation | async-start | bytes 1048576 | tf_op jit(solution)/shard_map/all_to_all | solution.py:21
  51.2 18.7 %all-to-all-start.1 = ((f32[64,4,128]{2,1,0:T(4,128)}), f32[64,4,128]{2,1,0:T(4,128)S(1)}, u32[]{:S(2)}, u32[]{:S(2)}) async-start(f32[64,4,128]{2,1,0:T(4,128)} %copy.191), calls=%async_computation.1 | async-start | bytes 262144 | tf_op jit(solution)/shard_map/all_to_all | solution.py:21
  73.0 9.7 %all-to-all-start.2 = ((bf16[16,4,512]{2,1,0:T(4,128)(2,1)}), bf16[16,4,512]{2,1,0:T(4,128)(2,1)S(1)}, u32[]{:S(2)}, u32[]{:S(2)}) async-start(bf16[16,4,512]{2,1,0:T(4,128)(2,1)} %get-tuple-element.9), calls=%async_computation.2 | async-start | bytes 131072 | tf_op jit(solution)/shard_map/all_to_all | solution.py:21
  82.9 37.7 %copy-start.5 = (bf16[1,2048,112]{1,2,0:T(8,128)(2,1)S(1)}, bf16[1,2048,112]{1,2,0:T(8,128)(2,1)}, u32[]{:S(2)}) copy-start(bf16[1,2048,112]{1,2,0:T(8,128)(2,1)} %param.28) | copy-start | bytes 1376260
  114.5 18.5 %all-to-all-start.4 = ((bf16[64,32,128]{2,1,0:T(8,128)(2,1)}), bf16[64,32,128]{2,1,0:T(8,128)(2,1)S(1)}, u32[]{:S(2)}, u32[]{:S(2)}) async-start(bf16[64,32,128]{2,1,0:T(8,128)(2,1)} %bitcast.24), calls=%async_computation.4 | async-start | bytes 1048576 | tf_op jit(solution)/shard_map/all_to_all | solution.py:21
  120.6 1.0 copy-start.6
  122.0 2.6 %copy-start.4 = (bf16[1,112,2048]{2,1,0:T(8,128)(2,1)S(1)}, bf16[1,112,2048]{2,1,0:T(8,128)(2,1)}, u32[]{:S(2)}) copy-start(bf16[1,112,2048]{2,1,0:T(8,128)(2,1)} %param.29) | copy-start | bytes 1376260
  122.2 5.5 %copy-start = (bf16[2048,256]{1,0:T(8,128)(2,1)}, bf16[2048,256]{1,0:T(8,128)(2,1)S(1)}, u32[]{:S(2)}) copy-start(bf16[2048,256]{1,0:T(8,128)(2,1)S(1)} %fusion.5.gu0_ref) | copy-start | bytes 3145732
  122.2 6.4 %collective-permute-start = (bf16[2048,256]{1,0:T(8,128)(2,1)S(1)}, bf16[2048,256]{1,0:T(8,128)(2,1)S(1)}, u32[]{:S(2)}, u32[]{:S(2)}) collective-permute-start(bf16[2048,256]{1,0:T(8,128)(2,1)S(1)} %fusion.5.gu0_ref), channel_id=1, source_target_pairs={{0,4},{4,0},{1,5},{5,1},{2,6},{6,2},{3,7},{7,3},{8,12},{12,8},{9,1... | collective-permute-start | bytes 3145736 | tf_op jit(solution)/shard_map/ppermute | solution.py:308
  124.6 8.5 %copy-start.2 = (bf16[128,2048]{1,0:T(8,128)(2,1)}, bf16[128,2048]{1,0:T(8,128)(2,1)S(1)}, u32[]{:S(2)}) copy-start(bf16[128,2048]{1,0:T(8,128)(2,1)S(1)} %pad.22.down0_ref) | copy-start | bytes 1572868
  124.6 3.9 %collective-permute-start.1 = (bf16[128,2048]{1,0:T(8,128)(2,1)S(1)}, bf16[128,2048]{1,0:T(8,128)(2,1)}, u32[]{:S(2)}, u32[]{:S(2)}) collective-permute-start(bf16[128,2048]{1,0:T(8,128)(2,1)S(1)} %pad.22.down0_ref), channel_id=1, source_target_pairs={{0,4},{4,0},{1,5},{5,1},{2,6},{6,2},{3,7},{7,3},{8,12},{12,8},{9,1... | collective-permute-start | bytes 1572872 | tf_op jit(solution)/shard_map/ppermute | solution.py:308
  128.6 4.5 %copy-start.3 = (bf16[2048,256]{1,0:T(8,128)(2,1)}, bf16[2048,256]{1,0:T(8,128)(2,1)S(1)}, u32[]{:S(2)}) copy-start(bf16[2048,256]{1,0:T(8,128)(2,1)S(1)} %collective-permute-done.gu1_ref) | copy-start | bytes 3145732
  137.2 5.7 %copy-start.13 = (f32[4,2]{0,1:T(2,128)S(1)}, f32[4,2]{0,1:T(2,128)}, u32[]{:S(2)}) copy-start(f32[4,2]{0,1:T(2,128)} %param.26) | copy-start | bytes 100
  137.2 5.8 %copy-start.10 = (f32[4,4,128]{2,1,0:T(4,128)S(1)}, f32[4,4,128]{2,1,0:T(4,128)}, u32[]{:S(2)}) copy-start(f32[4,4,128]{2,1,0:T(4,128)} %get-tuple-element.11) | copy-start | bytes 24580
  137.2 5.8 %copy-start.7 = (f32[4,4,128]{2,1,0:T(4,128)S(1)}, f32[4,4,128]{2,1,0:T(4,128)}, u32[]{:S(2)}) copy-start(f32[4,4,128]{2,1,0:T(4,128)} %get-tuple-element.10) | copy-start | bytes 24580
  137.3 5.8 %copy-start.1 = (f32[4,4,128,128]{3,2,1,0:T(8,128)S(1)}, f32[4,4,128,128]{3,2,1,0:T(8,128)}, u32[]{:S(2)}) copy-start(f32[4,4,128,128]{3,2,1,0:T(8,128)} %refs_1_.1) | copy-start | bytes 3145732
  137.3 19.2 %all-to-all-start.5 = ((bf16[64,8,640]{2,1,0:T(8,128)(2,1)}), bf16[64,8,640]{2,1,0:T(8,128)(2,1)S(1)}, u32[]{:S(2)}, u32[]{:S(2)}) async-start(bf16[64,8,640]{2,1,0:T(8,128)(2,1)} %bitcast.93), calls=%async_computation.5 | async-start | bytes 1310720 | tf_op jit(solution)/shard_map/all_to_all | solution.py:21
  157.3 14.7 %all-to-all-start.6 = ((bf16[8,2,512]{2,1,0:T(2,128)(2,1)}), bf16[8,2,512]{2,1,0:T(2,128)(2,1)S(1)}, u32[]{:S(2)}, u32[]{:S(2)}) async-start(bf16[8,2,512]{2,1,0:T(2,128)(2,1)} %bitcast.87), calls=%async_computation.6 | async-start | bytes 32768 | tf_op jit(solution)/shard_map/all_to_all | solution.py:21

commit v5 on v4

--- a/solution.py
+++ b/solution.py
@@ -9,10 +9,12 @@
 EXPERTS = 8
 EPS = 1e-06
 LANES = 128
-EP = ("zh", "zl", "xh", "xl", "c")
+ZH = ("za", "zm")
+EP = (*ZH, "zl", "xh", "xl", "c")
 ROW = ("zl", "xh", "xl", "c")
 PAIR = (*ROW, "tp")
-GATHER = ("zl", "xl", "xh", "c")
+WIDE = ("zm", *ROW)
+GATHER = ("zl", "zm", "xl", "xh", "c")
 bf16 = jnp.bfloat16
 f32 = jnp.float32
 
@@ -48,31 +50,31 @@
 ):
     copy = pltpu.make_async_copy(state_ref, held, sem)
     copy.start()
-    sources, parts, seq, lanes = got_ref.shape
-    heads = forget_ref.shape[0]
-    half = sources // 2
+    lanes = got_ref.shape[2]
+    heads, seq = forget_ref.shape[:2]
+    half = got_ref.shape[0] // heads
     col = lanes // half
-    summed = []
-    for s in range(half):
-        both = []
-        for source in (s, s + half):
-            block = got_ref[source, 0]
-            for part in range(1, parts):
-                block = block + got_ref[source, part]
-            both.append(block)
-        summed.append(jnp.concatenate(both, axis=0))
-    stat = summed[0][:seq, lanes - 1 :]
-    scale = lax.rsqrt(stat / width + EPS)
-    scale = jnp.concatenate([scale, scale], axis=0)
+    row = lax.broadcasted_iota(jnp.int32, (2 * seq, lanes), 0)
     lane = lax.broadcasted_iota(jnp.int32, (2 * seq, lanes), 1) // col
-    first = lax.broadcasted_iota(jnp.int32, (2 * seq, lanes), 0) < seq
+    first, early = row < seq, row % seq < seq // 2
+
+    def source(n):
+        block = got_ref[n]
+        block = block + pltpu.roll(block, 4, 0)
+        block = block + pltpu.roll(block, 2, 0)
+        return jnp.where(early, block, pltpu.roll(block, lanes // 2, 1))
+
+    summed = [
+        [jnp.where(first, source(2 * low * half + n), source((2 * low + 1) * half + n)) for n in range(half)]
+        for low in range(heads // 2)
+    ]
+    scale = lax.rsqrt(summed[0][0][:, 3 * col : 3 * col + 1] / width + EPS)
 
     def columns(low, which):
         total = jnp.zeros((2 * seq, lanes), f32)
-        at = (low * 3 + which) * col
-        for s in range(half):
-            moved = pltpu.roll(summed[s], (s * col - at) % lanes, 1)
-            total = jnp.where(lane == s, moved, total)
+        for n in range(half):
+            moved = pltpu.roll(summed[low][n], ((n - which) * col) % lanes, 1)
+            total = jnp.where(lane == n, moved, total)
         return total * scale
 
     rows = []
@@ -107,9 +109,8 @@
                 out_ref[n, :, head * lanes : (head + 1) * lanes] = block
 
 
-def recurrence(width, got, state, floors, gain):
-    sources, _, seq, lanes = got.shape
-    heads = state.shape[1]
+def recurrence(width, sources, got, state, floors, gain):
+    seq, heads, lanes = state.shape[:3]
     return pl.pallas_call(
         lambda *refs: recurrence_kernel(width, *refs),
         out_shape=(
@@ -224,7 +225,7 @@
 ):
     tp = lax.axis_size("tp")
     rows = lax.axis_size(ROW)
-    zh = lax.axis_size("zh")
+    zh = lax.axis_size(ZH)
     seq, feat = tokens.shape
     width = feat * tp
     heads, head = state.shape[1], state.shape[2]
@@ -235,39 +236,48 @@
     chips = rows // c
     cap = max(2, seq // 2)
 
-    w_joint = jnp.concatenate([w_query, w_forget, w_input, w_output], axis=1).T
-    w_all = gathered(w_joint, "zh", zh)
-
     routes = jnp.pad(route_experts.astype(bf16), ((0, 0), (0, feat - route_experts.shape[1])))
     all_rows = jnp.concatenate([tokens, routes], axis=0)
-    for axis in GATHER:
+    for axis in GATHER[:2]:
         all_rows = lax.all_gather(all_rows, axis, tiled=True)
 
-    all_rows = all_rows.reshape(2, 2, 2, 2, 2, seq, feat)
-    order = tuple(GATHER[::-1].index(axis) for axis in ROW)
-    all_rows = all_rows.transpose(*order, 4, 5, 6).reshape(rows, 2, seq, feat)
-    experts_all = all_rows[:, 1, :, : route_experts.shape[1]].astype(jnp.int32)
-    w_all, tok_all = lax.optimization_barrier((w_all, all_rows[:, 0].reshape(rows * seq, feat)))
-    w_in = w_all[:, : 3 * col].reshape(tp, low * 3 * col, feat)
-    w_out = w_all[:, 3 * col :].reshape(tp, low * col, feat)
+    w_joint = jnp.concatenate([w_query, w_forget, w_input, w_output], axis=1).T
+    w_joint, all_rows = lax.optimization_barrier((w_joint, all_rows))
+    w_all = gathered(w_joint, "za", tp)
+    for axis in GATHER[2:]:
+        all_rows = lax.all_gather(all_rows, axis, tiled=True)
+    all_rows = all_rows.reshape(2, 2, 2, 2, 2, 2, seq, feat)
+    order = tuple(GATHER[::-1].index(axis) for axis in WIDE)
+    all_rows = all_rows.transpose(*order, 5, 6, 7).reshape(2 * rows, 2, seq, feat)
+    mine = lax.dynamic_slice_in_dim(all_rows, lax.axis_index("zm") * rows, rows, 0)
+    experts_all = mine[:, 1, :, : route_experts.shape[1]].astype(jnp.int32)
+    tok_mine = mine[:, 0].reshape(rows * seq, feat)
+    w_all, tok_all = lax.optimization_barrier(
+        (w_all, all_rows[:, 0].reshape(2 * rows * seq, feat))
+    )
 
     tok_all = tok_all.astype(f32)
     sum_sq = jnp.sum(tok_all * tok_all, axis=1)
     scaled = (tok_all * norm_gain.astype(f32)).astype(bf16)
-    partial = jnp.einsum("td,pcd->tpc", scaled, w_in, preferred_element_type=f32)
-    partial = partial.reshape(rows, seq, tp, low * 3 * col).transpose(0, 2, 1, 3)
-    used = low * 3 * col
-    share = feat // (rows * seq)
+    partial = jnp.einsum("td,pcd->tpc", scaled, w_all[:, : 3 * col], preferred_element_type=f32)
+    partial = partial.reshape(2 * rows, seq, tp, 3 * col).transpose(0, 2, 1, 3)
+    share = feat // (2 * rows * seq)
+    rest = LANES // 2 - 3 * col - share
     gain_here = lax.dynamic_index_in_dim(
-        ffn_gain.astype(f32).reshape(rows, seq, share), here, 0, False
-    )
-    gain_sent = jnp.broadcast_to(gain_here, (rows, tp, seq, share))
-    stat = jnp.broadcast_to(sum_sq.reshape(rows, 1, seq, 1), (rows, tp, seq, LANES - used - share))
-    sent = jnp.concatenate([partial, gain_sent, stat], axis=3).reshape(rows * tp, seq, LANES)
-    got = exchange(sent, PAIR).reshape(rows, tp, seq, LANES)
+        ffn_gain.astype(f32).reshape(2 * rows, seq, share), lax.axis_index(WIDE), 0, False
+    )
+    gain_sent = jnp.broadcast_to(gain_here, (2 * rows, tp, seq, share))
+    stat = jnp.broadcast_to(sum_sq.reshape(2 * rows, 1, seq, 1), (2 * rows, tp, seq, rest))
+    sent = jnp.concatenate([partial, stat, gain_sent], axis=3)
+    sent = sent.reshape(2 * rows * tp, 2, seq // 2, LANES // 2).transpose(0, 2, 1, 3)
+    got = exchange(sent.reshape(2 * rows * tp, seq // 2, LANES), (*WIDE, "tp"))
+    got = got.reshape(2 * rows, tp * seq // 2, LANES)
+
+    w_out = lax.all_gather(w_all[:, 3 * col :], "zm", axis=1).reshape(tp, low * col, feat)
+    got, w_out = lax.optimization_barrier((got, w_out))
 
     heads_sent, forget, inputs = recurrence(
-        width, got, state, forget_floor.reshape(heads, head), head_gain.reshape(1, head)
+        width, rows, got, state, forget_floor.reshape(heads, head), head_gain.reshape(1, head)
     )
     forget, inputs = forget.transpose(1, 0, 2), inputs.transpose(1, 0, 2)
     new_state = forget[..., None] * state + (1.0 - forget)[..., None] * inputs[:, :, None, :]
@@ -282,13 +292,13 @@
     heads_all = exchange(heads_sent, ROW).reshape(rows * seq, feat)
     part_out = jnp.einsum("td,pcd->tpc", heads_all, w_out, preferred_element_type=f32)
     residual = lax.dynamic_index_in_dim(
-        tok_all.reshape(rows * seq, low, rows, col), here, 2, False
+        tok_mine.astype(f32).reshape(rows * seq, low, rows, col), here, 2, False
     ).reshape(rows * seq, 1, low * col)
     own = (jnp.arange(tp) == lax.axis_index("tp"))[None, :, None]
     with_tok = (part_out + jnp.where(own, residual, 0.0)).reshape(rows * seq, tp * low * col)
 
     outgoing = jnp.dot(sel, with_tok.astype(bf16), preferred_element_type=f32).astype(bf16)
-    arrived = exchange(outgoing.reshape(zh * tp, cap * quarter, LANES), ("zh", "tp"))
+    arrived = exchange(outgoing.reshape(zh * tp, cap * quarter, LANES), (*ZH, "tp"))
     arrived = arrived.astype(f32).reshape(zh, tp, cap, quarter, LANES).sum(axis=1).astype(bf16)
     arrived = arrived.transpose(1, 2, 0, 3).reshape(cap, quarter * zh, LANES)
     sent = jnp.broadcast_to(
@@ -307,7 +317,8 @@
     down = jnp.pad(w_down[0], fill[::-1])
     weights_of = [(gate_up, down), tuple(lax.ppermute(w, "c", [(0, 1), (1, 0)]) for w in (gate_up, down))]
 
-    gain_all = got[:, :, :, used : used + share].transpose(1, 0, 2, 3)
+    gain_all = got.reshape(2 * rows, tp, seq // 2, 2, LANES // 2)[..., LANES // 2 - share :]
+    gain_all = gain_all.transpose(1, 0, 3, 2, 4)
     gain_all = ordered(gain_all.reshape(width, 1)).reshape(rows, 1, LANES)
     rider = part_out.reshape(rows, seq, tp, low * col).transpose(0, 2, 1, 3)
     rider = jnp.pad(rider.astype(bf16), ((0, 0), (0, 0), (0, zh - seq), (0, LANES - low * col)))
@@ -315,7 +326,7 @@
     back = back.reshape(rows * tp, zh, feat + LANES)
     back = exchange(back, PAIR).astype(f32)
     summed = back[:, :, :feat].reshape(chips, c, tp, zh, feat).sum(axis=(0, 2)).astype(bf16)
-    returned = exchange(summed.transpose(1, 0, 2), "zh").astype(f32)
+    returned = exchange(summed.transpose(1, 0, 2), ZH).astype(f32)
     mixer = back[:, :seq, feat : feat + low * col].reshape(rows, tp, seq, low, col).sum(axis=1)
     mixer = mixer.transpose(1, 2, 0, 3).reshape(seq, feat).astype(bf16)
     middle = (tokens.astype(f32) + mixer.astype(f32)).astype(bf16)
@@ -328,7 +339,7 @@
 
 
 def solution(mesh):
-    torus = Mesh(mesh.devices.reshape(8, 2, 2, 2, 2, mesh.shape["tp"]), (*EP, "tp"))
+    torus = Mesh(mesh.devices.reshape(4, 2, 2, 2, 2, 2, mesh.shape["tp"]), (*EP, "tp"))
     in_specs = (
         P(EP, "tp"),
         P("tp"),

time: 174 us -> 171 us (0.983)
  waiting for transfers between devices: 39.7 us -> 30.4 us
  starting transfers between devices: 48.7 us -> 54.5 us
  blocking collectives: 61.2 us -> 56 us
  local copies, waits for them, and re-layouts: 9.16 us -> 12.7 us
    all_to_all x6, waiting for transfers between devices: 39.6 us -> 30.4 us  [exchange(): return lax.all_to_all(blocks, axes, split_axis=0, concat_axis=0, tiled=True)]
    all_gather x0 -> x1, blocking collectives: none -> 7.68 us  [shards(): lax.all_gather(w_all[:, 3 * col:], 'zm', axis=1)]
    all_to_all x1, blocking collectives: 30.5 us -> 23.3 us  [exchange(): return lax.all_to_all(blocks, axes, split_axis=0, concat_axis=0, tiled=True)]
    all_to_all x6, starting transfers between devices: 44.4 us -> 50.1 us  [exchange(): return lax.all_to_all(blocks, axes, split_axis=0, concat_axis=0, tiled=True)]
    all_gather x4 -> x5, blocking collectives: 30.8 us -> 25.1 us  [shards(): all_rows = lax.all_gather(all_rows, axis, tiled=True)]
    unnamed x33 -> x37, local copies, waits for them, and re-layouts: 2.12 us -> 3.59 us
  transfers between devices with their start and end apart: 8 -> 8, of which waited for: 6 -> 5; matrix products, arithmetic and copies ran while one was open for 4% -> 7% of each run, Pallas kernels for 0% -> 0%
where the time goes in v5:
time: 171 us; the launch traced here: 170 us
  blocking collectives  56 us (33%)
  starting transfers between devices  54.5 us (32%)
  waiting for transfers between devices  30.4 us (18%)
  local copies, waits for them, and re-layouts  12.7 us (7%)
  Pallas kernels  7.23 us (4%)
  other arithmetic  5.67 us (3%)
  matrix products  2.02 us (1%)
    all_to_all x6, starting transfers between devices, exchange(): return lax.all_to_all(blocks, axes, split_axis=0, concat_axis=0, tiled=True)  50.1 us
    all_to_all x6, waiting for transfers between devices, exchange(): return lax.all_to_all(blocks, axes, split_axis=0, concat_axis=0, tiled=True)  30.4 us
    all_gather x5, blocking collectives, shards(): all_rows = lax.all_gather(all_rows, axis, tiled=True)  25.1 us
    all_to_all x1, blocking collectives, exchange(): return lax.all_to_all(blocks, axes, split_axis=0, concat_axis=0, tiled=True)  23.3 us
    all_gather x1, blocking collectives, shards(): lax.all_gather(w_all[:, 3 * col:], 'zm', axis=1)  7.68 us
    ppermute x2, starting transfers between devices, shards(): lax.ppermute(w, 'c', [(0, 1), (1, 0)])  4.33 us
    pallas_call x1, Pallas kernels, experts(): pl.pallas_call(experts_kernel, out_shape=jax.ShapeDtypeStruct(whole, bf16...  4.13 us
    unnamed x37, local copies, waits for them, and re-layouts  3.59 us
  transfers between devices with their start and end apart: 8, of which 5 were waited for; matrix products, arithmetic and copies ran while one was open for 7% of the time, Pallas kernels for 0%

profile of v5, /device:TPU:1, one launch (start us, length us, event | category | flops | bytes accessed | tf_op | source)
XLA Modules:
  0.0 169.8 jit_solution(7177965887072912117)
XLA Ops:
  0.6 0.7 convert_element_type.151
  1.3 0.1 copy.218
  1.4 0.7 fusion.15
  2.1 4.2 %all_gather.21 = bf16[16,512]{1,0:T(8,128)(2,1)S(1)} all-gather(bf16[8,512]{1,0:T(8,128)(2,1)S(1)} %fusion.15), channel_id=1, replica_groups=mesh['za'=4,'zm'=2,'zl'=2,'xh'=2,'xl'=2,'c'=2,'tp'=4] {'zl'}, dimensions={0}, use_global_device_ids=true | all-gather | bytes 24576 | tf_op jit(solution)/shard_map/all_gather | solution.py:242
  6.3 4.8 %all_gather.22 = bf16[32,512]{1,0:T(8,128)(2,1)S(1)} all-gather(bf16[16,512]{1,0:T(8,128)(2,1)S(1)} %all_gather.21), channel_id=1, replica_groups=mesh['za'=4,'zm'=2,'zl'=2,'xh'=2,'xl'=2,'c'=2,'tp'=4] {'zm'}, dimensions={0}, use_global_device_ids=true | all-gather | bytes 49152 | tf_op jit(solution)/shard_map/all_gather | solution.py:242
  11.0 0.8 maximum_bitcast_fusion
  11.8 0.7 broadcast_in_dim.27
  12.5 14.0 %all-to-all-start = ((bf16[4,64,512]{2,1,0:T(8,128)(2,1)}), bf16[4,64,512]{2,1,0:T(8,128)(2,1)S(1)}, u32[]{:S(2)}, u32[]{:S(2)}) async-start(bf16[4,64,512]{2,1,0:T(8,128)(2,1)} %broadcast_in_dim.27), calls=%async_computation | async-start | bytes 524288 | tf_op jit(solution)/shard_map/all_to_all | solution.py:23
  26.6 3.5 %all_gather.23 = bf16[64,512]{1,0:T(8,128)(2,1)S(1)} all-gather(bf16[32,512]{1,0:T(8,128)(2,1)S(1)} %all_gather.22), channel_id=1, replica_groups=mesh['za'=4,'zm'=2,'zl'=2,'xh'=2,'xl'=2,'c'=2,'tp'=4] {'xl'}, dimensions={0}, use_global_device_ids=true | all-gather | bytes 98304 | tf_op jit(solution)/shard_map/all_gather | solution.py:248
  30.1 5.3 %all_gather.24 = bf16[128,512]{1,0:T(8,128)(2,1)S(1)} all-gather(bf16[64,512]{1,0:T(8,128)(2,1)S(1)} %all_gather.23), channel_id=1, replica_groups=mesh['za'=4,'zm'=2,'zl'=2,'xh'=2,'xl'=2,'c'=2,'tp'=4] {'xh'}, dimensions={0}, use_global_device_ids=true | all-gather | bytes 196608 | tf_op jit(solution)/shard_map/all_gather | solution.py:248
  35.4 7.3 %all_gather.25 = bf16[256,512]{1,0:T(8,128)(2,1)S(1)} all-gather(bf16[128,512]{1,0:T(8,128)(2,1)S(1)} %all_gather.24), channel_id=1, replica_groups=mesh['za'=4,'zm'=2,'zl'=2,'xh'=2,'xl'=2,'c'=2,'tp'=4] {'c'}, dimensions={0}, use_global_device_ids=true | all-gather | bytes 393216 | tf_op jit(solution)/shard_map/all_gather | solution.py:248
  42.8 0.1 copy.181
  43.0 0.1 copy.215
  43.1 0.1 reshape.240
  43.4 0.1 convert_reduce_fusion.1
  43.5 0.1 fusion.7
  43.6 0.1 broadcast_in_dim.28
  43.8 0.3 fusion.8
  44.2 0.3 pad_maximum_fusion
  44.5 0.2 copy.188
  44.7 0.1 copy.189
  44.8 0.8 copy.190
  45.6 14.6 %all-to-all-start.1 = ((f32[128,2,128]{2,1,0:T(2,128)}), f32[128,2,128]{2,1,0:T(2,128)S(1)}, u32[]{:S(2)}, u32[]{:S(2)}) async-start(f32[128,2,128]{2,1,0:T(2,128)} %copy.190), calls=%async_computation.1 | async-start | bytes 262144 | tf_op jit(solution)/shard_map/all_to_all | solution.py:23
  60.2 0.3 copy.186
  60.6 0.3 multiply_convert_fusion
  61.0 7.7 %all-gather = bf16[4,32,512]{2,1,0:T(8,128)(2,1)S(1)} all-gather(bf16[4,16,512]{2,1,0:T(8,128)(2,1)S(1)} %slice.27), channel_id=2, replica_groups=mesh['za'=4,'zm'=2,'zl'=2,'xh'=2,'xl'=2,'c'=2,'tp'=4] {'zm'}, dimensions={1}, use_global_device_ids=true | all-gather | bytes 196608 | tf_op jit(solution)/shard_map/all_gather | solution.py:276
  68.6 1.8 %all-to-all-done.1 = f32[128,2,128]{2,1,0:T(2,128)S(1)} async-done(((f32[128,2,128]{2,1,0:T(2,128)}), f32[128,2,128]{2,1,0:T(2,128)S(1)}, u32[]{:S(2)}, u32[]{:S(2)}) %all-to-all-start.1) | async-done | bytes 131104 | tf_op jit(solution)/shard_map/all_to_all | solution.py:23
  70.4 3.1 %recurrence.1 = (bf16[16,4,512]{2,1,0:T(4,128)(2,1)}, f32[4,4,128]{2,1,0:T(4,128)}, f32[4,4,128]{2,1,0:T(4,128)}) custom-call(f32[32,8,128]{2,1,0:T(8,128)S(1)} %bitcast.93, f32[4,4,128,128]{3,2,1,0:T(8,128)} %refs_1_.1, f32[4,128]{1,0:T(4,128)} %bitcast.121, bf16[1,128]{1,0:T(2,128)(2,1)} %bitcast.122), custom_call_target="tpu_custom_call" | custom-call | tf_op jit(solution)/shard_map/recurrence/pallas_call | solution.py:114
  73.5 4.5 %all-to-all-start.2 = ((bf16[16,4,512]{2,1,0:T(4,128)(2,1)}), bf16[16,4,512]{2,1,0:T(4,128)(2,1)S(1)}, u32[]{:S(2)}, u32[]{:S(2)}) async-start(bf16[16,4,512]{2,1,0:T(4,128)(2,1)} %get-tuple-element.16), calls=%async_computation.2 | async-start | bytes 131072 | tf_op jit(solution)/shard_map/all_to_all | solution.py:23
  78.1 1.1 convert_element_type.158
  79.2 0.3 copy.216
  79.5 0.3 copy.191
  79.8 0.4 reshape.241
  80.4 3.6 %all-to-all-done.2 = bf16[16,4,512]{2,1,0:T(4,128)(2,1)S(1)} async-done(((bf16[16,4,512]{2,1,0:T(4,128)(2,1)}), bf16[16,4,512]{2,1,0:T(4,128)(2,1)S(1)}, u32[]{:S(2)}, u32[]{:S(2)}) %all-to-all-start.2) | async-done | bytes 65568 | tf_op jit(solution)/shard_map/all_to_all | solution.py:23
  84.0 0.8 fusion.17
  84.8 0.2 fusion.2
  84.9 23.3 %all_to_all.35 = bf16[32,8,128]{2,1,0:T(8,128)(2,1)S(1)} all-to-all(bf16[32,8,128]{2,1,0:T(8,128)(2,1)S(1)} %fusion.2), channel_id=1, replica_groups=mesh['za'=4,'zm'=2,'zl'=2,'xh'=2,'xl'=2,'c'=2,'tp'=4] {'za','zm','tp'}, dimensions={0} | all-to-all | bytes 131072 | tf_op jit(solution)/shard_map/all_to_all | solution.py:23
  108.3 0.9 broadcast_in_dim.43
  109.2 6.1 %all-to-all-start.4 = ((bf16[64,32,128]{2,1,0:T(8,128)(2,1)}), bf16[64,32,128]{2,1,0:T(8,128)(2,1)S(1)}, u32[]{:S(2)}, u32[]{:S(2)}) async-start(bf16[64,32,128]{2,1,0:T(8,128)(2,1)} %bitcast.23), calls=%async_computation.4 | async-start | bytes 1048576 | tf_op jit(solution)/shard_map/all_to_all | solution.py:23
  115.3 0.3 copy.198
  115.7 0.7 copy-done.6
  116.3 0.3 copy.196
  116.7 0.2 fusion.5.gu0_ref
  116.9 2.4 %collective-permute-start = (bf16[2048,256]{1,0:T(8,128)(2,1)S(1)}, bf16[2048,256]{1,0:T(8,128)(2,1)S(1)}, u32[]{:S(2)}, u32[]{:S(2)}) collective-permute-start(bf16[2048,256]{1,0:T(8,128)(2,1)S(1)} %fusion.5.gu0_ref), channel_id=1, source_target_pairs={{0,4},{4,0},{1,5},{5,1},{2,6},{6,2},{3,7},{7,3},{8,12},{12,8},{9,1... | collective-permute-start | bytes 3145736 | tf_op jit(solution)/shard_map/ppermute | solution.py:318
  119.3 2.0 %collective-permute-start.1 = (bf16[128,2048]{1,0:T(8,128)(2,1)S(1)}, bf16[128,2048]{1,0:T(8,128)(2,1)}, u32[]{:S(2)}, u32[]{:S(2)}) collective-permute-start(bf16[128,2048]{1,0:T(8,128)(2,1)S(1)} %pad.22.down0_ref), channel_id=1, source_target_pairs={{0,4},{4,0},{1,5},{5,1},{2,6},{6,2},{3,7},{7,3},{8,12},{12,8},{9,1... | collective-permute-start | bytes 1572872 | tf_op jit(solution)/shard_map/ppermute | solution.py:318
  121.3 0.2 reshape.232
  121.5 1.0 slice.33
  122.6 1.1 copy.217
  123.9 0.7 reshape_reshape.7.gain_ref
  124.6 0.1 copy.200
  124.7 0.7 pad.23.rider_ref
  125.4 2.4 %all-to-all-done.4 = bf16[64,32,128]{2,1,0:T(8,128)(2,1)S(1)} async-done(((bf16[64,32,128]{2,1,0:T(8,128)(2,1)}), bf16[64,32,128]{2,1,0:T(8,128)(2,1)S(1)}, u32[]{:S(2)}, u32[]{:S(2)}) %all-to-all-start.4) | async-done | bytes 524320 | tf_op jit(solution)/shard_map/all_to_all | solution.py:23
  127.8 4.1 %experts.1 = bf16[16,4,8,640]{3,2,1,0:T(8,128)(2,1)} custom-call(bf16[16,4,32,128]{3,2,1,0:T(8,128)(2,1)S(1)} %bitcast.92, f32[16,1,128]{2,1,0:T(1,128)} %reshape_reshape.7.gain_ref, bf16[2048,256]{1,0:T(8,128)(2,1)} %copy-done, bf16[128,2048]{1,0:T(8,128)(2,1)} %copy-done.2, bf16[2048,256]{1,0:T(8,128)(2,1)} %copy-done.3, ...), custom_call_target="tpu_custom_call" | custom-call | tf_op jit(solution)/shard_map/experts/pallas_call | solution.py:192
  132.0 7.6 %all-to-all-start.5 = ((bf16[64,8,640]{2,1,0:T(8,128)(2,1)}), bf16[64,8,640]{2,1,0:T(8,128)(2,1)S(1)}, u32[]{:S(2)}, u32[]{:S(2)}) async-start(bf16[64,8,640]{2,1,0:T(8,128)(2,1)} %bitcast.96), calls=%async_computation.5 | async-start | bytes 1310720 | tf_op jit(solution)/shard_map/all_to_all | solution.py:23
  139.6 0.2 convert_reduce_fusion.2
  140.1 1.6 multiply_add_fusion
  141.6 11.8 %all-to-all-done.5 = bf16[64,8,640]{2,1,0:T(8,128)(2,1)S(1)} async-done(((bf16[64,8,640]{2,1,0:T(8,128)(2,1)}), bf16[64,8,640]{2,1,0:T(8,128)(2,1)S(1)}, u32[]{:S(2)}, u32[]{:S(2)}) %all-to-all-start.5) | async-done | bytes 655392 | tf_op jit(solution)/shard_map/all_to_all | solution.py:23
  153.5 0.1 slice.35
  153.7 0.6 copy.229
  154.3 3.3 %all-to-all-start.6 = ((bf16[8,2,512]{2,1,0:T(2,128)(2,1)}), bf16[8,2,512]{2,1,0:T(2,128)(2,1)S(1)}, u32[]{:S(2)}, u32[]{:S(2)}) async-start(bf16[8,2,512]{2,1,0:T(2,128)(2,1)} %bitcast.90), calls=%async_computation.6 | async-start | bytes 32768 | tf_op jit(solution)/shard_map/all_to_all | solution.py:23
  157.7 0.2 reshape.236
  157.8 0.2 reduce_sum.76
  158.2 10.8 %all-to-all-done.6 = bf16[8,2,512]{2,1,0:T(2,128)(2,1)S(1)} async-done(((bf16[8,2,512]{2,1,0:T(2,128)(2,1)}), bf16[8,2,512]{2,1,0:T(2,128)(2,1)S(1)}, u32[]{:S(2)}, u32[]{:S(2)}) %all-to-all-start.6) | async-done | bytes 16416 | tf_op jit(solution)/shard_map/all_to_all | solution.py:23
  169.0 0.8 fusion.4
  (76 shorter events, 1.6 us)
Async XLA Ops:
  12.5 31.0 %all-to-all-start = ((bf16[4,64,512]{2,1,0:T(8,128)(2,1)}), bf16[4,64,512]{2,1,0:T(8,128)(2,1)S(1)}, u32[]{:S(2)}, u32[]{:S(2)}) async-start(bf16[4,64,512]{2,1,0:T(8,128)(2,1)} %broadcast_in_dim.27), calls=%async_computation | async-start | bytes 524288 | tf_op jit(solution)/shard_map/all_to_all | solution.py:23
  26.6 16.6 %copy-start.12 = (bf16[512]{0:T(512)(128)(2,1)S(1)}, bf16[512]{0:T(512)(128)(2,1)}, u32[]{:S(2)}) copy-start(bf16[512]{0:T(512)(128)(2,1)} %param.24) | copy-start | bytes 3076
  35.4 7.9 %copy-start.13 = (bf16[512]{0:T(512)(128)(2,1)S(1)}, bf16[512]{0:T(512)(128)(2,1)}, u32[]{:S(2)}) copy-start(bf16[512]{0:T(512)(128)(2,1)} %param.16) | copy-start | bytes 3076
  45.6 24.8 %all-to-all-start.1 = ((f32[128,2,128]{2,1,0:T(2,128)}), f32[128,2,128]{2,1,0:T(2,128)S(1)}, u32[]{:S(2)}, u32[]{:S(2)}) async-start(f32[128,2,128]{2,1,0:T(2,128)} %copy.190), calls=%async_computation.1 | async-start | bytes 262144 | tf_op jit(solution)/shard_map/all_to_all | solution.py:23
  73.5 10.4 %all-to-all-start.2 = ((bf16[16,4,512]{2,1,0:T(4,128)(2,1)}), bf16[16,4,512]{2,1,0:T(4,128)(2,1)S(1)}, u32[]{:S(2)}, u32[]{:S(2)}) async-start(bf16[16,4,512]{2,1,0:T(4,128)(2,1)} %get-tuple-element.16), calls=%async_computation.2 | async-start | bytes 131072 | tf_op jit(solution)/shard_map/all_to_all | solution.py:23
  84.8 30.5 %copy-start.5 = (bf16[1,2048,112]{1,2,0:T(8,128)(2,1)S(1)}, bf16[1,2048,112]{1,2,0:T(8,128)(2,1)}, u32[]{:S(2)}) copy-start(bf16[1,2048,112]{1,2,0:T(8,128)(2,1)} %param.28) | copy-start | bytes 1376260
  109.2 18.6 %all-to-all-start.4 = ((bf16[64,32,128]{2,1,0:T(8,128)(2,1)}), bf16[64,32,128]{2,1,0:T(8,128)(2,1)S(1)}, u32[]{:S(2)}, u32[]{:S(2)}) async-start(bf16[64,32,128]{2,1,0:T(8,128)(2,1)} %bitcast.23), calls=%async_computation.4 | async-start | bytes 1048576 | tf_op jit(solution)/shard_map/all_to_all | solution.py:23
  115.3 1.0 copy-start.6
  116.7 2.6 %copy-start.4 = (bf16[1,112,2048]{2,1,0:T(8,128)(2,1)S(1)}, bf16[1,112,2048]{2,1,0:T(8,128)(2,1)}, u32[]{:S(2)}) copy-start(bf16[1,112,2048]{2,1,0:T(8,128)(2,1)} %param.29) | copy-start | bytes 1376260
  116.9 6.8 %copy-start = (bf16[2048,256]{1,0:T(8,128)(2,1)}, bf16[2048,256]{1,0:T(8,128)(2,1)S(1)}, u32[]{:S(2)}) copy-start(bf16[2048,256]{1,0:T(8,128)(2,1)S(1)} %fusion.5.gu0_ref) | copy-start | bytes 3145732
  116.9 8.5 %collective-permute-start = (bf16[2048,256]{1,0:T(8,128)(2,1)S(1)}, bf16[2048,256]{1,0:T(8,128)(2,1)S(1)}, u32[]{:S(2)}, u32[]{:S(2)}) collective-permute-start(bf16[2048,256]{1,0:T(8,128)(2,1)S(1)} %fusion.5.gu0_ref), channel_id=1, source_target_pairs={{0,4},{4,0},{1,5},{5,1},{2,6},{6,2},{3,7},{7,3},{8,12},{12,8},{9,1... | collective-permute-start | bytes 3145736 | tf_op jit(solution)/shard_map/ppermute | solution.py:318
  119.3 8.5 %copy-start.2 = (bf16[128,2048]{1,0:T(8,128)(2,1)}, bf16[128,2048]{1,0:T(8,128)(2,1)S(1)}, u32[]{:S(2)}) copy-start(bf16[128,2048]{1,0:T(8,128)(2,1)S(1)} %pad.22.down0_ref) | copy-start | bytes 1572868
  119.3 6.0 %collective-permute-start.1 = (bf16[128,2048]{1,0:T(8,128)(2,1)S(1)}, bf16[128,2048]{1,0:T(8,128)(2,1)}, u32[]{:S(2)}, u32[]{:S(2)}) collective-permute-start(bf16[128,2048]{1,0:T(8,128)(2,1)S(1)} %pad.22.down0_ref), channel_id=1, source_target_pairs={{0,4},{4,0},{1,5},{5,1},{2,6},{6,2},{3,7},{7,3},{8,12},{12,8},{9,1... | collective-permute-start | bytes 1572872 | tf_op jit(solution)/shard_map/ppermute | solution.py:318
  121.5 3.1 %copy-start.7 = (bf16[64,4,32]{0,2,1:T(8,128)(2,1)S(1)}, bf16[64,4,32]{0,2,1:T(8,128)(2,1)}, u32[]{:S(2)}) copy-start(bf16[64,4,32]{0,2,1:T(8,128)(2,1)} %get-tuple-element.20) | copy-start | bytes 49156
  125.4 2.4 %copy-start.3 = (bf16[2048,256]{1,0:T(8,128)(2,1)}, bf16[2048,256]{1,0:T(8,128)(2,1)S(1)}, u32[]{:S(2)}) copy-start(bf16[2048,256]{1,0:T(8,128)(2,1)S(1)} %collective-permute-done.gu1_ref) | copy-start | bytes 3145732
  131.9 7.7 %copy-start.10 = (s32[4,2]{0,1:T(2,128)S(1)}, s32[4,2]{0,1:T(2,128)}, u32[]{:S(2)}) copy-start(s32[4,2]{0,1:T(2,128)} %param.25) | copy-start | bytes 100
  131.9 8.0 %copy-start.14 = (f32[4,2]{0,1:T(2,128)S(1)}, f32[4,2]{0,1:T(2,128)}, u32[]{:S(2)}) copy-start(f32[4,2]{0,1:T(2,128)} %param.26) | copy-start | bytes 100
  132.0 8.0 %copy-start.11 = (f32[4,4,128]{2,1,0:T(4,128)S(1)}, f32[4,4,128]{2,1,0:T(4,128)}, u32[]{:S(2)}) copy-start(f32[4,4,128]{2,1,0:T(4,128)} %get-tuple-element.19) | copy-start | bytes 24580
  132.0 8.0 %copy-start.8 = (f32[4,4,128]{2,1,0:T(4,128)S(1)}, f32[4,4,128]{2,1,0:T(4,128)}, u32[]{:S(2)}) copy-start(f32[4,4,128]{2,1,0:T(4,128)} %get-tuple-element.18) | copy-start | bytes 24580
  132.0 8.1 %copy-start.1 = (f32[4,4,128,128]{3,2,1,0:T(8,128)S(1)}, f32[4,4,128,128]{3,2,1,0:T(8,128)}, u32[]{:S(2)}) copy-start(f32[4,4,128,128]{3,2,1,0:T(8,128)} %refs_1_.1) | copy-start | bytes 3145732
  132.0 21.5 %all-to-all-start.5 = ((bf16[64,8,640]{2,1,0:T(8,128)(2,1)}), bf16[64,8,640]{2,1,0:T(8,128)(2,1)S(1)}, u32[]{:S(2)}, u32[]{:S(2)}) async-start(bf16[64,8,640]{2,1,0:T(8,128)(2,1)} %bitcast.96), calls=%async_computation.5 | async-start | bytes 1310720 | tf_op jit(solution)/shard_map/all_to_all | solution.py:23
  153.7 15.4 %copy-start.9 = (bf16[4,512]{1,0:T(4,128)(2,1)S(1)}, bf16[4,512]{1,0:T(4,128)(2,1)}, u32[]{:S(2)}) copy-start(bf16[4,512]{1,0:T(4,128)(2,1)} %param.15) | copy-start | bytes 12292
  154.3 14.7 %all-to-all-start.6 = ((bf16[8,2,512]{2,1,0:T(2,128)(2,1)}), bf16[8,2,512]{2,1,0:T(2,128)(2,1)S(1)}, u32[]{:S(2)}, u32[]{:S(2)}) async-start(bf16[8,2,512]{2,1,0:T(2,128)(2,1)} %bitcast.90), calls=%async_computation.6 | async-start | bytes 32768 | tf_op jit(solution)/shard_map/all_to_all | solution.py:23

commit v6 on v4

--- a/solution.py
+++ b/solution.py
@@ -12,7 +12,7 @@
 EP = ("zh", "zl", "xh", "xl", "c")
 ROW = ("zl", "xh", "xl", "c")
 PAIR = (*ROW, "tp")
-GATHER = ("zl", "xl", "xh", "c")
+GATHER = ("c", "xl", "xh", "zl")
 bf16 = jnp.bfloat16
 f32 = jnp.float32
 
@@ -44,10 +44,8 @@
 
 
 def recurrence_kernel(
-    width, got_ref, state_ref, floor_ref, gain_ref, out_ref, forget_ref, input_ref, held, sem
+    width, got_ref, held, floor_ref, gain_ref, out_ref, forget_ref, input_ref
 ):
-    copy = pltpu.make_async_copy(state_ref, held, sem)
-    copy.start()
     sources, parts, seq, lanes = got_ref.shape
     heads = forget_ref.shape[0]
     half = sources // 2
@@ -86,7 +84,6 @@
             input_ref[2 * low + k] = value[k * seq : (k + 1) * seq]
         fresh = jnp.sum(query * (1.0 - forget), axis=1, keepdims=True)
         rows.append((fresh * value, (query * forget).T))
-    copy.wait()
     gain = gain_ref[...].astype(f32)
     for low in range(heads // 2):
         fresh, kept = rows[low]
@@ -119,14 +116,13 @@
         ),
         in_specs=[
             pl.BlockSpec(memory_space=pltpu.VMEM),
-            pl.BlockSpec(memory_space=pl.ANY),
+            pl.BlockSpec(memory_space=pltpu.VMEM),
             pl.BlockSpec(memory_space=pltpu.VMEM),
             pl.BlockSpec(memory_space=pltpu.VMEM),
         ],
         out_specs=tuple(pl.BlockSpec(memory_space=pltpu.VMEM) for _ in range(3)),
-        scratch_shapes=[pltpu.VMEM(state.shape, f32), pltpu.SemaphoreType.DMA],
         name="recurrence",
-    )(resident(got), state, floors, gain)
+    )(resident(got), resident(state), floors, gain)
 
 
 def experts_kernel(

time: 174 us -> 161 us (0.925)
  blocking collectives: 61.2 us -> 39.7 us
  starting transfers between devices: 48.7 us -> 54.6 us
  waiting for transfers between devices: 39.7 us -> 43.5 us
    all_to_all x1, blocking collectives: 30.5 us -> 18.6 us  [exchange(): return lax.all_to_all(blocks, axes, split_axis=0, concat_axis=0, tiled=True)]
    all_gather x4, blocking collectives: 30.8 us -> 21.1 us  [shards(): all_rows = lax.all_gather(all_rows, axis, tiled=True)]
    all_to_all x6, starting transfers between devices: 44.4 us -> 50.3 us  [exchange(): return lax.all_to_all(blocks, axes, split_axis=0, concat_axis=0, tiled=True)]
    all_to_all x6, waiting for transfers between devices: 39.6 us -> 43.4 us  [exchange(): return lax.all_to_all(blocks, axes, split_axis=0, concat_axis=0, tiled=True)]
  transfers between devices with their start and end apart: 8 -> 8, of which waited for: 6 -> 7; matrix products, arithmetic and copies ran while one was open for 4% -> 5% of each run, Pallas kernels for 0% -> 0%
where the time goes in v6:
time: 161 us; the launch traced here: 160 us
  starting transfers between devices  54.6 us (34%)
  waiting for transfers between devices  43.5 us (27%)
  blocking collectives  39.7 us (25%)
  local copies, waits for them, and re-layouts  9.39 us (6%)
  Pallas kernels  6.22 us (4%)
  other arithmetic  4.11 us (3%)
    all_to_all x6, starting transfers between devices, exchange(): return lax.all_to_all(blocks, axes, split_axis=0, concat_axis=0, tiled=True)  50.3 us
    all_to_all x6, waiting for transfers between devices, exchange(): return lax.all_to_all(blocks, axes, split_axis=0, concat_axis=0, tiled=True)  43.4 us
    all_gather x4, blocking collectives, shards(): all_rows = lax.all_gather(all_rows, axis, tiled=True)  21.1 us
    all_to_all x1, blocking collectives, exchange(): return lax.all_to_all(blocks, axes, split_axis=0, concat_axis=0, tiled=True)  18.6 us
    ppermute x2, starting transfers between devices, shards(): lax.ppermute(w, 'c', [(0, 1), (1, 0)])  4.33 us
    pallas_call x1, Pallas kernels, experts(): pl.pallas_call(experts_kernel, out_shape=jax.ShapeDtypeStruct(whole, bf16...  4.13 us
  transfers between devices with their start and end apart: 8, of which 7 were waited for; matrix products, arithmetic and copies ran while one was open for 5% of the time, Pallas kernels for 0%

profile of v6, /device:TPU:1, one launch (start us, length us, event | category | flops | bytes accessed | tf_op | source)
XLA Modules:
  0.0 160.1 jit_solution(3783966005760911374)
XLA Ops:
  0.7 0.8 maximum_bitcast_fusion
  1.4 0.8 broadcast_in_dim.27
  2.3 15.8 %all-to-all-start = ((bf16[8,64,512]{2,1,0:T(8,128)(2,1)}), bf16[8,64,512]{2,1,0:T(8,128)(2,1)S(1)}, u32[]{:S(2)}, u32[]{:S(2)}) async-start(bf16[8,64,512]{2,1,0:T(8,128)(2,1)} %broadcast_in_dim.27), calls=%async_computation | async-start | bytes 1048576 | tf_op jit(solution)/shard_map/all_to_all | solution.py:21
  18.1 0.1 copy.211
  18.2 2.4 %all_gather.12 = bf16[16,512]{1,0:T(8,128)(2,1)S(1)} all-gather(bf16[8,512]{1,0:T(8,128)(2,1)S(1)} %fusion.9), channel_id=1, replica_groups=mesh['zh'=8,'zl'=2,'xh'=2,'xl'=2,'c'=2,'tp'=4] {'c'}, dimensions={0}, use_global_device_ids=true | all-gather | bytes 24576 | tf_op jit(solution)/shard_map/all_gather | solution.py:240
  20.6 3.2 %all_gather.13 = bf16[32,512]{1,0:T(8,128)(2,1)S(1)} all-gather(bf16[16,512]{1,0:T(8,128)(2,1)S(1)} %all_gather.12), channel_id=1, replica_groups=mesh['zh'=8,'zl'=2,'xh'=2,'xl'=2,'c'=2,'tp'=4] {'xl'}, dimensions={0}, use_global_device_ids=true | all-gather | bytes 49152 | tf_op jit(solution)/shard_map/all_gather | solution.py:240
  23.8 4.9 %all_gather.14 = bf16[64,512]{1,0:T(8,128)(2,1)S(1)} all-gather(bf16[32,512]{1,0:T(8,128)(2,1)S(1)} %all_gather.13), channel_id=1, replica_groups=mesh['zh'=8,'zl'=2,'xh'=2,'xl'=2,'c'=2,'tp'=4] {'xh'}, dimensions={0}, use_global_device_ids=true | all-gather | bytes 98304 | tf_op jit(solution)/shard_map/all_gather | solution.py:240
  28.8 10.5 %all_gather.15 = bf16[128,512]{1,0:T(8,128)(2,1)S(1)} all-gather(bf16[64,512]{1,0:T(8,128)(2,1)S(1)} %all_gather.14), channel_id=1, replica_groups=mesh['zh'=8,'zl'=2,'xh'=2,'xl'=2,'c'=2,'tp'=4] {'zl'}, dimensions={0}, use_global_device_ids=true | all-gather | bytes 196608 | tf_op jit(solution)/shard_map/all_gather | solution.py:240
  39.3 0.1 copy.210
  39.5 0.1 reshape.226
  39.7 0.1 convert_reduce_fusion.1
  39.8 4.0 %all-to-all-done = bf16[8,64,512]{2,1,0:T(8,128)(2,1)S(1)} async-done(((bf16[8,64,512]{2,1,0:T(8,128)(2,1)}), bf16[8,64,512]{2,1,0:T(8,128)(2,1)S(1)}, u32[]{:S(2)}, u32[]{:S(2)}) %all-to-all-start) | async-done | bytes 524320 | tf_op jit(solution)/shard_map/all_to_all | solution.py:21
  43.8 0.1 multiply_convert_fusion.1
  43.9 0.1 broadcast_in_dim.29
  44.0 0.1 copy.183
  44.1 0.3 convolution_bitcast_fusion
  44.4 0.1 broadcast_in_dim.30
  44.5 0.1 pad_maximum_fusion
  44.7 0.7 copy.185
  45.5 16.5 %all-to-all-start.1 = ((f32[64,4,128]{2,1,0:T(4,128)}), f32[64,4,128]{2,1,0:T(4,128)S(1)}, u32[]{:S(2)}, u32[]{:S(2)}) async-start(f32[64,4,128]{2,1,0:T(4,128)} %copy.185), calls=%async_computation.1 | async-start | bytes 262144 | tf_op jit(solution)/shard_map/all_to_all | solution.py:21
  62.0 0.1 copy.180
  62.1 0.3 copy.181
  62.4 0.1 fusion.10
  62.4 8.1 %all-to-all-done.1 = f32[64,4,128]{2,1,0:T(4,128)S(1)} async-done(((f32[64,4,128]{2,1,0:T(4,128)}), f32[64,4,128]{2,1,0:T(4,128)S(1)}, u32[]{:S(2)}, u32[]{:S(2)}) %all-to-all-start.1) | async-done | bytes 131104 | tf_op jit(solution)/shard_map/all_to_all | solution.py:21
  70.5 2.1 %recurrence.1 = (bf16[16,4,512]{2,1,0:T(4,128)(2,1)}, f32[4,4,128]{2,1,0:T(4,128)}, f32[4,4,128]{2,1,0:T(4,128)}) custom-call(f32[16,4,4,128]{3,2,1,0:T(4,128)S(1)} %bitcast.88, f32[4,4,128,128]{3,2,1,0:T(8,128)S(1)} %copy-done, f32[4,128]{1,0:T(4,128)} %bitcast.113, bf16[1,128]{1,0:T(2,128)(2,1)} %bitcast.114), custom_call_target="tpu_custom_call" | custom-call | tf_op jit(solution)/shard_map/recurrence/pallas_call | solution.py:110
  72.6 3.8 %all-to-all-start.2 = ((bf16[16,4,512]{2,1,0:T(4,128)(2,1)}), bf16[16,4,512]{2,1,0:T(4,128)(2,1)S(1)}, u32[]{:S(2)}, u32[]{:S(2)}) async-start(bf16[16,4,512]{2,1,0:T(4,128)(2,1)} %get-tuple-element.9), calls=%async_computation.2 | async-start | bytes 131072 | tf_op jit(solution)/shard_map/all_to_all | solution.py:21
  76.4 0.3 multiply_convert_fusion
  76.7 1.1 convert_element_type.151
  77.8 0.1 copy.186
  77.9 4.3 %all-to-all-done.2 = bf16[16,4,512]{2,1,0:T(4,128)(2,1)S(1)} async-done(((bf16[16,4,512]{2,1,0:T(4,128)(2,1)}), bf16[16,4,512]{2,1,0:T(4,128)(2,1)S(1)}, u32[]{:S(2)}, u32[]{:S(2)}) %all-to-all-start.2) | async-done | bytes 65568 | tf_op jit(solution)/shard_map/all_to_all | solution.py:21
  82.3 0.2 fusion.11
  82.5 0.2 fusion.2
  82.7 18.6 %all_to_all.35 = bf16[32,8,128]{2,1,0:T(8,128)(2,1)S(1)} all-to-all(bf16[32,8,128]{2,1,0:T(8,128)(2,1)S(1)} %fusion.2), channel_id=1, replica_groups=mesh['zh'=8,'zl'=2,'xh'=2,'xl'=2,'c'=2,'tp'=4] {'zh','tp'}, dimensions={0} | all-to-all | bytes 131072 | tf_op jit(solution)/shard_map/all_to_all | solution.py:21
  101.3 0.9 broadcast_in_dim.43
  102.2 6.1 %all-to-all-start.4 = ((bf16[64,32,128]{2,1,0:T(8,128)(2,1)}), bf16[64,32,128]{2,1,0:T(8,128)(2,1)S(1)}, u32[]{:S(2)}, u32[]{:S(2)}) async-start(bf16[64,32,128]{2,1,0:T(8,128)(2,1)} %bitcast.22), calls=%async_computation.4 | async-start | bytes 1048576 | tf_op jit(solution)/shard_map/all_to_all | solution.py:21
  108.3 0.3 copy.192
  108.6 1.0 copy-done.5
  109.6 0.3 copy.190
  110.0 0.2 fusion.5.gu0_ref
  110.2 2.4 %collective-permute-start = (bf16[2048,256]{1,0:T(8,128)(2,1)S(1)}, bf16[2048,256]{1,0:T(8,128)(2,1)}, u32[]{:S(2)}, u32[]{:S(2)}) collective-permute-start(bf16[2048,256]{1,0:T(8,128)(2,1)S(1)} %fusion.5.gu0_ref), channel_id=1, source_target_pairs={{0,4},{4,0},{1,5},{5,1},{2,6},{6,2},{3,7},{7,3},{8,12},{12,8},{9,1... | collective-permute-start | bytes 3145736 | tf_op jit(solution)/shard_map/ppermute | solution.py:304
  112.6 2.0 %collective-permute-start.1 = (bf16[128,2048]{1,0:T(8,128)(2,1)S(1)}, bf16[128,2048]{1,0:T(8,128)(2,1)}, u32[]{:S(2)}, u32[]{:S(2)}) collective-permute-start(bf16[128,2048]{1,0:T(8,128)(2,1)S(1)} %pad.22.down0_ref), channel_id=1, source_target_pairs={{0,4},{4,0},{1,5},{5,1},{2,6},{6,2},{3,7},{7,3},{8,12},{12,8},{9,1... | collective-permute-start | bytes 1572872 | tf_op jit(solution)/shard_map/ppermute | solution.py:304
  114.6 0.1 slice_bitcast_fusion
  114.7 0.1 reshape_reshape.10
  114.9 0.7 reshape_reshape.11.gain_ref
  115.6 0.1 copy.194
  115.7 0.7 pad.23.rider_ref
  116.4 0.1 collective-permute-done.1.down1_ref
  116.6 4.2 %all-to-all-done.4 = bf16[64,32,128]{2,1,0:T(8,128)(2,1)S(1)} async-done(((bf16[64,32,128]{2,1,0:T(8,128)(2,1)}), bf16[64,32,128]{2,1,0:T(8,128)(2,1)S(1)}, u32[]{:S(2)}, u32[]{:S(2)}) %all-to-all-start.4) | async-done | bytes 524320 | tf_op jit(solution)/shard_map/all_to_all | solution.py:21
  120.8 4.1 %experts.1 = bf16[16,4,8,640]{3,2,1,0:T(8,128)(2,1)} custom-call(bf16[16,4,32,128]{3,2,1,0:T(8,128)(2,1)S(1)} %bitcast.87, f32[16,1,128]{2,1,0:T(1,128)} %reshape_reshape.11.gain_ref, bf16[2048,256]{1,0:T(8,128)(2,1)} %copy-done.1, bf16[128,2048]{1,0:T(8,128)(2,1)} %copy-done.2, bf16[2048,256]{1,0:T(8,128)(2,1)} %collective-permute-done.gu1_ref, ...), custom_call_target="tpu_custom_call" | custom-call | tf_op jit(solution)/shard_map/experts/pallas_call | solution.py:187
  125.0 4.9 %all-to-all-start.5 = ((bf16[64,8,640]{2,1,0:T(8,128)(2,1)}), bf16[64,8,640]{2,1,0:T(8,128)(2,1)S(1)}, u32[]{:S(2)}, u32[]{:S(2)}) async-start(bf16[64,8,640]{2,1,0:T(8,128)(2,1)} %bitcast.91), calls=%async_computation.5 | async-start | bytes 1310720 | tf_op jit(solution)/shard_map/all_to_all | solution.py:21
  129.8 0.2 convert_reduce_fusion.2
  130.0 0.1 iota_compare_fusion.6
  130.1 0.1 select_reduce_fusion
  130.3 1.6 multiply_add_fusion
  131.9 11.9 %all-to-all-done.5 = bf16[64,8,640]{2,1,0:T(8,128)(2,1)S(1)} async-done(((bf16[64,8,640]{2,1,0:T(8,128)(2,1)}), bf16[64,8,640]{2,1,0:T(8,128)(2,1)S(1)}, u32[]{:S(2)}, u32[]{:S(2)}) %all-to-all-start.5) | async-done | bytes 655392 | tf_op jit(solution)/shard_map/all_to_all | solution.py:21
  143.8 0.1 slice.32
  143.9 0.1 reduce_sum.79
  144.0 0.6 copy.224
  144.6 3.3 %all-to-all-start.6 = ((bf16[8,2,512]{2,1,0:T(2,128)(2,1)}), bf16[8,2,512]{2,1,0:T(2,128)(2,1)S(1)}, u32[]{:S(2)}, u32[]{:S(2)}) async-start(bf16[8,2,512]{2,1,0:T(2,128)(2,1)} %bitcast.85), calls=%async_computation.6 | async-start | bytes 32768 | tf_op jit(solution)/shard_map/all_to_all | solution.py:21
  148.0 0.2 reshape.222
  148.2 0.2 reduce_sum.76
  148.4 0.1 reshape.227
  148.5 10.8 %all-to-all-done.6 = bf16[8,2,512]{2,1,0:T(2,128)(2,1)S(1)} async-done(((bf16[8,2,512]{2,1,0:T(2,128)(2,1)}), bf16[8,2,512]{2,1,0:T(2,128)(2,1)S(1)}, u32[]{:S(2)}, u32[]{:S(2)}) %all-to-all-start.6) | async-done | bytes 16416 | tf_op jit(solution)/shard_map/all_to_all | solution.py:21
  159.3 0.8 fusion.4
  (66 shorter events, 0.8 us)
Async XLA Ops:
  0.6 17.4 %copy-start.8 = (s32[4,2]{0,1:T(2,128)S(1)}, s32[4,2]{0,1:T(2,128)}, u32[]{:S(2)}) copy-start(s32[4,2]{0,1:T(2,128)} %param.25) | copy-start | bytes 100
  0.6 17.5 %copy-start.7 = (bf16[4,512]{1,0:T(4,128)(2,1)S(1)}, bf16[4,512]{1,0:T(4,128)(2,1)}, u32[]{:S(2)}) copy-start(bf16[4,512]{1,0:T(4,128)(2,1)} %param.15) | copy-start | bytes 12292
  2.3 37.2 %copy-start.10 = (bf16[512]{0:T(512)(128)(2,1)S(1)}, bf16[512]{0:T(512)(128)(2,1)}, u32[]{:S(2)}) copy-start(bf16[512]{0:T(512)(128)(2,1)} %param.16) | copy-start | bytes 3076
  2.3 37.3 %copy-start.11 = (bf16[512]{0:T(512)(128)(2,1)S(1)}, bf16[512]{0:T(512)(128)(2,1)}, u32[]{:S(2)}) copy-start(bf16[512]{0:T(512)(128)(2,1)} %param.24) | copy-start | bytes 3076
  2.3 41.5 %all-to-all-start = ((bf16[8,64,512]{2,1,0:T(8,128)(2,1)}), bf16[8,64,512]{2,1,0:T(8,128)(2,1)S(1)}, u32[]{:S(2)}, u32[]{:S(2)}) async-start(bf16[8,64,512]{2,1,0:T(8,128)(2,1)} %broadcast_in_dim.27), calls=%async_computation | async-start | bytes 1048576 | tf_op jit(solution)/shard_map/all_to_all | solution.py:21
  44.4 26.1 %copy-start = (f32[4,4,128,128]{3,2,1,0:T(8,128)S(1)}, f32[4,4,128,128]{3,2,1,0:T(8,128)}, u32[]{:S(2)}) copy-start(f32[4,4,128,128]{3,2,1,0:T(8,128)} %refs_1_.1) | copy-start | bytes 3145732
  45.5 25.1 %all-to-all-start.1 = ((f32[64,4,128]{2,1,0:T(4,128)}), f32[64,4,128]{2,1,0:T(4,128)S(1)}, u32[]{:S(2)}, u32[]{:S(2)}) async-start(f32[64,4,128]{2,1,0:T(4,128)} %copy.185), calls=%async_computation.1 | async-start | bytes 262144 | tf_op jit(solution)/shard_map/all_to_all | solution.py:21
  72.6 9.7 %all-to-all-start.2 = ((bf16[16,4,512]{2,1,0:T(4,128)(2,1)}), bf16[16,4,512]{2,1,0:T(4,128)(2,1)S(1)}, u32[]{:S(2)}, u32[]{:S(2)}) async-start(bf16[16,4,512]{2,1,0:T(4,128)(2,1)} %get-tuple-element.9), calls=%async_computation.2 | async-start | bytes 131072 | tf_op jit(solution)/shard_map/all_to_all | solution.py:21
  82.5 25.8 %copy-start.4 = (bf16[1,2048,112]{1,2,0:T(8,128)(2,1)S(1)}, bf16[1,2048,112]{1,2,0:T(8,128)(2,1)}, u32[]{:S(2)}) copy-start(bf16[1,2048,112]{1,2,0:T(8,128)(2,1)} %param.28) | copy-start | bytes 1376260
  102.2 18.6 %all-to-all-start.4 = ((bf16[64,32,128]{2,1,0:T(8,128)(2,1)}), bf16[64,32,128]{2,1,0:T(8,128)(2,1)S(1)}, u32[]{:S(2)}, u32[]{:S(2)}) async-start(bf16[64,32,128]{2,1,0:T(8,128)(2,1)} %bitcast.22), calls=%async_computation.4 | async-start | bytes 1048576 | tf_op jit(solution)/shard_map/all_to_all | solution.py:21
  108.6 1.0 copy-start.5
  109.9 2.6 %copy-start.3 = (bf16[1,112,2048]{2,1,0:T(8,128)(2,1)S(1)}, bf16[1,112,2048]{2,1,0:T(8,128)(2,1)}, u32[]{:S(2)}) copy-start(bf16[1,112,2048]{2,1,0:T(8,128)(2,1)} %param.29) | copy-start | bytes 1376260
  110.2 5.6 %copy-start.1 = (bf16[2048,256]{1,0:T(8,128)(2,1)}, bf16[2048,256]{1,0:T(8,128)(2,1)S(1)}, u32[]{:S(2)}) copy-start(bf16[2048,256]{1,0:T(8,128)(2,1)S(1)} %fusion.5.gu0_ref) | copy-start | bytes 3145732
  110.2 6.4 %collective-permute-start = (bf16[2048,256]{1,0:T(8,128)(2,1)S(1)}, bf16[2048,256]{1,0:T(8,128)(2,1)}, u32[]{:S(2)}, u32[]{:S(2)}) collective-permute-start(bf16[2048,256]{1,0:T(8,128)(2,1)S(1)} %fusion.5.gu0_ref), channel_id=1, source_target_pairs={{0,4},{4,0},{1,5},{5,1},{2,6},{6,2},{3,7},{7,3},{8,12},{12,8},{9,1... | collective-permute-start | bytes 3145736 | tf_op jit(solution)/shard_map/ppermute | solution.py:304
  112.6 8.2 %copy-start.2 = (bf16[128,2048]{1,0:T(8,128)(2,1)}, bf16[128,2048]{1,0:T(8,128)(2,1)S(1)}, u32[]{:S(2)}) copy-start(bf16[128,2048]{1,0:T(8,128)(2,1)S(1)} %pad.22.down0_ref) | copy-start | bytes 1572868
  112.6 3.9 %collective-permute-start.1 = (bf16[128,2048]{1,0:T(8,128)(2,1)S(1)}, bf16[128,2048]{1,0:T(8,128)(2,1)}, u32[]{:S(2)}, u32[]{:S(2)}) collective-permute-start(bf16[128,2048]{1,0:T(8,128)(2,1)S(1)} %pad.22.down0_ref), channel_id=1, source_target_pairs={{0,4},{4,0},{1,5},{5,1},{2,6},{6,2},{3,7},{7,3},{8,12},{12,8},{9,1... | collective-permute-start | bytes 1572872 | tf_op jit(solution)/shard_map/ppermute | solution.py:304
  124.9 5.2 %copy-start.12 = (f32[4,2]{0,1:T(2,128)S(1)}, f32[4,2]{0,1:T(2,128)}, u32[]{:S(2)}) copy-start(f32[4,2]{0,1:T(2,128)} %param.26) | copy-start | bytes 100
  124.9 5.3 %copy-start.9 = (f32[4,4,128]{2,1,0:T(4,128)S(1)}, f32[4,4,128]{2,1,0:T(4,128)}, u32[]{:S(2)}) copy-start(f32[4,4,128]{2,1,0:T(4,128)} %get-tuple-element.11) | copy-start | bytes 24580
  124.9 5.3 %copy-start.6 = (f32[4,4,128]{2,1,0:T(4,128)S(1)}, f32[4,4,128]{2,1,0:T(4,128)}, u32[]{:S(2)}) copy-start(f32[4,4,128]{2,1,0:T(4,128)} %get-tuple-element.10) | copy-start | bytes 24580
  125.0 18.8 %all-to-all-start.5 = ((bf16[64,8,640]{2,1,0:T(8,128)(2,1)}), bf16[64,8,640]{2,1,0:T(8,128)(2,1)S(1)}, u32[]{:S(2)}, u32[]{:S(2)}) async-start(bf16[64,8,640]{2,1,0:T(8,128)(2,1)} %bitcast.91), calls=%async_computation.5 | async-start | bytes 1310720 | tf_op jit(solution)/shard_map/all_to_all | solution.py:21
  144.6 14.7 %all-to-all-start.6 = ((bf16[8,2,512]{2,1,0:T(2,128)(2,1)}), bf16[8,2,512]{2,1,0:T(2,128)(2,1)S(1)}, u32[]{:S(2)}, u32[]{:S(2)}) async-start(bf16[8,2,512]{2,1,0:T(2,128)(2,1)} %bitcast.85), calls=%async_computation.6 | async-start | bytes 32768 | tf_op jit(solution)/shard_map/all_to_all | solution.py:21

commit v7 on v6

--- a/solution.py
+++ b/solution.py
@@ -9,7 +9,8 @@
 EXPERTS = 8
 EPS = 1e-06
 LANES = 128
-EP = ("zh", "zl", "xh", "xl", "c")
+ZH = ("za", "zm")
+EP = (*ZH, "zl", "xh", "xl", "c")
 ROW = ("zl", "xh", "xl", "c")
 PAIR = (*ROW, "tp")
 GATHER = ("c", "xl", "xh", "zl")
@@ -154,10 +155,9 @@
     for n in range(sources):
         block = rows_v[n].reshape(count, lanes).astype(f32)
         second[:, n * lanes : (n + 1) * lanes] = (block * scale * gain_ref[n]).astype(bf16)
-    copies[0].wait()
-    copies[1].wait()
     hidden = []
     for k in range(2):
+        copies[k].wait()
         both = jnp.dot(second[...], gu_v[k], preferred_element_type=f32)
         gate = both[:, :lanes]
         hidden.append((gate / (1.0 + jnp.exp(-gate)) * both[:, lanes:]).astype(bf16))
@@ -176,7 +176,7 @@
 
 
 def experts(block, gain, weights_of, rider):
-    sources, parts, height, lanes = block.shape
+    _, parts, height, lanes = block.shape
     (gate_up, down), (gate_up_1, down_1) = weights_of
     zh = rider.shape[2]
     feat = gate_up.shape[0] // parts
@@ -220,7 +220,7 @@
 ):
     tp = lax.axis_size("tp")
     rows = lax.axis_size(ROW)
-    zh = lax.axis_size("zh")
+    zh = lax.axis_size(ZH)
     seq, feat = tokens.shape
     width = feat * tp
     heads, head = state.shape[1], state.shape[2]
@@ -232,25 +232,39 @@
     cap = max(2, seq // 2)
 
     w_joint = jnp.concatenate([w_query, w_forget, w_input, w_output], axis=1).T
-    w_all = gathered(w_joint, "zh", zh)
+    w_mine = gathered(w_joint, "za", zh // 2)
 
     routes = jnp.pad(route_experts.astype(bf16), ((0, 0), (0, feat - route_experts.shape[1])))
     all_rows = jnp.concatenate([tokens, routes], axis=0)
-    for axis in GATHER:
+    for axis in GATHER[:-1]:
         all_rows = lax.all_gather(all_rows, axis, tiled=True)
-
+    w_mine, all_rows = lax.optimization_barrier((w_mine, all_rows))
+
+    swap = [(0, 1), (1, 0)]
+    in_mine, out_mine = w_mine[:, : 3 * col], w_mine[:, 3 * col :]
+    in_other = lax.ppermute(in_mine, "zm", swap)
+    out_other = lax.ppermute(out_mine, "zm", swap)
+    even = lax.axis_index("zm") == 0
+
+    def projected(rows_in, own, other):
+        own, other = (
+            jnp.einsum("td,pcd->tpc", rows_in, w, preferred_element_type=f32) for w in (own, other)
+        )
+        return jnp.where(
+            even, jnp.concatenate([own, other], axis=2), jnp.concatenate([other, own], axis=2)
+        )
+
+    all_rows = lax.all_gather(all_rows, GATHER[-1], tiled=True)
     all_rows = all_rows.reshape(2, 2, 2, 2, 2, seq, feat)
     order = tuple(GATHER[::-1].index(axis) for axis in ROW)
     all_rows = all_rows.transpose(*order, 4, 5, 6).reshape(rows, 2, seq, feat)
     experts_all = all_rows[:, 1, :, : route_experts.shape[1]].astype(jnp.int32)
-    w_all, tok_all = lax.optimization_barrier((w_all, all_rows[:, 0].reshape(rows * seq, feat)))
-    w_in = w_all[:, : 3 * col].reshape(tp, low * 3 * col, feat)
-    w_out = w_all[:, 3 * col :].reshape(tp, low * col, feat)
+    tok_all = all_rows[:, 0].reshape(rows * seq, feat)
 
     tok_all = tok_all.astype(f32)
     sum_sq = jnp.sum(tok_all * tok_all, axis=1)
     scaled = (tok_all * norm_gain.astype(f32)).astype(bf16)
-    partial = jnp.einsum("td,pcd->tpc", scaled, w_in, preferred_element_type=f32)
+    partial = projected(scaled, in_mine, in_other)
     partial = partial.reshape(rows, seq, tp, low * 3 * col).transpose(0, 2, 1, 3)
     used = low * 3 * col
     share = feat // (rows * seq)
@@ -276,7 +290,7 @@
     sel = sel.reshape(EXPERTS * rows * cap, rows * seq).astype(bf16)
 
     heads_all = exchange(heads_sent, ROW).reshape(rows * seq, feat)
-    part_out = jnp.einsum("td,pcd->tpc", heads_all, w_out, preferred_element_type=f32)
+    part_out = projected(heads_all, out_mine, out_other)
     residual = lax.dynamic_index_in_dim(
         tok_all.reshape(rows * seq, low, rows, col), here, 2, False
     ).reshape(rows * seq, 1, low * col)
@@ -284,7 +298,7 @@
     with_tok = (part_out + jnp.where(own, residual, 0.0)).reshape(rows * seq, tp * low * col)
 
     outgoing = jnp.dot(sel, with_tok.astype(bf16), preferred_element_type=f32).astype(bf16)
-    arrived = exchange(outgoing.reshape(zh * tp, cap * quarter, LANES), ("zh", "tp"))
+    arrived = exchange(outgoing.reshape(zh * tp, cap * quarter, LANES), (*ZH, "tp"))
     arrived = arrived.astype(f32).reshape(zh, tp, cap, quarter, LANES).sum(axis=1).astype(bf16)
     arrived = arrived.transpose(1, 2, 0, 3).reshape(cap, quarter * zh, LANES)
     sent = jnp.broadcast_to(
@@ -311,7 +325,7 @@
     back = back.reshape(rows * tp, zh, feat + LANES)
     back = exchange(back, PAIR).astype(f32)
     summed = back[:, :, :feat].reshape(chips, c, tp, zh, feat).sum(axis=(0, 2)).astype(bf16)
-    returned = exchange(summed.transpose(1, 0, 2), "zh").astype(f32)
+    returned = exchange(summed.transpose(1, 0, 2), ZH).astype(f32)
     mixer = back[:, :seq, feat : feat + low * col].reshape(rows, tp, seq, low, col).sum(axis=1)
     mixer = mixer.transpose(1, 2, 0, 3).reshape(seq, feat).astype(bf16)
     middle = (tokens.astype(f32) + mixer.astype(f32)).astype(bf16)
@@ -324,7 +338,7 @@
 
 
 def solution(mesh):
-    torus = Mesh(mesh.devices.reshape(8, 2, 2, 2, 2, mesh.shape["tp"]), (*EP, "tp"))
+    torus = Mesh(mesh.devices.reshape(4, 2, 2, 2, 2, 2, mesh.shape["tp"]), (*EP, "tp"))
     in_specs = (
         P(EP, "tp"),
         P("tp"),
@@ -343,6 +357,7 @@
         P(EP, "tp", None),
     )
     out_specs = (P(EP, "tp"), P(EP, "tp", None, None))
+
     return jax.shard_map(
         shards, mesh=torus, in_specs=in_specs, out_specs=out_specs, check_vma=False
     )

time: 161 us -> 167 us (1.037)
  waiting for transfers between devices: 43.5 us -> 48.1 us
    all_gather x4 -> x3, blocking collectives: 21.1 us -> 10.6 us  [shards(): all_rows = lax.all_gather(all_rows, axis, tiled=True)]
    all_gather x0 -> x1, blocking collectives: none -> 8.83 us  [shards(): all_rows = lax.all_gather(all_rows, GATHER[-1], tiled=True)]
    ppermute x0 -> x2, waiting for transfers between devices: none -> 6.63 us  [the longest x1 6.62 us: shards(): in_other = lax.ppermute(in_mine, 'zm', swap)]
    all_to_all x6, starting transfers between devices: 50.3 us -> 43.7 us  [exchange(): return lax.all_to_all(blocks, axes, split_axis=0, concat_axis=0, tiled=True)]
    ppermute x0 -> x2, starting transfers between devices: none -> 6.18 us  [the longest x1 3.79 us: shards(): in_other = lax.ppermute(in_mine, 'zm', swap)]
    all_to_all x6, waiting for transfers between devices: 43.4 us -> 41.5 us  [exchange(): return lax.all_to_all(blocks, axes, split_axis=0, concat_axis=0, tiled=True)]
  transfers between devices with their start and end apart: 8 -> 10, of which waited for: 7 -> 7; matrix products, arithmetic and copies ran while one was open for 5% -> 7% of each run, Pallas kernels for 0% -> 1%
where the time goes in v7:
time: 167 us; the launch traced here: 166 us
  starting transfers between devices  54.3 us (33%)
  waiting for transfers between devices  48.1 us (29%)
  blocking collectives  39.5 us (24%)
  local copies, waits for them, and re-layouts  10.3 us (6%)
  Pallas kernels  6.32 us (4%)
  other arithmetic  4.57 us (3%)
  matrix products  1.72 us (1%)
    all_to_all x6, starting transfers between devices, exchange(): return lax.all_to_all(blocks, axes, split_axis=0, concat_axis=0, tiled=True)  43.7 us
    all_to_all x6, waiting for transfers between devices, exchange(): return lax.all_to_all(blocks, axes, split_axis=0, concat_axis=0, tiled=True)  41.5 us
    all_to_all x1, blocking collectives, exchange(): return lax.all_to_all(blocks, axes, split_axis=0, concat_axis=0, tiled=True)  20 us
    all_gather x3, blocking collectives, shards(): all_rows = lax.all_gather(all_rows, axis, tiled=True)  10.6 us
    all_gather x1, blocking collectives, shards(): all_rows = lax.all_gather(all_rows, GATHER[-1], tiled=True)  8.83 us
    ppermute x1, waiting for transfers between devices, shards(): in_other = lax.ppermute(in_mine, 'zm', swap)  6.62 us
    ppermute x2, starting transfers between devices, shards(): lax.ppermute(w, 'c', [(0, 1), (1, 0)])  4.33 us
    pallas_call x1, Pallas kernels, experts(): pl.pallas_call(experts_kernel, out_shape=jax.ShapeDtypeStruct(whole, bf16...  4.23 us
  transfers between devices with their start and end apart: 10, of which 7 were waited for; matrix products, arithmetic and copies ran while one was open for 7% of the time, Pallas kernels for 1%

profile of v7, /device:TPU:1, one launch (start us, length us, event | category | flops | bytes accessed | tf_op | source)
XLA Modules:
  0.0 166.0 jit_solution(7336207927781105678)
XLA Ops:
  0.7 0.8 maximum_bitcast_fusion
  1.5 0.7 broadcast_in_dim.25
  2.2 15.6 %all-to-all-start = ((bf16[4,64,512]{2,1,0:T(8,128)(2,1)}), bf16[4,64,512]{2,1,0:T(8,128)(2,1)S(1)}, u32[]{:S(2)}, u32[]{:S(2)}) async-start(bf16[4,64,512]{2,1,0:T(8,128)(2,1)} %broadcast_in_dim.25), calls=%async_computation | async-start | bytes 524288 | tf_op jit(solution)/shard_map/all_to_all | solution.py:22
  17.8 0.8 reshape.282
  18.6 0.1 copy.241
  18.7 2.4 %all_gather.12 = bf16[16,512]{1,0:T(8,128)(2,1)S(1)} all-gather(bf16[8,512]{1,0:T(8,128)(2,1)S(1)} %fusion.21), channel_id=1, replica_groups=mesh['za'=4,'zm'=2,'zl'=2,'xh'=2,'xl'=2,'c'=2,'tp'=4] {'c'}, dimensions={0}, use_global_device_ids=true | all-gather | bytes 24576 | tf_op jit(solution)/shard_map/all_gather | solution.py:240
  21.2 3.2 %all_gather.13 = bf16[32,512]{1,0:T(8,128)(2,1)S(1)} all-gather(bf16[16,512]{1,0:T(8,128)(2,1)S(1)} %all_gather.12), channel_id=1, replica_groups=mesh['za'=4,'zm'=2,'zl'=2,'xh'=2,'xl'=2,'c'=2,'tp'=4] {'xl'}, dimensions={0}, use_global_device_ids=true | all-gather | bytes 49152 | tf_op jit(solution)/shard_map/all_gather | solution.py:240
  24.4 4.9 %all_gather.14 = bf16[64,512]{1,0:T(8,128)(2,1)S(1)} all-gather(bf16[32,512]{1,0:T(8,128)(2,1)S(1)} %all_gather.13), channel_id=1, replica_groups=mesh['za'=4,'zm'=2,'zl'=2,'xh'=2,'xl'=2,'c'=2,'tp'=4] {'xh'}, dimensions={0}, use_global_device_ids=true | all-gather | bytes 98304 | tf_op jit(solution)/shard_map/all_gather | solution.py:240
  29.4 2.2 %all-to-all-done = bf16[4,64,512]{2,1,0:T(8,128)(2,1)S(1)} async-done(((bf16[4,64,512]{2,1,0:T(8,128)(2,1)}), bf16[4,64,512]{2,1,0:T(8,128)(2,1)S(1)}, u32[]{:S(2)}, u32[]{:S(2)}) %all-to-all-start) | async-done | bytes 262176 | tf_op jit(solution)/shard_map/all_to_all | solution.py:22
  31.6 8.8 %all_gather.15 = bf16[128,512]{1,0:T(8,128)(2,1)S(1)} all-gather(bf16[64,512]{1,0:T(8,128)(2,1)S(1)} %all_gather.14), channel_id=1, replica_groups=mesh['za'=4,'zm'=2,'zl'=2,'xh'=2,'xl'=2,'c'=2,'tp'=4] {'zl'}, dimensions={0}, use_global_device_ids=true | all-gather | bytes 196608 | tf_op jit(solution)/shard_map/all_gather | solution.py:257
  40.5 0.1 multiply_reduce_fusion
  40.7 3.8 %collective-permute-start = (bf16[4,48,512]{2,1,0:T(8,128)(2,1)S(1)}, bf16[4,48,512]{2,1,0:T(8,128)(2,1)S(1)}, u32[]{:S(2)}, u32[]{:S(2)}) collective-permute-start(bf16[4,48,512]{2,1,0:T(8,128)(2,1)S(1)} %slice.23), channel_id=1, source_target_pairs={{0,64},{64,0},{1,65},{65,1},{2,66},{66,2},{3,67},{67,3},{4,68},{68... | collective-permute-start | bytes 589832 | tf_op jit(solution)/shard_map/ppermute | solution.py:245
  44.5 2.4 %collective-permute-start.1 = (bf16[4,16,512]{2,1,0:T(8,128)(2,1)S(1)}, bf16[4,16,512]{2,1,0:T(8,128)(2,1)S(1)}, u32[]{:S(2)}, u32[]{:S(2)}) collective-permute-start(bf16[4,16,512]{2,1,0:T(8,128)(2,1)S(1)} %slice.24), channel_id=1, source_target_pairs={{0,64},{64,0},{1,65},{65,1},{2,66},{66,2},{3,67},{67,3},{4,68},{68... | collective-permute-start | bytes 196616 | tf_op jit(solution)/shard_map/ppermute | solution.py:246
  46.9 0.1 copy.209
  47.0 0.4 reshape.283
  47.5 0.1 copy.239
  47.6 0.1 convert_reduce_fusion.1
  47.7 0.2 fusion.8
  48.0 6.6 %collective-permute-done = bf16[4,48,512]{2,1,0:T(8,128)(2,1)S(1)} collective-permute-done((bf16[4,48,512]{2,1,0:T(8,128)(2,1)S(1)}, bf16[4,48,512]{2,1,0:T(8,128)(2,1)S(1)}, u32[]{:S(2)}, u32[]{:S(2)}) %collective-permute-start) | collective-permute-done | bytes 196640 | tf_op jit(solution)/shard_map/ppermute | solution.py:245
  54.6 0.2 fusion.6
  54.8 0.1 fusion.10
  55.1 0.1 pad_maximum_fusion
  55.3 0.7 copy.208
  56.0 10.0 %all-to-all-start.1 = ((f32[64,4,128]{2,1,0:T(4,128)}), f32[64,4,128]{2,1,0:T(4,128)S(1)}, u32[]{:S(2)}, u32[]{:S(2)}) async-start(f32[64,4,128]{2,1,0:T(4,128)} %copy.208), calls=%async_computation.1 | async-start | bytes 262144 | tf_op jit(solution)/shard_map/all_to_all | solution.py:22
  66.2 0.3 copy.203
  66.4 8.1 %all-to-all-done.1 = f32[64,4,128]{2,1,0:T(4,128)S(1)} async-done(((f32[64,4,128]{2,1,0:T(4,128)}), f32[64,4,128]{2,1,0:T(4,128)S(1)}, u32[]{:S(2)}, u32[]{:S(2)}) %all-to-all-start.1) | async-done | bytes 131104 | tf_op jit(solution)/shard_map/all_to_all | solution.py:22
  74.6 2.1 %recurrence.1 = (bf16[16,4,512]{2,1,0:T(4,128)(2,1)}, f32[4,4,128]{2,1,0:T(4,128)}, f32[4,4,128]{2,1,0:T(4,128)}) custom-call(f32[16,4,4,128]{3,2,1,0:T(4,128)S(1)} %bitcast.105, f32[4,4,128,128]{3,2,1,0:T(8,128)S(1)} %copy-done, f32[4,128]{1,0:T(4,128)} %bitcast.126, bf16[1,128]{1,0:T(2,128)(2,1)} %bitcast.127), custom_call_target="tpu_custom_call" | custom-call | tf_op jit(solution)/shard_map/recurrence/pallas_call | solution.py:111
  76.7 3.8 %all-to-all-start.2 = ((bf16[16,4,512]{2,1,0:T(4,128)(2,1)}), bf16[16,4,512]{2,1,0:T(4,128)(2,1)S(1)}, u32[]{:S(2)}, u32[]{:S(2)}) async-start(bf16[16,4,512]{2,1,0:T(4,128)(2,1)} %get-tuple-element.9), calls=%async_computation.2 | async-start | bytes 131072 | tf_op jit(solution)/shard_map/all_to_all | solution.py:22
  80.4 0.3 multiply_convert_fusion
  80.8 1.1 convert_element_type.170
  81.8 4.5 %all-to-all-done.2 = bf16[16,4,512]{2,1,0:T(4,128)(2,1)S(1)} async-done(((bf16[16,4,512]{2,1,0:T(4,128)(2,1)}), bf16[16,4,512]{2,1,0:T(4,128)(2,1)S(1)}, u32[]{:S(2)}, u32[]{:S(2)}) %all-to-all-start.2) | async-done | bytes 65568 | tf_op jit(solution)/shard_map/all_to_all | solution.py:22
  86.4 0.1 fusion.23
  86.5 0.1 fusion.26
  86.8 0.2 fusion.2
  86.9 20.0 %all_to_all.35 = bf16[32,8,128]{2,1,0:T(8,128)(2,1)S(1)} all-to-all(bf16[32,8,128]{2,1,0:T(8,128)(2,1)S(1)} %fusion.2), channel_id=1, replica_groups=mesh['za'=4,'zm'=2,'zl'=2,'xh'=2,'xl'=2,'c'=2,'tp'=4] {'za','zm','tp'}, dimensions={0} | all-to-all | bytes 131072 | tf_op jit(solution)/shard_map/all_to_all | solution.py:22
  107.0 0.9 broadcast_in_dim.40
  107.9 6.1 %all-to-all-start.4 = ((bf16[64,32,128]{2,1,0:T(8,128)(2,1)}), bf16[64,32,128]{2,1,0:T(8,128)(2,1)S(1)}, u32[]{:S(2)}, u32[]{:S(2)}) async-start(bf16[64,32,128]{2,1,0:T(8,128)(2,1)} %bitcast.23), calls=%async_computation.4 | async-start | bytes 1048576 | tf_op jit(solution)/shard_map/all_to_all | solution.py:22
  114.0 0.3 copy.214
  114.3 1.0 copy-done.5
  115.3 0.3 copy.216
  115.6 0.2 fusion.5.gu0_ref
  115.9 2.4 %collective-permute-start.2 = (bf16[2048,256]{1,0:T(8,128)(2,1)S(1)}, bf16[2048,256]{1,0:T(8,128)(2,1)}, u32[]{:S(2)}, u32[]{:S(2)}) collective-permute-start(bf16[2048,256]{1,0:T(8,128)(2,1)S(1)} %fusion.5.gu0_ref), channel_id=1, source_target_pairs={{0,4},{4,0},{1,5},{5,1},{2,6},{6,2},{3,7},{7,3},{8,12},{12,8},{9,1... | collective-permute-start | bytes 3145736 | tf_op jit(solution)/shard_map/ppermute | solution.py:318
  118.3 2.0 %collective-permute-start.3 = (bf16[128,2048]{1,0:T(8,128)(2,1)S(1)}, bf16[128,2048]{1,0:T(8,128)(2,1)}, u32[]{:S(2)}, u32[]{:S(2)}) collective-permute-start(bf16[128,2048]{1,0:T(8,128)(2,1)S(1)} %pad.22.down0_ref), channel_id=1, source_target_pairs={{0,4},{4,0},{1,5},{5,1},{2,6},{6,2},{3,7},{7,3},{8,12},{12,8},{9,1... | collective-permute-start | bytes 1572872 | tf_op jit(solution)/shard_map/ppermute | solution.py:318
  120.3 0.1 slice_bitcast_fusion
  120.4 0.1 reshape_reshape.10
  120.6 0.7 reshape_reshape.11.gain_ref
  121.3 0.1 copy.218
  121.4 0.1 copy.219
  121.5 0.2 pad_maximum_fusion.1
  121.7 0.7 pad.23.rider_ref
  122.4 4.1 %all-to-all-done.4 = bf16[64,32,128]{2,1,0:T(8,128)(2,1)S(1)} async-done(((bf16[64,32,128]{2,1,0:T(8,128)(2,1)}), bf16[64,32,128]{2,1,0:T(8,128)(2,1)S(1)}, u32[]{:S(2)}, u32[]{:S(2)}) %all-to-all-start.4) | async-done | bytes 524320 | tf_op jit(solution)/shard_map/all_to_all | solution.py:22
  126.5 4.2 %experts.1 = bf16[16,4,8,640]{3,2,1,0:T(8,128)(2,1)} custom-call(bf16[16,4,32,128]{3,2,1,0:T(8,128)(2,1)S(1)} %bitcast.104, f32[16,1,128]{2,1,0:T(1,128)} %reshape_reshape.11.gain_ref, bf16[2048,256]{1,0:T(8,128)(2,1)} %copy-done.1, bf16[128,2048]{1,0:T(8,128)(2,1)} %copy-done.2, bf16[2048,256]{1,0:T(8,128)(2,1)} %collective-permute-done.2.gu1_ref, ...), custom_call_target="tpu_custom_call" | custom-call | tf_op jit(solution)/shard_map/experts/pallas_call | solution.py:187
  130.7 5.0 %all-to-all-start.5 = ((bf16[64,8,640]{2,1,0:T(8,128)(2,1)}), bf16[64,8,640]{2,1,0:T(8,128)(2,1)S(1)}, u32[]{:S(2)}, u32[]{:S(2)}) async-start(bf16[64,8,640]{2,1,0:T(8,128)(2,1)} %bitcast.108), calls=%async_computation.5 | async-start | bytes 1310720 | tf_op jit(solution)/shard_map/all_to_all | solution.py:22
  135.7 0.2 convert_reduce_fusion.2
  136.2 1.6 multiply_add_fusion
  137.8 11.8 %all-to-all-done.5 = bf16[64,8,640]{2,1,0:T(8,128)(2,1)S(1)} async-done(((bf16[64,8,640]{2,1,0:T(8,128)(2,1)}), bf16[64,8,640]{2,1,0:T(8,128)(2,1)S(1)}, u32[]{:S(2)}, u32[]{:S(2)}) %all-to-all-start.5) | async-done | bytes 655392 | tf_op jit(solution)/shard_map/all_to_all | solution.py:22
  149.6 0.1 slice.32
  149.8 0.6 copy.266
  150.4 3.3 %all-to-all-start.6 = ((bf16[8,2,512]{2,1,0:T(2,128)(2,1)}), bf16[8,2,512]{2,1,0:T(2,128)(2,1)S(1)}, u32[]{:S(2)}, u32[]{:S(2)}) async-start(bf16[8,2,512]{2,1,0:T(2,128)(2,1)} %bitcast.102), calls=%async_computation.6 | async-start | bytes 32768 | tf_op jit(solution)/shard_map/all_to_all | solution.py:22
  153.8 0.2 reshape.277
  154.0 0.2 reduce_sum.76
  154.2 0.1 reshape.284
  154.3 10.8 %all-to-all-done.6 = bf16[8,2,512]{2,1,0:T(2,128)(2,1)S(1)} async-done(((bf16[8,2,512]{2,1,0:T(2,128)(2,1)}), bf16[8,2,512]{2,1,0:T(2,128)(2,1)S(1)}, u32[]{:S(2)}, u32[]{:S(2)}) %all-to-all-start.6) | async-done | bytes 16416 | tf_op jit(solution)/shard_map/all_to_all | solution.py:22
  165.2 0.8 fusion.4
  (73 shorter events, 1.4 us)
Async XLA Ops:
  0.6 17.9 %copy-start.8 = (s32[4,2]{0,1:T(2,128)S(1)}, s32[4,2]{0,1:T(2,128)}, u32[]{:S(2)}) copy-start(s32[4,2]{0,1:T(2,128)} %param.25) | copy-start | bytes 100
  0.6 18.1 %copy-start.10 = (bf16[512]{0:T(512)(128)(2,1)S(1)}, bf16[512]{0:T(512)(128)(2,1)}, u32[]{:S(2)}) copy-start(bf16[512]{0:T(512)(128)(2,1)} %param.16) | copy-start | bytes 3076
  0.7 18.1 %copy-start.7 = (bf16[4,512]{1,0:T(4,128)(2,1)S(1)}, bf16[4,512]{1,0:T(4,128)(2,1)}, u32[]{:S(2)}) copy-start(bf16[4,512]{1,0:T(4,128)(2,1)} %param.15) | copy-start | bytes 12292
  2.2 29.4 %all-to-all-start = ((bf16[4,64,512]{2,1,0:T(8,128)(2,1)}), bf16[4,64,512]{2,1,0:T(8,128)(2,1)S(1)}, u32[]{:S(2)}, u32[]{:S(2)}) async-start(bf16[4,64,512]{2,1,0:T(8,128)(2,1)} %broadcast_in_dim.25), calls=%async_computation | async-start | bytes 524288 | tf_op jit(solution)/shard_map/all_to_all | solution.py:22
  40.7 13.9 %collective-permute-start = (bf16[4,48,512]{2,1,0:T(8,128)(2,1)S(1)}, bf16[4,48,512]{2,1,0:T(8,128)(2,1)S(1)}, u32[]{:S(2)}, u32[]{:S(2)}) collective-permute-start(bf16[4,48,512]{2,1,0:T(8,128)(2,1)S(1)} %slice.23), channel_id=1, source_target_pairs={{0,64},{64,0},{1,65},{65,1},{2,66},{66,2},{3,67},{67,3},{4,68},{68... | collective-permute-start | bytes 589832 | tf_op jit(solution)/shard_map/ppermute | solution.py:245
  44.5 42.0 %collective-permute-start.1 = (bf16[4,16,512]{2,1,0:T(8,128)(2,1)S(1)}, bf16[4,16,512]{2,1,0:T(8,128)(2,1)S(1)}, u32[]{:S(2)}, u32[]{:S(2)}) collective-permute-start(bf16[4,16,512]{2,1,0:T(8,128)(2,1)S(1)} %slice.24), channel_id=1, source_target_pairs={{0,64},{64,0},{1,65},{65,1},{2,66},{66,2},{3,67},{67,3},{4,68},{68... | collective-permute-start | bytes 196616 | tf_op jit(solution)/shard_map/ppermute | solution.py:246
  55.0 19.6 %copy-start = (f32[4,4,128,128]{3,2,1,0:T(8,128)S(1)}, f32[4,4,128,128]{3,2,1,0:T(8,128)}, u32[]{:S(2)}) copy-start(f32[4,4,128,128]{3,2,1,0:T(8,128)} %refs_1_.1) | copy-start | bytes 3145732
  56.0 18.5 %all-to-all-start.1 = ((f32[64,4,128]{2,1,0:T(4,128)}), f32[64,4,128]{2,1,0:T(4,128)S(1)}, u32[]{:S(2)}, u32[]{:S(2)}) async-start(f32[64,4,128]{2,1,0:T(4,128)} %copy.208), calls=%async_computation.1 | async-start | bytes 262144 | tf_op jit(solution)/shard_map/all_to_all | solution.py:22
  76.7 9.7 %all-to-all-start.2 = ((bf16[16,4,512]{2,1,0:T(4,128)(2,1)}), bf16[16,4,512]{2,1,0:T(4,128)(2,1)S(1)}, u32[]{:S(2)}, u32[]{:S(2)}) async-start(bf16[16,4,512]{2,1,0:T(4,128)(2,1)} %get-tuple-element.9), calls=%async_computation.2 | async-start | bytes 131072 | tf_op jit(solution)/shard_map/all_to_all | solution.py:22
  86.7 27.3 %copy-start.4 = (bf16[1,2048,112]{1,2,0:T(8,128)(2,1)S(1)}, bf16[1,2048,112]{1,2,0:T(8,128)(2,1)}, u32[]{:S(2)}) copy-start(bf16[1,2048,112]{1,2,0:T(8,128)(2,1)} %param.27) | copy-start | bytes 1376260
  107.9 18.5 %all-to-all-start.4 = ((bf16[64,32,128]{2,1,0:T(8,128)(2,1)}), bf16[64,32,128]{2,1,0:T(8,128)(2,1)S(1)}, u32[]{:S(2)}, u32[]{:S(2)}) async-start(bf16[64,32,128]{2,1,0:T(8,128)(2,1)} %bitcast.23), calls=%async_computation.4 | async-start | bytes 1048576 | tf_op jit(solution)/shard_map/all_to_all | solution.py:22
  114.3 1.0 copy-start.5
  115.6 2.6 %copy-start.3 = (bf16[1,112,2048]{2,1,0:T(8,128)(2,1)S(1)}, bf16[1,112,2048]{2,1,0:T(8,128)(2,1)}, u32[]{:S(2)}) copy-start(bf16[1,112,2048]{2,1,0:T(8,128)(2,1)} %param.29) | copy-start | bytes 1376260
  115.9 5.6 %copy-start.1 = (bf16[2048,256]{1,0:T(8,128)(2,1)}, bf16[2048,256]{1,0:T(8,128)(2,1)S(1)}, u32[]{:S(2)}) copy-start(bf16[2048,256]{1,0:T(8,128)(2,1)S(1)} %fusion.5.gu0_ref) | copy-start | bytes 3145732
  115.9 6.5 %collective-permute-start.2 = (bf16[2048,256]{1,0:T(8,128)(2,1)S(1)}, bf16[2048,256]{1,0:T(8,128)(2,1)}, u32[]{:S(2)}, u32[]{:S(2)}) collective-permute-start(bf16[2048,256]{1,0:T(8,128)(2,1)S(1)} %fusion.5.gu0_ref), channel_id=1, source_target_pairs={{0,4},{4,0},{1,5},{5,1},{2,6},{6,2},{3,7},{7,3},{8,12},{12,8},{9,1... | collective-permute-start | bytes 3145736 | tf_op jit(solution)/shard_map/ppermute | solution.py:318
  118.3 8.2 %copy-start.2 = (bf16[128,2048]{1,0:T(8,128)(2,1)}, bf16[128,2048]{1,0:T(8,128)(2,1)S(1)}, u32[]{:S(2)}) copy-start(bf16[128,2048]{1,0:T(8,128)(2,1)S(1)} %pad.22.down0_ref) | copy-start | bytes 1572868
  118.3 4.1 %collective-permute-start.3 = (bf16[128,2048]{1,0:T(8,128)(2,1)S(1)}, bf16[128,2048]{1,0:T(8,128)(2,1)}, u32[]{:S(2)}, u32[]{:S(2)}) collective-permute-start(bf16[128,2048]{1,0:T(8,128)(2,1)S(1)} %pad.22.down0_ref), channel_id=1, source_target_pairs={{0,4},{4,0},{1,5},{5,1},{2,6},{6,2},{3,7},{7,3},{8,12},{12,8},{9,1... | collective-permute-start | bytes 1572872 | tf_op jit(solution)/shard_map/ppermute | solution.py:318
  130.7 5.3 %copy-start.11 = (f32[4,2]{0,1:T(2,128)S(1)}, f32[4,2]{0,1:T(2,128)}, u32[]{:S(2)}) copy-start(f32[4,2]{0,1:T(2,128)} %param.26) | copy-start | bytes 100
  130.7 5.4 %copy-start.6 = (f32[4,4,128]{2,1,0:T(4,128)S(1)}, f32[4,4,128]{2,1,0:T(4,128)}, u32[]{:S(2)}) copy-start(f32[4,4,128]{2,1,0:T(4,128)} %get-tuple-element.10) | copy-start | bytes 24580
  130.7 5.4 %copy-start.9 = (f32[4,4,128]{2,1,0:T(4,128)S(1)}, f32[4,4,128]{2,1,0:T(4,128)}, u32[]{:S(2)}) copy-start(f32[4,4,128]{2,1,0:T(4,128)} %get-tuple-element.11) | copy-start | bytes 24580
  130.7 18.9 %all-to-all-start.5 = ((bf16[64,8,640]{2,1,0:T(8,128)(2,1)}), bf16[64,8,640]{2,1,0:T(8,128)(2,1)S(1)}, u32[]{:S(2)}, u32[]{:S(2)}) async-start(bf16[64,8,640]{2,1,0:T(8,128)(2,1)} %bitcast.108), calls=%async_computation.5 | async-start | bytes 1310720 | tf_op jit(solution)/shard_map/all_to_all | solution.py:22
  150.4 14.7 %all-to-all-start.6 = ((bf16[8,2,512]{2,1,0:T(2,128)(2,1)}), bf16[8,2,512]{2,1,0:T(2,128)(2,1)S(1)}, u32[]{:S(2)}, u32[]{:S(2)}) async-start(bf16[8,2,512]{2,1,0:T(2,128)(2,1)} %bitcast.102), calls=%async_computation.6 | async-start | bytes 32768 | tf_op jit(solution)/shard_map/all_to_all | solution.py:22

commit v8 on v6

--- a/solution.py
+++ b/solution.py
@@ -154,10 +154,9 @@
     for n in range(sources):
         block = rows_v[n].reshape(count, lanes).astype(f32)
         second[:, n * lanes : (n + 1) * lanes] = (block * scale * gain_ref[n]).astype(bf16)
-    copies[0].wait()
-    copies[1].wait()
     hidden = []
     for k in range(2):
+        copies[k].wait()
         both = jnp.dot(second[...], gu_v[k], preferred_element_type=f32)
         gate = both[:, :lanes]
         hidden.append((gate / (1.0 + jnp.exp(-gate)) * both[:, lanes:]).astype(bf16))
@@ -239,11 +238,24 @@
     for axis in GATHER:
         all_rows = lax.all_gather(all_rows, axis, tiled=True)
 
+    def ordered(w):
+        return w.reshape(zh, rows, col, -1).transpose(1, 0, 2, 3).reshape(width, -1)
+
+    units = w_gate.shape[2]
+    fill = ((0, 0), (0, LANES - units))
+    gate_up = jnp.concatenate(
+        [jnp.pad(ordered(w_gate[0]), fill), jnp.pad(ordered(w_up[0]), fill)], axis=1
+    )
+    down = jnp.pad(w_down[0], fill[::-1])
+    weights_of = [(gate_up, down), tuple(lax.ppermute(w, "c", [(0, 1), (1, 0)]) for w in (gate_up, down))]
+
     all_rows = all_rows.reshape(2, 2, 2, 2, 2, seq, feat)
     order = tuple(GATHER[::-1].index(axis) for axis in ROW)
     all_rows = all_rows.transpose(*order, 4, 5, 6).reshape(rows, 2, seq, feat)
     experts_all = all_rows[:, 1, :, : route_experts.shape[1]].astype(jnp.int32)
-    w_all, tok_all = lax.optimization_barrier((w_all, all_rows[:, 0].reshape(rows * seq, feat)))
+    w_all, tok_all, weights_of = lax.optimization_barrier(
+        (w_all, all_rows[:, 0].reshape(rows * seq, feat), weights_of)
+    )
     w_in = w_all[:, : 3 * col].reshape(tp, low * 3 * col, feat)
     w_out = w_all[:, 3 * col :].reshape(tp, low * col, feat)
 
@@ -291,17 +303,6 @@
         arrived[None, :, None], (chips, c, tp, quarter * zh, LANES)
     ).reshape(rows * tp, quarter * zh, LANES)
     block = exchange(sent, PAIR).reshape(rows, tp, quarter * zh, LANES)
-
-    def ordered(w):
-        return w.reshape(zh, rows, col, -1).transpose(1, 0, 2, 3).reshape(width, -1)
-
-    units = w_gate.shape[2]
-    fill = ((0, 0), (0, LANES - units))
-    gate_up = jnp.concatenate(
-        [jnp.pad(ordered(w_gate[0]), fill), jnp.pad(ordered(w_up[0]), fill)], axis=1
-    )
-    down = jnp.pad(w_down[0], fill[::-1])
-    weights_of = [(gate_up, down), tuple(lax.ppermute(w, "c", [(0, 1), (1, 0)]) for w in (gate_up, down))]
 
     gain_all = got[:, :, :, used : used + share].transpose(1, 0, 2, 3)
     gain_all = ordered(gain_all.reshape(width, 1)).reshape(rows, 1, LANES)

time: 161 us -> 161 us (level)
  starting transfers between devices: 54.6 us -> 49.6 us
  waiting for transfers between devices: 43.5 us -> 46.6 us
  blocking collectives: 39.7 us -> 41.8 us
    all_to_all x6, starting transfers between devices: 50.3 us -> 44.7 us  [exchange(): return lax.all_to_all(blocks, axes, split_axis=0, concat_axis=0, tiled=True)]
    all_to_all x1, blocking collectives: 18.6 us -> 24 us  [exchange(): return lax.all_to_all(blocks, axes, split_axis=0, concat_axis=0, tiled=True)]
    all_gather x4, blocking collectives: 21.1 us -> 17.8 us  [shards(): all_rows = lax.all_gather(all_rows, axis, tiled=True)]
    all_to_all x6, waiting for transfers between devices: 43.4 us -> 46.6 us  [exchange(): return lax.all_to_all(blocks, axes, split_axis=0, concat_axis=0, tiled=True)]
  transfers between devices with their start and end apart: 8 -> 8, of which waited for: 7 -> 6; matrix products, arithmetic and copies ran while one was open for 5% -> 5% of each run, Pallas kernels for 0% -> 0%
where the time goes in v8:
time: 161 us; the launch traced here: 160 us
  starting transfers between devices  49.6 us (31%)
  waiting for transfers between devices  46.6 us (29%)
  blocking collectives  41.8 us (26%)
  local copies, waits for them, and re-layouts  9.13 us (6%)
  Pallas kernels  6.29 us (4%)
  other arithmetic  4.15 us (3%)
    all_to_all x6, waiting for transfers between devices, exchange(): return lax.all_to_all(blocks, axes, split_axis=0, concat_axis=0, tiled=True)  46.6 us
    all_to_all x6, starting transfers between devices, exchange(): return lax.all_to_all(blocks, axes, split_axis=0, concat_axis=0, tiled=True)  44.7 us
    all_to_all x1, blocking collectives, exchange(): return lax.all_to_all(blocks, axes, split_axis=0, concat_axis=0, tiled=True)  24 us
    all_gather x4, blocking collectives, shards(): all_rows = lax.all_gather(all_rows, axis, tiled=True)  17.8 us
    ppermute x2, starting transfers between devices, shards(): lax.ppermute(w, 'c', [(0, 1), (1, 0)])  4.92 us
    pallas_call x1, Pallas kernels, experts(): pl.pallas_call(experts_kernel, out_shape=jax.ShapeDtypeStruct(whole, bf16...  4.22 us
  transfers between devices with their start and end apart: 8, of which 6 were waited for; matrix products, arithmetic and copies ran while one was open for 5% of the time, Pallas kernels for 0%

profile of v8, /device:TPU:1, one launch (start us, length us, event | category | flops | bytes accessed | tf_op | source)
XLA Modules:
  0.0 160.2 jit_solution(2701353533213715158)
XLA Ops:
  0.6 0.8 maximum_bitcast_fusion
  1.5 0.9 broadcast_in_dim.27
  2.3 15.6 %all-to-all-start = ((bf16[8,64,512]{2,1,0:T(8,128)(2,1)}), bf16[8,64,512]{2,1,0:T(8,128)(2,1)S(1)}, u32[]{:S(2)}, u32[]{:S(2)}) async-start(bf16[8,64,512]{2,1,0:T(8,128)(2,1)} %broadcast_in_dim.27), calls=%async_computation | async-start | bytes 1048576 | tf_op jit(solution)/shard_map/all_to_all | solution.py:21
  18.0 0.3 copy.184
  18.3 0.7 copy-done.6
  19.0 0.3 copy.182
  19.4 0.2 fusion.5.gu0_ref
  19.6 3.0 %collective-permute-start = (bf16[2048,256]{1,0:T(8,128)(2,1)S(1)}, bf16[2048,256]{1,0:T(8,128)(2,1)S(1)}, u32[]{:S(2)}, u32[]{:S(2)}) collective-permute-start(bf16[2048,256]{1,0:T(8,128)(2,1)S(1)} %fusion.5.gu0_ref), channel_id=1, source_target_pairs={{0,4},{4,0},{1,5},{5,1},{2,6},{6,2},{3,7},{7,3},{8,12},{12,8},{9,1... | collective-permute-start | bytes 3145736 | tf_op jit(solution)/shard_map/ppermute | solution.py:250
  22.7 1.9 %collective-permute-start.1 = (bf16[128,2048]{1,0:T(8,128)(2,1)S(1)}, bf16[128,2048]{1,0:T(8,128)(2,1)}, u32[]{:S(2)}, u32[]{:S(2)}) collective-permute-start(bf16[128,2048]{1,0:T(8,128)(2,1)S(1)} %pad.22.down0_ref), channel_id=1, source_target_pairs={{0,4},{4,0},{1,5},{5,1},{2,6},{6,2},{3,7},{7,3},{8,12},{12,8},{9,1... | collective-permute-start | bytes 1572872 | tf_op jit(solution)/shard_map/ppermute | solution.py:250
  24.6 0.1 copy.211
  24.7 2.0 %all_gather.12 = bf16[16,512]{1,0:T(8,128)(2,1)S(1)} all-gather(bf16[8,512]{1,0:T(8,128)(2,1)S(1)} %fusion.9), channel_id=1, replica_groups=mesh['zh'=8,'zl'=2,'xh'=2,'xl'=2,'c'=2,'tp'=4] {'c'}, dimensions={0}, use_global_device_ids=true | all-gather | bytes 24576 | tf_op jit(solution)/shard_map/all_gather | solution.py:239
  26.7 3.5 %all_gather.13 = bf16[32,512]{1,0:T(8,128)(2,1)S(1)} all-gather(bf16[16,512]{1,0:T(8,128)(2,1)S(1)} %all_gather.12), channel_id=1, replica_groups=mesh['zh'=8,'zl'=2,'xh'=2,'xl'=2,'c'=2,'tp'=4] {'xl'}, dimensions={0}, use_global_device_ids=true | all-gather | bytes 49152 | tf_op jit(solution)/shard_map/all_gather | solution.py:239
  30.2 5.2 %all_gather.14 = bf16[64,512]{1,0:T(8,128)(2,1)S(1)} all-gather(bf16[32,512]{1,0:T(8,128)(2,1)S(1)} %all_gather.13), channel_id=1, replica_groups=mesh['zh'=8,'zl'=2,'xh'=2,'xl'=2,'c'=2,'tp'=4] {'xh'}, dimensions={0}, use_global_device_ids=true | all-gather | bytes 98304 | tf_op jit(solution)/shard_map/all_gather | solution.py:239
  35.5 7.0 %all_gather.15 = bf16[128,512]{1,0:T(8,128)(2,1)S(1)} all-gather(bf16[64,512]{1,0:T(8,128)(2,1)S(1)} %all_gather.14), channel_id=1, replica_groups=mesh['zh'=8,'zl'=2,'xh'=2,'xl'=2,'c'=2,'tp'=4] {'zl'}, dimensions={0}, use_global_device_ids=true | all-gather | bytes 196608 | tf_op jit(solution)/shard_map/all_gather | solution.py:239
  42.6 0.1 copy.210
  42.8 0.1 reshape.226
  42.9 0.1 convert_reduce_fusion.1
  43.1 0.7 all-to-all-done
  43.8 0.1 multiply_convert_fusion.1
  43.9 0.1 broadcast_in_dim.29
  44.0 0.1 copy.187
  44.2 0.3 convolution_bitcast_fusion
  44.4 0.1 broadcast_in_dim.30
  44.5 0.1 pad_maximum_fusion
  44.7 0.1 copy.188
  44.7 0.7 copy.189
  45.5 11.1 %all-to-all-start.1 = ((f32[64,4,128]{2,1,0:T(4,128)}), f32[64,4,128]{2,1,0:T(4,128)S(1)}, u32[]{:S(2)}, u32[]{:S(2)}) async-start(f32[64,4,128]{2,1,0:T(4,128)} %copy.189), calls=%async_computation.1 | async-start | bytes 262144 | tf_op jit(solution)/shard_map/all_to_all | solution.py:21
  56.6 0.1 copy.180
  56.7 0.3 copy.181
  57.0 0.1 fusion.10
  57.0 8.1 %all-to-all-done.1 = f32[64,4,128]{2,1,0:T(4,128)S(1)} async-done(((f32[64,4,128]{2,1,0:T(4,128)}), f32[64,4,128]{2,1,0:T(4,128)S(1)}, u32[]{:S(2)}, u32[]{:S(2)}) %all-to-all-start.1) | async-done | bytes 131104 | tf_op jit(solution)/shard_map/all_to_all | solution.py:21
  65.1 2.1 %recurrence.1 = (bf16[16,4,512]{2,1,0:T(4,128)(2,1)}, f32[4,4,128]{2,1,0:T(4,128)}, f32[4,4,128]{2,1,0:T(4,128)}) custom-call(f32[16,4,4,128]{3,2,1,0:T(4,128)S(1)} %bitcast.88, f32[4,4,128,128]{3,2,1,0:T(8,128)S(1)} %copy-done, f32[4,128]{1,0:T(4,128)} %bitcast.113, bf16[1,128]{1,0:T(2,128)(2,1)} %bitcast.114), custom_call_target="tpu_custom_call" | custom-call | tf_op jit(solution)/shard_map/recurrence/pallas_call | solution.py:110
  67.2 3.8 %all-to-all-start.2 = ((bf16[16,4,512]{2,1,0:T(4,128)(2,1)}), bf16[16,4,512]{2,1,0:T(4,128)(2,1)S(1)}, u32[]{:S(2)}, u32[]{:S(2)}) async-start(bf16[16,4,512]{2,1,0:T(4,128)(2,1)} %get-tuple-element.13), calls=%async_computation.2 | async-start | bytes 131072 | tf_op jit(solution)/shard_map/all_to_all | solution.py:21
  70.9 0.3 multiply_convert_fusion
  71.3 1.1 convert_element_type.151
  72.4 0.1 copy.190
  72.5 4.3 %all-to-all-done.2 = bf16[16,4,512]{2,1,0:T(4,128)(2,1)S(1)} async-done(((bf16[16,4,512]{2,1,0:T(4,128)(2,1)}), bf16[16,4,512]{2,1,0:T(4,128)(2,1)S(1)}, u32[]{:S(2)}, u32[]{:S(2)}) %all-to-all-start.2) | async-done | bytes 65568 | tf_op jit(solution)/shard_map/all_to_all | solution.py:21
  76.9 0.2 fusion.11
  77.0 0.2 fusion.2
  77.2 24.0 %all_to_all.35 = bf16[32,8,128]{2,1,0:T(8,128)(2,1)S(1)} all-to-all(bf16[32,8,128]{2,1,0:T(8,128)(2,1)S(1)} %fusion.2), channel_id=1, replica_groups=mesh['zh'=8,'zl'=2,'xh'=2,'xl'=2,'c'=2,'tp'=4] {'zh','tp'}, dimensions={0} | all-to-all | bytes 131072 | tf_op jit(solution)/shard_map/all_to_all | solution.py:21
  101.3 0.9 broadcast_in_dim.43
  102.2 6.0 %all-to-all-start.4 = ((bf16[64,32,128]{2,1,0:T(8,128)(2,1)}), bf16[64,32,128]{2,1,0:T(8,128)(2,1)S(1)}, u32[]{:S(2)}, u32[]{:S(2)}) async-start(bf16[64,32,128]{2,1,0:T(8,128)(2,1)} %bitcast.29), calls=%async_computation.4 | async-start | bytes 1048576 | tf_op jit(solution)/shard_map/all_to_all | solution.py:21
  108.3 0.1 slice_bitcast_fusion
  108.4 0.1 reshape_reshape.10
  108.6 0.7 reshape_reshape.11.gain_ref
  109.3 0.1 copy.194
  109.4 0.7 pad.23.rider_ref
  110.1 10.7 %all-to-all-done.4 = bf16[64,32,128]{2,1,0:T(8,128)(2,1)S(1)} async-done(((bf16[64,32,128]{2,1,0:T(8,128)(2,1)}), bf16[64,32,128]{2,1,0:T(8,128)(2,1)S(1)}, u32[]{:S(2)}, u32[]{:S(2)}) %all-to-all-start.4) | async-done | bytes 524320 | tf_op jit(solution)/shard_map/all_to_all | solution.py:21
  120.8 4.2 %experts.1 = bf16[16,4,8,640]{3,2,1,0:T(8,128)(2,1)} custom-call(bf16[16,4,32,128]{3,2,1,0:T(8,128)(2,1)S(1)} %bitcast.87, f32[16,1,128]{2,1,0:T(1,128)} %reshape_reshape.11.gain_ref, bf16[2048,256]{1,0:T(8,128)(2,1)} %copy-done.1, bf16[128,2048]{1,0:T(8,128)(2,1)} %copy-done.2, bf16[2048,256]{1,0:T(8,128)(2,1)} %copy-done.3, ...), custom_call_target="tpu_custom_call" | custom-call | tf_op jit(solution)/shard_map/experts/pallas_call | solution.py:186
  125.0 4.9 %all-to-all-start.5 = ((bf16[64,8,640]{2,1,0:T(8,128)(2,1)}), bf16[64,8,640]{2,1,0:T(8,128)(2,1)S(1)}, u32[]{:S(2)}, u32[]{:S(2)}) async-start(bf16[64,8,640]{2,1,0:T(8,128)(2,1)} %bitcast.91), calls=%async_computation.5 | async-start | bytes 1310720 | tf_op jit(solution)/shard_map/all_to_all | solution.py:21
  129.9 0.2 convert_reduce_fusion.2
  130.1 0.1 iota_compare_fusion.6
  130.2 0.1 select_reduce_fusion
  130.3 1.6 multiply_add_fusion
  131.9 11.9 %all-to-all-done.5 = bf16[64,8,640]{2,1,0:T(8,128)(2,1)S(1)} async-done(((bf16[64,8,640]{2,1,0:T(8,128)(2,1)}), bf16[64,8,640]{2,1,0:T(8,128)(2,1)S(1)}, u32[]{:S(2)}, u32[]{:S(2)}) %all-to-all-start.5) | async-done | bytes 655392 | tf_op jit(solution)/shard_map/all_to_all | solution.py:21
  143.9 0.1 slice.32
  144.0 0.1 reduce_sum.79
  144.1 0.6 copy.224
  144.7 3.3 %all-to-all-start.6 = ((bf16[8,2,512]{2,1,0:T(2,128)(2,1)}), bf16[8,2,512]{2,1,0:T(2,128)(2,1)S(1)}, u32[]{:S(2)}, u32[]{:S(2)}) async-start(bf16[8,2,512]{2,1,0:T(2,128)(2,1)} %bitcast.85), calls=%async_computation.6 | async-start | bytes 32768 | tf_op jit(solution)/shard_map/all_to_all | solution.py:21
  148.0 0.2 reshape.222
  148.2 0.2 reduce_sum.76
  148.5 0.1 reshape.227
  148.6 10.8 %all-to-all-done.6 = bf16[8,2,512]{2,1,0:T(2,128)(2,1)S(1)} async-done(((bf16[8,2,512]{2,1,0:T(2,128)(2,1)}), bf16[8,2,512]{2,1,0:T(2,128)(2,1)S(1)}, u32[]{:S(2)}, u32[]{:S(2)}) %all-to-all-start.6) | async-done | bytes 16416 | tf_op jit(solution)/shard_map/all_to_all | solution.py:21
  159.4 0.8 fusion.4
  (68 shorter events, 0.7 us)
Async XLA Ops:
  0.6 17.3 %copy-start.5 = (bf16[1,2048,112]{1,2,0:T(8,128)(2,1)S(1)}, bf16[1,2048,112]{1,2,0:T(8,128)(2,1)}, u32[]{:S(2)}) copy-start(bf16[1,2048,112]{1,2,0:T(8,128)(2,1)} %param.28) | copy-start | bytes 1376260
  2.3 41.5 %all-to-all-start = ((bf16[8,64,512]{2,1,0:T(8,128)(2,1)}), bf16[8,64,512]{2,1,0:T(8,128)(2,1)S(1)}, u32[]{:S(2)}, u32[]{:S(2)}) async-start(bf16[8,64,512]{2,1,0:T(8,128)(2,1)} %broadcast_in_dim.27), calls=%async_computation | async-start | bytes 1048576 | tf_op jit(solution)/shard_map/all_to_all | solution.py:21
  18.0 1.0 copy-start.6
  19.3 3.3 %copy-start.4 = (bf16[1,112,2048]{2,1,0:T(8,128)(2,1)S(1)}, bf16[1,112,2048]{2,1,0:T(8,128)(2,1)}, u32[]{:S(2)}) copy-start(bf16[1,112,2048]{2,1,0:T(8,128)(2,1)} %param.29) | copy-start | bytes 1376260
  19.3 5.3 %copy-start.9 = (s32[4,2]{0,1:T(2,128)S(1)}, s32[4,2]{0,1:T(2,128)}, u32[]{:S(2)}) copy-start(s32[4,2]{0,1:T(2,128)} %param.25) | copy-start | bytes 100
  19.3 5.4 %copy-start.8 = (bf16[4,512]{1,0:T(4,128)(2,1)S(1)}, bf16[4,512]{1,0:T(4,128)(2,1)}, u32[]{:S(2)}) copy-start(bf16[4,512]{1,0:T(4,128)(2,1)} %param.15) | copy-start | bytes 12292
  19.6 24.4 %copy-start.1 = (bf16[2048,256]{1,0:T(8,128)(2,1)}, bf16[2048,256]{1,0:T(8,128)(2,1)S(1)}, u32[]{:S(2)}) copy-start(bf16[2048,256]{1,0:T(8,128)(2,1)S(1)} %fusion.5.gu0_ref) | copy-start | bytes 3145732
  19.6 23.2 %copy-start.11 = (bf16[512]{0:T(512)(128)(2,1)S(1)}, bf16[512]{0:T(512)(128)(2,1)}, u32[]{:S(2)}) copy-start(bf16[512]{0:T(512)(128)(2,1)} %param.16) | copy-start | bytes 3076
  19.6 23.2 %copy-start.12 = (bf16[512]{0:T(512)(128)(2,1)S(1)}, bf16[512]{0:T(512)(128)(2,1)}, u32[]{:S(2)}) copy-start(bf16[512]{0:T(512)(128)(2,1)} %param.24) | copy-start | bytes 3076
  19.6 23.5 %collective-permute-start = (bf16[2048,256]{1,0:T(8,128)(2,1)S(1)}, bf16[2048,256]{1,0:T(8,128)(2,1)S(1)}, u32[]{:S(2)}, u32[]{:S(2)}) collective-permute-start(bf16[2048,256]{1,0:T(8,128)(2,1)S(1)} %fusion.5.gu0_ref), channel_id=1, source_target_pairs={{0,4},{4,0},{1,5},{5,1},{2,6},{6,2},{3,7},{7,3},{8,12},{12,8},{9,1... | collective-permute-start | bytes 3145736 | tf_op jit(solution)/shard_map/ppermute | solution.py:250
  22.7 21.5 %copy-start.2 = (bf16[128,2048]{1,0:T(8,128)(2,1)}, bf16[128,2048]{1,0:T(8,128)(2,1)S(1)}, u32[]{:S(2)}) copy-start(bf16[128,2048]{1,0:T(8,128)(2,1)S(1)} %pad.22.down0_ref) | copy-start | bytes 1572868
  22.7 20.4 %collective-permute-start.1 = (bf16[128,2048]{1,0:T(8,128)(2,1)S(1)}, bf16[128,2048]{1,0:T(8,128)(2,1)}, u32[]{:S(2)}, u32[]{:S(2)}) collective-permute-start(bf16[128,2048]{1,0:T(8,128)(2,1)S(1)} %pad.22.down0_ref), channel_id=1, source_target_pairs={{0,4},{4,0},{1,5},{5,1},{2,6},{6,2},{3,7},{7,3},{8,12},{12,8},{9,1... | collective-permute-start | bytes 1572872 | tf_op jit(solution)/shard_map/ppermute | solution.py:250
  43.1 1.6 %copy-start.3 = (bf16[2048,256]{1,0:T(8,128)(2,1)}, bf16[2048,256]{1,0:T(8,128)(2,1)S(1)}, u32[]{:S(2)}) copy-start(bf16[2048,256]{1,0:T(8,128)(2,1)S(1)} %collective-permute-done.gu1_ref) | copy-start | bytes 3145732
  44.4 20.7 %copy-start = (f32[4,4,128,128]{3,2,1,0:T(8,128)S(1)}, f32[4,4,128,128]{3,2,1,0:T(8,128)}, u32[]{:S(2)}) copy-start(f32[4,4,128,128]{3,2,1,0:T(8,128)} %refs_1_.1) | copy-start | bytes 3145732
  45.5 19.6 %all-to-all-start.1 = ((f32[64,4,128]{2,1,0:T(4,128)}), f32[64,4,128]{2,1,0:T(4,128)S(1)}, u32[]{:S(2)}, u32[]{:S(2)}) async-start(f32[64,4,128]{2,1,0:T(4,128)} %copy.189), calls=%async_computation.1 | async-start | bytes 262144 | tf_op jit(solution)/shard_map/all_to_all | solution.py:21
  67.2 9.7 %all-to-all-start.2 = ((bf16[16,4,512]{2,1,0:T(4,128)(2,1)}), bf16[16,4,512]{2,1,0:T(4,128)(2,1)S(1)}, u32[]{:S(2)}, u32[]{:S(2)}) async-start(bf16[16,4,512]{2,1,0:T(4,128)(2,1)} %get-tuple-element.13), calls=%async_computation.2 | async-start | bytes 131072 | tf_op jit(solution)/shard_map/all_to_all | solution.py:21
  102.2 18.5 %all-to-all-start.4 = ((bf16[64,32,128]{2,1,0:T(8,128)(2,1)}), bf16[64,32,128]{2,1,0:T(8,128)(2,1)S(1)}, u32[]{:S(2)}, u32[]{:S(2)}) async-start(bf16[64,32,128]{2,1,0:T(8,128)(2,1)} %bitcast.29), calls=%async_computation.4 | async-start | bytes 1048576 | tf_op jit(solution)/shard_map/all_to_all | solution.py:21
  125.0 5.2 %copy-start.13 = (f32[4,2]{0,1:T(2,128)S(1)}, f32[4,2]{0,1:T(2,128)}, u32[]{:S(2)}) copy-start(f32[4,2]{0,1:T(2,128)} %param.26) | copy-start | bytes 100
  125.0 5.3 %copy-start.10 = (f32[4,4,128]{2,1,0:T(4,128)S(1)}, f32[4,4,128]{2,1,0:T(4,128)}, u32[]{:S(2)}) copy-start(f32[4,4,128]{2,1,0:T(4,128)} %get-tuple-element.19) | copy-start | bytes 24580
  125.0 5.3 %copy-start.7 = (f32[4,4,128]{2,1,0:T(4,128)S(1)}, f32[4,4,128]{2,1,0:T(4,128)}, u32[]{:S(2)}) copy-start(f32[4,4,128]{2,1,0:T(4,128)} %get-tuple-element.18) | copy-start | bytes 24580
  125.0 18.8 %all-to-all-start.5 = ((bf16[64,8,640]{2,1,0:T(8,128)(2,1)}), bf16[64,8,640]{2,1,0:T(8,128)(2,1)S(1)}, u32[]{:S(2)}, u32[]{:S(2)}) async-start(bf16[64,8,640]{2,1,0:T(8,128)(2,1)} %bitcast.91), calls=%async_computation.5 | async-start | bytes 1310720 | tf_op jit(solution)/shard_map/all_to_all | solution.py:21
  144.7 14.7 %all-to-all-start.6 = ((bf16[8,2,512]{2,1,0:T(2,128)(2,1)}), bf16[8,2,512]{2,1,0:T(2,128)(2,1)S(1)}, u32[]{:S(2)}, u32[]{:S(2)}) async-start(bf16[8,2,512]{2,1,0:T(2,128)(2,1)} %bitcast.85), calls=%async_computation.6 | async-start | bytes 32768 | tf_op jit(solution)/shard_map/all_to_all | solution.py:21

commit v9 on v6

--- a/solution.py
+++ b/solution.py
@@ -121,25 +121,19 @@
             pl.BlockSpec(memory_space=pltpu.VMEM),
         ],
         out_specs=tuple(pl.BlockSpec(memory_space=pltpu.VMEM) for _ in range(3)),
+        compiler_params=pltpu.CompilerParams(vmem_limit_bytes=16 << 20),
         name="recurrence",
     )(resident(got), resident(state), floors, gain)
 
 
 def experts_kernel(
-    rows_v, gain_ref, gu0_ref, down0_ref, gu1_ref, down1_ref, rider_ref, out_ref,
-    second, gu_v, down_v, out_v, sems, out_sems,
+    rows_v, gain_ref, gu0_ref, down0_ref, gu1_any, down1_any, rider_ref, out_ref,
+    second, gu1_ref, down1_ref, out_v, sems, out_sems,
 ):
-    copies = [
-        pltpu.make_async_copy(src, dst, sems.at[n])
-        for n, (src, dst) in enumerate(
-            (
-                (gu0_ref, gu_v.at[0]),
-                (gu1_ref, gu_v.at[1]),
-                (down0_ref, down_v.at[0]),
-                (down1_ref, down_v.at[1]),
-            )
-        )
-    ]
+    copies = (
+        pltpu.make_async_copy(gu1_any, gu1_ref, sems.at[0]),
+        pltpu.make_async_copy(down1_any, down1_ref, sems.at[1]),
+    )
     for copy in copies:
         copy.start()
     sources, parts, height, lanes = rows_v.shape
@@ -154,20 +148,19 @@
     for n in range(sources):
         block = rows_v[n].reshape(count, lanes).astype(f32)
         second[:, n * lanes : (n + 1) * lanes] = (block * scale * gain_ref[n]).astype(bf16)
-    copies[0].wait()
-    copies[1].wait()
     hidden = []
-    for k in range(2):
-        both = jnp.dot(second[...], gu_v[k], preferred_element_type=f32)
+    for gu_ref in (gu0_ref, gu1_ref):
+        if gu_ref is gu1_ref:
+            copies[0].wait()
+        both = jnp.dot(second[...], gu_ref[...], preferred_element_type=f32)
         gate = both[:, :lanes]
         hidden.append((gate / (1.0 + jnp.exp(-gate)) * both[:, lanes:]).astype(bf16))
-    copies[2].wait()
-    copies[3].wait()
+    copies[1].wait()
     outs = []
     for part in range(parts):
         at = slice(part * feat, (part + 1) * feat)
-        piece = jnp.dot(hidden[0], down_v[0, :, at], preferred_element_type=f32)
-        piece = piece + jnp.dot(hidden[1], down_v[1, :, at], preferred_element_type=f32)
+        piece = jnp.dot(hidden[0], down0_ref[:, at], preferred_element_type=f32)
+        piece = piece + jnp.dot(hidden[1], down1_ref[:, at], preferred_element_type=f32)
         out_v[:, part, :, :feat] = piece.astype(bf16).reshape(count // zh, zh, feat)
         outs.append(pltpu.make_async_copy(out_v.at[:, part], out_ref.at[:, part], out_sems.at[part]))
         outs[-1].start()
@@ -187,18 +180,19 @@
     return pl.pallas_call(
         experts_kernel,
         out_shape=jax.ShapeDtypeStruct(whole, bf16),
-        in_specs=[vmem, vmem, anywhere, anywhere, anywhere, anywhere, vmem],
+        in_specs=[vmem, vmem, vmem, vmem, anywhere, anywhere, vmem],
         out_specs=anywhere,
         scratch_shapes=[
             pltpu.VMEM((count, gate_up.shape[0]), bf16),
-            pltpu.VMEM((2, *gate_up.shape), bf16),
-            pltpu.VMEM((2, *down.shape), bf16),
+            pltpu.VMEM(gate_up.shape, bf16),
+            pltpu.VMEM(down.shape, bf16),
             pltpu.VMEM(whole, bf16),
-            pltpu.SemaphoreType.DMA((4,)),
+            pltpu.SemaphoreType.DMA((2,)),
             pltpu.SemaphoreType.DMA((parts,)),
         ],
+        compiler_params=pltpu.CompilerParams(vmem_limit_bytes=16 << 20),
         name="experts",
-    )(resident(block), gain, gate_up, down, gate_up_1, down_1, rider)
+    )(*(resident(v) for v in (block, gain, gate_up, down)), gate_up_1, down_1, resident(rider))
 
 
 def shards(

time: 161 us -> 160 us (level)
  no operation moved by 1% of the time
where the time goes in v9:
time: 160 us; the launch traced here: 159 us
  starting transfers between devices  54.9 us (34%)
  waiting for transfers between devices  43.9 us (27%)
  blocking collectives  39.7 us (25%)
  local copies, waits for them, and re-layouts  8.95 us (6%)
  Pallas kernels  4.62 us (3%)
  other arithmetic  4.1 us (3%)
    all_to_all x6, starting transfers between devices, exchange(): return lax.all_to_all(blocks, axes, split_axis=0, concat_axis=0, tiled=True)  50.6 us
    all_to_all x6, waiting for transfers between devices, exchange(): return lax.all_to_all(blocks, axes, split_axis=0, concat_axis=0, tiled=True)  42.5 us
    all_gather x4, blocking collectives, shards(): all_rows = lax.all_gather(all_rows, axis, tiled=True)  21.1 us
    all_to_all x1, blocking collectives, exchange(): return lax.all_to_all(blocks, axes, split_axis=0, concat_axis=0, tiled=True)  18.6 us
    ppermute x2, starting transfers between devices, shards(): lax.ppermute(w, 'c', [(0, 1), (1, 0)])  4.33 us
    pallas_call x1, Pallas kernels, experts(): pl.pallas_call(experts_kernel, out_shape=jax.ShapeDtypeStruct(whole, bf16...  3.22 us
  transfers between devices with their start and end apart: 8, of which 7 were waited for; matrix products, arithmetic and copies ran while one was open for 5% of the time, Pallas kernels for 0%

profile of v9, /device:TPU:1, one launch (start us, length us, event | category | flops | bytes accessed | tf_op | source)
XLA Modules:
  0.0 158.8 jit_solution(892381705980489901)
XLA Ops:
  0.7 0.8 maximum_bitcast_fusion
  1.4 0.8 broadcast_in_dim.27
  2.3 15.8 %all-to-all-start = ((bf16[8,64,512]{2,1,0:T(8,128)(2,1)}), bf16[8,64,512]{2,1,0:T(8,128)(2,1)S(1)}, u32[]{:S(2)}, u32[]{:S(2)}) async-start(bf16[8,64,512]{2,1,0:T(8,128)(2,1)} %broadcast_in_dim.27), calls=%async_computation | async-start | bytes 1048576 | tf_op jit(solution)/shard_map/all_to_all | solution.py:21
  18.1 0.1 copy.211
  18.2 2.4 %all_gather.12 = bf16[16,512]{1,0:T(8,128)(2,1)S(1)} all-gather(bf16[8,512]{1,0:T(8,128)(2,1)S(1)} %fusion.9), channel_id=1, replica_groups=mesh['zh'=8,'zl'=2,'xh'=2,'xl'=2,'c'=2,'tp'=4] {'c'}, dimensions={0}, use_global_device_ids=true | all-gather | bytes 24576 | tf_op jit(solution)/shard_map/all_gather | solution.py:234
  20.6 3.2 %all_gather.13 = bf16[32,512]{1,0:T(8,128)(2,1)S(1)} all-gather(bf16[16,512]{1,0:T(8,128)(2,1)S(1)} %all_gather.12), channel_id=1, replica_groups=mesh['zh'=8,'zl'=2,'xh'=2,'xl'=2,'c'=2,'tp'=4] {'xl'}, dimensions={0}, use_global_device_ids=true | all-gather | bytes 49152 | tf_op jit(solution)/shard_map/all_gather | solution.py:234
  23.8 4.9 %all_gather.14 = bf16[64,512]{1,0:T(8,128)(2,1)S(1)} all-gather(bf16[32,512]{1,0:T(8,128)(2,1)S(1)} %all_gather.13), channel_id=1, replica_groups=mesh['zh'=8,'zl'=2,'xh'=2,'xl'=2,'c'=2,'tp'=4] {'xh'}, dimensions={0}, use_global_device_ids=true | all-gather | bytes 98304 | tf_op jit(solution)/shard_map/all_gather | solution.py:234
  28.8 10.5 %all_gather.15 = bf16[128,512]{1,0:T(8,128)(2,1)S(1)} all-gather(bf16[64,512]{1,0:T(8,128)(2,1)S(1)} %all_gather.14), channel_id=1, replica_groups=mesh['zh'=8,'zl'=2,'xh'=2,'xl'=2,'c'=2,'tp'=4] {'zl'}, dimensions={0}, use_global_device_ids=true | all-gather | bytes 196608 | tf_op jit(solution)/shard_map/all_gather | solution.py:234
  39.3 0.1 copy.210
  39.5 0.1 reshape.226
  39.7 0.1 convert_reduce_fusion.1
  39.8 4.0 %all-to-all-done = bf16[8,64,512]{2,1,0:T(8,128)(2,1)S(1)} async-done(((bf16[8,64,512]{2,1,0:T(8,128)(2,1)}), bf16[8,64,512]{2,1,0:T(8,128)(2,1)S(1)}, u32[]{:S(2)}, u32[]{:S(2)}) %all-to-all-start) | async-done | bytes 524320 | tf_op jit(solution)/shard_map/all_to_all | solution.py:21
  43.8 0.1 multiply_convert_fusion.1
  43.9 0.1 broadcast_in_dim.29
  44.0 0.1 copy.183
  44.1 0.3 convolution_bitcast_fusion
  44.4 0.1 broadcast_in_dim.30
  44.5 0.1 pad_maximum_fusion
  44.7 0.7 copy.185
  45.5 16.5 %all-to-all-start.1 = ((f32[64,4,128]{2,1,0:T(4,128)}), f32[64,4,128]{2,1,0:T(4,128)S(1)}, u32[]{:S(2)}, u32[]{:S(2)}) async-start(f32[64,4,128]{2,1,0:T(4,128)} %copy.185), calls=%async_computation.1 | async-start | bytes 262144 | tf_op jit(solution)/shard_map/all_to_all | solution.py:21
  62.0 0.1 copy.180
  62.1 0.3 copy.181
  62.4 0.1 fusion.10
  62.5 8.1 %all-to-all-done.1 = f32[64,4,128]{2,1,0:T(4,128)S(1)} async-done(((f32[64,4,128]{2,1,0:T(4,128)}), f32[64,4,128]{2,1,0:T(4,128)S(1)}, u32[]{:S(2)}, u32[]{:S(2)}) %all-to-all-start.1) | async-done | bytes 131104 | tf_op jit(solution)/shard_map/all_to_all | solution.py:21
  70.5 1.4 recurrence.1
  72.0 3.8 %all-to-all-start.2 = ((bf16[16,4,512]{2,1,0:T(4,128)(2,1)}), bf16[16,4,512]{2,1,0:T(4,128)(2,1)S(1)}, u32[]{:S(2)}, u32[]{:S(2)}) async-start(bf16[16,4,512]{2,1,0:T(4,128)(2,1)} %get-tuple-element.9), calls=%async_computation.2 | async-start | bytes 131072 | tf_op jit(solution)/shard_map/all_to_all | solution.py:21
  75.7 0.3 multiply_convert_fusion
  76.1 1.1 convert_element_type.151
  77.1 0.1 copy.186
  77.3 4.3 %all-to-all-done.2 = bf16[16,4,512]{2,1,0:T(4,128)(2,1)S(1)} async-done(((bf16[16,4,512]{2,1,0:T(4,128)(2,1)}), bf16[16,4,512]{2,1,0:T(4,128)(2,1)S(1)}, u32[]{:S(2)}, u32[]{:S(2)}) %all-to-all-start.2) | async-done | bytes 65568 | tf_op jit(solution)/shard_map/all_to_all | solution.py:21
  81.6 0.2 fusion.11
  81.8 0.2 fusion.2
  82.0 18.6 %all_to_all.35 = bf16[32,8,128]{2,1,0:T(8,128)(2,1)S(1)} all-to-all(bf16[32,8,128]{2,1,0:T(8,128)(2,1)S(1)} %fusion.2), channel_id=1, replica_groups=mesh['zh'=8,'zl'=2,'xh'=2,'xl'=2,'c'=2,'tp'=4] {'zh','tp'}, dimensions={0} | all-to-all | bytes 131072 | tf_op jit(solution)/shard_map/all_to_all | solution.py:21
  100.7 0.9 broadcast_in_dim.43
  101.6 6.1 %all-to-all-start.4 = ((bf16[64,32,128]{2,1,0:T(8,128)(2,1)}), bf16[64,32,128]{2,1,0:T(8,128)(2,1)S(1)}, u32[]{:S(2)}, u32[]{:S(2)}) async-start(bf16[64,32,128]{2,1,0:T(8,128)(2,1)} %bitcast.22), calls=%async_computation.4 | async-start | bytes 1048576 | tf_op jit(solution)/shard_map/all_to_all | solution.py:21
  107.7 0.3 copy.192
  107.9 0.8 copy.193
  108.8 0.3 copy.190
  109.1 1.0 copy-done.3
  110.1 0.2 fusion.5.gu0_ref
  110.3 2.4 %collective-permute-start = (bf16[2048,256]{1,0:T(8,128)(2,1)S(1)}, bf16[2048,256]{1,0:T(8,128)(2,1)}, u32[]{:S(2)}, u32[]{:S(2)}) collective-permute-start(bf16[2048,256]{1,0:T(8,128)(2,1)S(1)} %fusion.5.gu0_ref), channel_id=1, source_target_pairs={{0,4},{4,0},{1,5},{5,1},{2,6},{6,2},{3,7},{7,3},{8,12},{12,8},{9,1... | collective-permute-start | bytes 3145736 | tf_op jit(solution)/shard_map/ppermute | solution.py:298
  112.7 2.0 %collective-permute-start.1 = (bf16[128,2048]{1,0:T(8,128)(2,1)S(1)}, bf16[128,2048]{1,0:T(8,128)(2,1)}, u32[]{:S(2)}, u32[]{:S(2)}) collective-permute-start(bf16[128,2048]{1,0:T(8,128)(2,1)S(1)} %pad.22.down0_ref), channel_id=1, source_target_pairs={{0,4},{4,0},{1,5},{5,1},{2,6},{6,2},{3,7},{7,3},{8,12},{12,8},{9,1... | collective-permute-start | bytes 1572872 | tf_op jit(solution)/shard_map/ppermute | solution.py:298
  114.7 0.1 slice_bitcast_fusion
  114.9 0.1 reshape_reshape.10
  115.0 0.1 reshape_reshape.11.gain_ref
  115.1 0.1 copy.194
  115.3 1.4 collective-permute-done.1.down1_any
  116.7 3.4 %all-to-all-done.4 = bf16[64,32,128]{2,1,0:T(8,128)(2,1)S(1)} async-done(((bf16[64,32,128]{2,1,0:T(8,128)(2,1)}), bf16[64,32,128]{2,1,0:T(8,128)(2,1)S(1)}, u32[]{:S(2)}, u32[]{:S(2)}) %all-to-all-start.4) | async-done | bytes 524320 | tf_op jit(solution)/shard_map/all_to_all | solution.py:21
  120.1 3.2 %experts.1 = bf16[16,4,8,640]{3,2,1,0:T(8,128)(2,1)} custom-call(bf16[16,4,32,128]{3,2,1,0:T(8,128)(2,1)S(1)} %bitcast.87, f32[16,1,128]{2,1,0:T(1,128)S(1)} %reshape_reshape.11.gain_ref, bf16[2048,256]{1,0:T(8,128)(2,1)S(1)} %fusion.5.gu0_ref, bf16[128,2048]{1,0:T(8,128)(2,1)S(1)} %pad.22.down0_ref, bf16[2048,256]{1,0:T(8,128)(2,1)} %collective-permute-done.gu1_any, ...), custom_call_target="tpu_custom_call" | custom-call | tf_op jit(solution)/shard_map/experts/pallas_call | solution.py:180
  123.4 5.2 %all-to-all-start.5 = ((bf16[64,8,640]{2,1,0:T(8,128)(2,1)}), bf16[64,8,640]{2,1,0:T(8,128)(2,1)S(1)}, u32[]{:S(2)}, u32[]{:S(2)}) async-start(bf16[64,8,640]{2,1,0:T(8,128)(2,1)} %bitcast.35), calls=%async_computation.5 | async-start | bytes 1310720 | tf_op jit(solution)/shard_map/all_to_all | solution.py:21
  128.5 0.2 convert_reduce_fusion.2
  128.7 0.1 iota_compare_fusion.6
  128.8 0.1 select_reduce_fusion
  129.0 1.6 multiply_add_fusion
  130.5 11.9 %all-to-all-done.5 = bf16[64,8,640]{2,1,0:T(8,128)(2,1)S(1)} async-done(((bf16[64,8,640]{2,1,0:T(8,128)(2,1)}), bf16[64,8,640]{2,1,0:T(8,128)(2,1)S(1)}, u32[]{:S(2)}, u32[]{:S(2)}) %all-to-all-start.5) | async-done | bytes 655392 | tf_op jit(solution)/shard_map/all_to_all | solution.py:21
  142.4 0.1 slice.32
  142.5 0.1 reduce_sum.79
  142.6 0.6 copy.224
  143.2 3.3 %all-to-all-start.6 = ((bf16[8,2,512]{2,1,0:T(2,128)(2,1)}), bf16[8,2,512]{2,1,0:T(2,128)(2,1)S(1)}, u32[]{:S(2)}, u32[]{:S(2)}) async-start(bf16[8,2,512]{2,1,0:T(2,128)(2,1)} %bitcast.85), calls=%async_computation.6 | async-start | bytes 32768 | tf_op jit(solution)/shard_map/all_to_all | solution.py:21
  146.6 0.2 reshape.222
  146.8 0.2 reduce_sum.76
  147.0 0.1 reshape.227
  147.1 10.8 %all-to-all-done.6 = bf16[8,2,512]{2,1,0:T(2,128)(2,1)S(1)} async-done(((bf16[8,2,512]{2,1,0:T(2,128)(2,1)}), bf16[8,2,512]{2,1,0:T(2,128)(2,1)S(1)}, u32[]{:S(2)}, u32[]{:S(2)}) %all-to-all-start.6) | async-done | bytes 16416 | tf_op jit(solution)/shard_map/all_to_all | solution.py:21
  158.0 0.8 fusion.4
  (64 shorter events, 0.8 us)
Async XLA Ops:
  0.6 17.4 %copy-start.8 = (s32[4,2]{0,1:T(2,128)S(1)}, s32[4,2]{0,1:T(2,128)}, u32[]{:S(2)}) copy-start(s32[4,2]{0,1:T(2,128)} %param.25) | copy-start | bytes 100
  0.6 17.5 %copy-start.7 = (bf16[4,512]{1,0:T(4,128)(2,1)S(1)}, bf16[4,512]{1,0:T(4,128)(2,1)}, u32[]{:S(2)}) copy-start(bf16[4,512]{1,0:T(4,128)(2,1)} %param.15) | copy-start | bytes 12292
  2.3 37.2 %copy-start.9 = (bf16[512]{0:T(512)(128)(2,1)S(1)}, bf16[512]{0:T(512)(128)(2,1)}, u32[]{:S(2)}) copy-start(bf16[512]{0:T(512)(128)(2,1)} %param.16) | copy-start | bytes 3076
  2.3 37.3 %copy-start.10 = (bf16[512]{0:T(512)(128)(2,1)S(1)}, bf16[512]{0:T(512)(128)(2,1)}, u32[]{:S(2)}) copy-start(bf16[512]{0:T(512)(128)(2,1)} %param.24) | copy-start | bytes 3076
  2.3 41.5 %all-to-all-start = ((bf16[8,64,512]{2,1,0:T(8,128)(2,1)}), bf16[8,64,512]{2,1,0:T(8,128)(2,1)S(1)}, u32[]{:S(2)}, u32[]{:S(2)}) async-start(bf16[8,64,512]{2,1,0:T(8,128)(2,1)} %broadcast_in_dim.27), calls=%async_computation | async-start | bytes 1048576 | tf_op jit(solution)/shard_map/all_to_all | solution.py:21
  44.4 26.1 %copy-start = (f32[4,4,128,128]{3,2,1,0:T(8,128)S(1)}, f32[4,4,128,128]{3,2,1,0:T(8,128)}, u32[]{:S(2)}) copy-start(f32[4,4,128,128]{3,2,1,0:T(8,128)} %refs_1_.1) | copy-start | bytes 3145732
  44.4 26.1 %copy-start.1 = (f32[512]{0:T(512)S(1)}, f32[512]{0:T(512)}, u32[]{:S(2)}) copy-start(f32[512]{0:T(512)} %param.20) | copy-start | bytes 6148
  44.4 26.1 %copy-start.2 = (bf16[128]{0:T(256)(128)(2,1)S(1)}, bf16[128]{0:T(256)(128)(2,1)}, u32[]{:S(2)}) copy-start(bf16[128]{0:T(256)(128)(2,1)} %param.21) | copy-start | bytes 772
  45.5 25.1 %all-to-all-start.1 = ((f32[64,4,128]{2,1,0:T(4,128)}), f32[64,4,128]{2,1,0:T(4,128)S(1)}, u32[]{:S(2)}, u32[]{:S(2)}) async-start(f32[64,4,128]{2,1,0:T(4,128)} %copy.185), calls=%async_computation.1 | async-start | bytes 262144 | tf_op jit(solution)/shard_map/all_to_all | solution.py:21
  72.0 9.7 %all-to-all-start.2 = ((bf16[16,4,512]{2,1,0:T(4,128)(2,1)}), bf16[16,4,512]{2,1,0:T(4,128)(2,1)S(1)}, u32[]{:S(2)}, u32[]{:S(2)}) async-start(bf16[16,4,512]{2,1,0:T(4,128)(2,1)} %get-tuple-element.9), calls=%async_computation.2 | async-start | bytes 131072 | tf_op jit(solution)/shard_map/all_to_all | solution.py:21
  81.8 25.8 %copy-start.5 = (bf16[1,2048,112]{1,2,0:T(8,128)(2,1)S(1)}, bf16[1,2048,112]{1,2,0:T(8,128)(2,1)}, u32[]{:S(2)}) copy-start(bf16[1,2048,112]{1,2,0:T(8,128)(2,1)} %param.28) | copy-start | bytes 1376260
  101.6 18.6 %all-to-all-start.4 = ((bf16[64,32,128]{2,1,0:T(8,128)(2,1)}), bf16[64,32,128]{2,1,0:T(8,128)(2,1)S(1)}, u32[]{:S(2)}, u32[]{:S(2)}) async-start(bf16[64,32,128]{2,1,0:T(8,128)(2,1)} %bitcast.22), calls=%async_computation.4 | async-start | bytes 1048576 | tf_op jit(solution)/shard_map/all_to_all | solution.py:21
  107.6 1.1 copy-start.6
  109.1 1.0 copy-start.3
  110.1 2.6 %copy-start.4 = (bf16[1,112,2048]{2,1,0:T(8,128)(2,1)S(1)}, bf16[1,112,2048]{2,1,0:T(8,128)(2,1)}, u32[]{:S(2)}) copy-start(bf16[1,112,2048]{2,1,0:T(8,128)(2,1)} %param.29) | copy-start | bytes 1376260
  110.3 6.4 %collective-permute-start = (bf16[2048,256]{1,0:T(8,128)(2,1)S(1)}, bf16[2048,256]{1,0:T(8,128)(2,1)}, u32[]{:S(2)}, u32[]{:S(2)}) collective-permute-start(bf16[2048,256]{1,0:T(8,128)(2,1)S(1)} %fusion.5.gu0_ref), channel_id=1, source_target_pairs={{0,4},{4,0},{1,5},{5,1},{2,6},{6,2},{3,7},{7,3},{8,12},{12,8},{9,1... | collective-permute-start | bytes 3145736 | tf_op jit(solution)/shard_map/ppermute | solution.py:298
  112.7 3.9 %collective-permute-start.1 = (bf16[128,2048]{1,0:T(8,128)(2,1)S(1)}, bf16[128,2048]{1,0:T(8,128)(2,1)}, u32[]{:S(2)}, u32[]{:S(2)}) collective-permute-start(bf16[128,2048]{1,0:T(8,128)(2,1)S(1)} %pad.22.down0_ref), channel_id=1, source_target_pairs={{0,4},{4,0},{1,5},{5,1},{2,6},{6,2},{3,7},{7,3},{8,12},{12,8},{9,1... | collective-permute-start | bytes 1572872 | tf_op jit(solution)/shard_map/ppermute | solution.py:298
  123.3 5.5 %copy-start.11 = (f32[4,2]{0,1:T(2,128)S(1)}, f32[4,2]{0,1:T(2,128)}, u32[]{:S(2)}) copy-start(f32[4,2]{0,1:T(2,128)} %param.26) | copy-start | bytes 100
  123.4 19.0 %all-to-all-start.5 = ((bf16[64,8,640]{2,1,0:T(8,128)(2,1)}), bf16[64,8,640]{2,1,0:T(8,128)(2,1)S(1)}, u32[]{:S(2)}, u32[]{:S(2)}) async-start(bf16[64,8,640]{2,1,0:T(8,128)(2,1)} %bitcast.35), calls=%async_computation.5 | async-start | bytes 1310720 | tf_op jit(solution)/shard_map/all_to_all | solution.py:21
  143.2 14.7 %all-to-all-start.6 = ((bf16[8,2,512]{2,1,0:T(2,128)(2,1)}), bf16[8,2,512]{2,1,0:T(2,128)(2,1)S(1)}, u32[]{:S(2)}, u32[]{:S(2)}) async-start(bf16[8,2,512]{2,1,0:T(2,128)(2,1)} %bitcast.85), calls=%async_computation.6 | async-start | bytes 32768 | tf_op jit(solution)/shard_map/all_to_all | solution.py:21

commit v10 on v9

--- a/solution.py
+++ b/solution.py
@@ -127,12 +127,13 @@
 
 
 def experts_kernel(
-    rows_v, gain_ref, gu0_ref, down0_ref, gu1_any, down1_any, rider_ref, out_ref,
-    second, gu1_ref, down1_ref, out_v, sems, out_sems,
+    rows_v, gain_ref, gu0_ref, down0_any, gu1_any, down1_any, rider_ref, out_ref,
+    second, gu1_ref, down0_ref, down1_ref, out_v, sems, out_sems,
 ):
     copies = (
         pltpu.make_async_copy(gu1_any, gu1_ref, sems.at[0]),
-        pltpu.make_async_copy(down1_any, down1_ref, sems.at[1]),
+        pltpu.make_async_copy(down0_any, down0_ref, sems.at[1]),
+        pltpu.make_async_copy(down1_any, down1_ref, sems.at[2]),
     )
     for copy in copies:
         copy.start()
@@ -156,6 +157,7 @@
         gate = both[:, :lanes]
         hidden.append((gate / (1.0 + jnp.exp(-gate)) * both[:, lanes:]).astype(bf16))
     copies[1].wait()
+    copies[2].wait()
     outs = []
     for part in range(parts):
         at = slice(part * feat, (part + 1) * feat)
@@ -176,23 +178,29 @@
     count = parts * height
     whole = (count // zh, parts, zh, feat + lanes)
     anywhere = pl.BlockSpec(memory_space=pl.ANY)
+    far = pl.BlockSpec(memory_space=pltpu.HBM)
     vmem = pl.BlockSpec(memory_space=pltpu.VMEM)
     return pl.pallas_call(
         experts_kernel,
         out_shape=jax.ShapeDtypeStruct(whole, bf16),
-        in_specs=[vmem, vmem, vmem, vmem, anywhere, anywhere, vmem],
+        in_specs=[vmem, vmem, vmem, far, far, far, vmem],
         out_specs=anywhere,
         scratch_shapes=[
             pltpu.VMEM((count, gate_up.shape[0]), bf16),
             pltpu.VMEM(gate_up.shape, bf16),
             pltpu.VMEM(down.shape, bf16),
+            pltpu.VMEM(down.shape, bf16),
             pltpu.VMEM(whole, bf16),
-            pltpu.SemaphoreType.DMA((2,)),
+            pltpu.SemaphoreType.DMA((3,)),
             pltpu.SemaphoreType.DMA((parts,)),
         ],
         compiler_params=pltpu.CompilerParams(vmem_limit_bytes=16 << 20),
         name="experts",
-    )(*(resident(v) for v in (block, gain, gate_up, down)), gate_up_1, down_1, resident(rider))
+    )(
+        *(resident(v) for v in (block, gain, gate_up)),
+        *(pltpu.with_memory_space_constraint(v, pltpu.HBM) for v in (down, gate_up_1, down_1)),
+        resident(rider),
+    )
 
 
 def shards(
@@ -233,11 +241,16 @@
     for axis in GATHER:
         all_rows = lax.all_gather(all_rows, axis, tiled=True)
 
+    swap = [(0, 1), (1, 0)]
+    down = jnp.pad(w_down[0], ((0, LANES - w_down.shape[1]), (0, 0)))
+    down_other = lax.ppermute(down, "c", swap)
     all_rows = all_rows.reshape(2, 2, 2, 2, 2, seq, feat)
     order = tuple(GATHER[::-1].index(axis) for axis in ROW)
     all_rows = all_rows.transpose(*order, 4, 5, 6).reshape(rows, 2, seq, feat)
     experts_all = all_rows[:, 1, :, : route_experts.shape[1]].astype(jnp.int32)
-    w_all, tok_all = lax.optimization_barrier((w_all, all_rows[:, 0].reshape(rows * seq, feat)))
+    w_all, tok_all, down, down_other = lax.optimization_barrier(
+        (w_all, all_rows[:, 0].reshape(rows * seq, feat), down, down_other)
+    )
     w_in = w_all[:, : 3 * col].reshape(tp, low * 3 * col, feat)
     w_out = w_all[:, 3 * col :].reshape(tp, low * col, feat)
 
@@ -294,8 +307,7 @@
     gate_up = jnp.concatenate(
         [jnp.pad(ordered(w_gate[0]), fill), jnp.pad(ordered(w_up[0]), fill)], axis=1
     )
-    down = jnp.pad(w_down[0], fill[::-1])
-    weights_of = [(gate_up, down), tuple(lax.ppermute(w, "c", [(0, 1), (1, 0)]) for w in (gate_up, down))]
+    weights_of = [(gate_up, down), (lax.ppermute(gate_up, "c", swap), down_other)]
 
     gain_all = got[:, :, :, used : used + share].transpose(1, 0, 2, 3)
     gain_all = ordered(gain_all.reshape(width, 1)).reshape(rows, 1, LANES)

time: 160 us -> 160 us (level)
  blocking collectives: 39.7 us -> 41.8 us
    all_to_all x1, blocking collectives: 18.6 us -> 20.6 us  [exchange(): return lax.all_to_all(blocks, axes, split_axis=0, concat_axis=0, tiled=True)]
    all_to_all x6, starting transfers between devices: 50.6 us -> 48.7 us  [exchange(): return lax.all_to_all(blocks, axes, split_axis=0, concat_axis=0, tiled=True)]
  transfers between devices with their start and end apart: 8 -> 8, of which waited for: 7 -> 7; matrix products, arithmetic and copies ran while one was open for 5% -> 4% of each run, Pallas kernels for 0% -> 0%
where the time goes in v10:
time: 160 us; the launch traced here: 159 us
  starting transfers between devices  53.9 us (34%)
  waiting for transfers between devices  43.9 us (27%)
  blocking collectives  41.8 us (26%)
  local copies, waits for them, and re-layouts  8.12 us (5%)
  Pallas kernels  4.61 us (3%)
  other arithmetic  4.16 us (3%)
    all_to_all x6, starting transfers between devices, exchange(): return lax.all_to_all(blocks, axes, split_axis=0, concat_axis=0, tiled=True)  48.7 us
    all_to_all x6, waiting for transfers between devices, exchange(): return lax.all_to_all(blocks, axes, split_axis=0, concat_axis=0, tiled=True)  42 us
    all_gather x4, blocking collectives, shards(): all_rows = lax.all_gather(all_rows, axis, tiled=True)  21.2 us
    all_to_all x1, blocking collectives, exchange(): return lax.all_to_all(blocks, axes, split_axis=0, concat_axis=0, tiled=True)  20.6 us
    pallas_call x1, Pallas kernels, experts(): pl.pallas_call(experts_kernel, out_shape=jax.ShapeDtypeStruct(whole, bf16...  3.21 us
  transfers between devices with their start and end apart: 8, of which 7 were waited for; matrix products, arithmetic and copies ran while one was open for 4% of the time, Pallas kernels for 0%

profile of v10, /device:TPU:1, one launch (start us, length us, event | category | flops | bytes accessed | tf_op | source)
XLA Modules:
  0.0 159.0 jit_solution(18174894858767788554)
XLA Ops:
  0.6 0.8 maximum_bitcast_fusion
  1.5 0.8 broadcast_in_dim.27
  2.3 15.8 %all-to-all-start = ((bf16[8,64,512]{2,1,0:T(8,128)(2,1)}), bf16[8,64,512]{2,1,0:T(8,128)(2,1)S(1)}, u32[]{:S(2)}, u32[]{:S(2)}) async-start(bf16[8,64,512]{2,1,0:T(8,128)(2,1)} %broadcast_in_dim.27), calls=%async_computation | async-start | bytes 1048576 | tf_op jit(solution)/shard_map/all_to_all | solution.py:21
  18.2 2.9 %collective-permute-start = (bf16[128,2048]{1,0:T(8,128)(2,1)S(1)}, bf16[128,2048]{1,0:T(8,128)(2,1)S(1)}, u32[]{:S(2)}, u32[]{:S(2)}) collective-permute-start(bf16[128,2048]{1,0:T(8,128)(2,1)S(1)} %pad.20.down0_any), channel_id=1, source_target_pairs={{0,4},{4,0},{1,5},{5,1},{2,6},{6,2},{3,7},{7,3},{8,12},{12,8},{9,1... | collective-permute-start | bytes 1572872 | tf_op jit(solution)/shard_map/ppermute | solution.py:246
  21.0 0.1 copy.211
  21.2 1.8 %all_gather.12 = bf16[16,512]{1,0:T(8,128)(2,1)S(1)} all-gather(bf16[8,512]{1,0:T(8,128)(2,1)S(1)} %fusion.9), channel_id=1, replica_groups=mesh['zh'=8,'zl'=2,'xh'=2,'xl'=2,'c'=2,'tp'=4] {'c'}, dimensions={0}, use_global_device_ids=true | all-gather | bytes 24576 | tf_op jit(solution)/shard_map/all_gather | solution.py:242
  23.0 3.5 %all_gather.13 = bf16[32,512]{1,0:T(8,128)(2,1)S(1)} all-gather(bf16[16,512]{1,0:T(8,128)(2,1)S(1)} %all_gather.12), channel_id=1, replica_groups=mesh['zh'=8,'zl'=2,'xh'=2,'xl'=2,'c'=2,'tp'=4] {'xl'}, dimensions={0}, use_global_device_ids=true | all-gather | bytes 49152 | tf_op jit(solution)/shard_map/all_gather | solution.py:242
  26.5 5.2 %all_gather.14 = bf16[64,512]{1,0:T(8,128)(2,1)S(1)} all-gather(bf16[32,512]{1,0:T(8,128)(2,1)S(1)} %all_gather.13), channel_id=1, replica_groups=mesh['zh'=8,'zl'=2,'xh'=2,'xl'=2,'c'=2,'tp'=4] {'xh'}, dimensions={0}, use_global_device_ids=true | all-gather | bytes 98304 | tf_op jit(solution)/shard_map/all_gather | solution.py:242
  31.7 10.6 %all_gather.15 = bf16[128,512]{1,0:T(8,128)(2,1)S(1)} all-gather(bf16[64,512]{1,0:T(8,128)(2,1)S(1)} %all_gather.14), channel_id=1, replica_groups=mesh['zh'=8,'zl'=2,'xh'=2,'xl'=2,'c'=2,'tp'=4] {'zl'}, dimensions={0}, use_global_device_ids=true | all-gather | bytes 196608 | tf_op jit(solution)/shard_map/all_gather | solution.py:242
  42.4 0.1 copy.210
  42.6 0.1 reshape.226
  42.8 0.1 convert_reduce_fusion.1
  42.9 1.0 all-to-all-done
  43.9 0.1 multiply_convert_fusion.1
  44.0 0.1 broadcast_in_dim.29
  44.1 0.1 copy.183
  44.3 0.3 convolution_bitcast_fusion
  44.6 0.1 broadcast_in_dim.30
  44.7 0.1 pad_maximum_fusion
  44.8 0.1 copy.184
  44.9 0.7 copy.185
  45.6 15.0 %all-to-all-start.1 = ((f32[64,4,128]{2,1,0:T(4,128)}), f32[64,4,128]{2,1,0:T(4,128)S(1)}, u32[]{:S(2)}, u32[]{:S(2)}) async-start(f32[64,4,128]{2,1,0:T(4,128)} %copy.185), calls=%async_computation.1 | async-start | bytes 262144 | tf_op jit(solution)/shard_map/all_to_all | solution.py:21
  60.7 0.1 copy.180
  60.8 0.3 copy.181
  61.1 0.1 fusion.10
  61.1 8.1 %all-to-all-done.1 = f32[64,4,128]{2,1,0:T(4,128)S(1)} async-done(((f32[64,4,128]{2,1,0:T(4,128)}), f32[64,4,128]{2,1,0:T(4,128)S(1)}, u32[]{:S(2)}, u32[]{:S(2)}) %all-to-all-start.1) | async-done | bytes 131104 | tf_op jit(solution)/shard_map/all_to_all | solution.py:21
  69.2 1.4 recurrence.1
  70.6 3.8 %all-to-all-start.2 = ((bf16[16,4,512]{2,1,0:T(4,128)(2,1)}), bf16[16,4,512]{2,1,0:T(4,128)(2,1)S(1)}, u32[]{:S(2)}, u32[]{:S(2)}) async-start(bf16[16,4,512]{2,1,0:T(4,128)(2,1)} %get-tuple-element.11), calls=%async_computation.2 | async-start | bytes 131072 | tf_op jit(solution)/shard_map/all_to_all | solution.py:21
  74.4 0.3 multiply_convert_fusion
  74.7 1.1 convert_element_type.151
  75.8 0.1 copy.186
  75.9 4.3 %all-to-all-done.2 = bf16[16,4,512]{2,1,0:T(4,128)(2,1)S(1)} async-done(((bf16[16,4,512]{2,1,0:T(4,128)(2,1)}), bf16[16,4,512]{2,1,0:T(4,128)(2,1)S(1)}, u32[]{:S(2)}, u32[]{:S(2)}) %all-to-all-start.2) | async-done | bytes 65568 | tf_op jit(solution)/shard_map/all_to_all | solution.py:21
  80.3 0.2 fusion.11
  80.5 0.2 fusion.2
  80.7 20.6 %all_to_all.35 = bf16[32,8,128]{2,1,0:T(8,128)(2,1)S(1)} all-to-all(bf16[32,8,128]{2,1,0:T(8,128)(2,1)S(1)} %fusion.2), channel_id=1, replica_groups=mesh['zh'=8,'zl'=2,'xh'=2,'xl'=2,'c'=2,'tp'=4] {'zh','tp'}, dimensions={0} | all-to-all | bytes 131072 | tf_op jit(solution)/shard_map/all_to_all | solution.py:21
  101.3 0.9 broadcast_in_dim.43
  102.2 6.0 %all-to-all-start.4 = ((bf16[64,32,128]{2,1,0:T(8,128)(2,1)}), bf16[64,32,128]{2,1,0:T(8,128)(2,1)S(1)}, u32[]{:S(2)}, u32[]{:S(2)}) async-start(bf16[64,32,128]{2,1,0:T(8,128)(2,1)} %bitcast.23), calls=%async_computation.4 | async-start | bytes 1048576 | tf_op jit(solution)/shard_map/all_to_all | solution.py:21
  108.3 0.3 copy.192
  108.6 1.0 copy-done.7
  109.6 0.3 copy.190
  109.9 0.2 fusion.5.gu0_ref
  110.1 2.4 %collective-permute-start.1 = (bf16[2048,256]{1,0:T(8,128)(2,1)S(1)}, bf16[2048,256]{1,0:T(8,128)(2,1)}, u32[]{:S(2)}, u32[]{:S(2)}) collective-permute-start(bf16[2048,256]{1,0:T(8,128)(2,1)S(1)} %fusion.5.gu0_ref), channel_id=1, source_target_pairs={{0,4},{4,0},{1,5},{5,1},{2,6},{6,2},{3,7},{7,3},{8,12},{12,8},{9,1... | collective-permute-start | bytes 3145736 | tf_op jit(solution)/shard_map/ppermute | solution.py:310
  112.5 0.1 slice_bitcast_fusion
  112.6 0.1 reshape_reshape.10
  112.8 0.1 reshape_reshape.11.gain_ref
  112.9 0.1 copy.194
  113.1 1.8 %collective-permute-done.1.gu1_any = bf16[2048,256]{1,0:T(8,128)(2,1)} collective-permute-done((bf16[2048,256]{1,0:T(8,128)(2,1)S(1)}, bf16[2048,256]{1,0:T(8,128)(2,1)}, u32[]{:S(2)}, u32[]{:S(2)}) %collective-permute-start.1) | collective-permute-done | bytes 1048608 | tf_op jit(solution)/shard_map/ppermute | solution.py:310
  114.9 5.9 %all-to-all-done.4 = bf16[64,32,128]{2,1,0:T(8,128)(2,1)S(1)} async-done(((bf16[64,32,128]{2,1,0:T(8,128)(2,1)}), bf16[64,32,128]{2,1,0:T(8,128)(2,1)S(1)}, u32[]{:S(2)}, u32[]{:S(2)}) %all-to-all-start.4) | async-done | bytes 524320 | tf_op jit(solution)/shard_map/all_to_all | solution.py:21
  120.7 3.2 %experts.1 = bf16[16,4,8,640]{3,2,1,0:T(8,128)(2,1)} custom-call(bf16[16,4,32,128]{3,2,1,0:T(8,128)(2,1)S(1)} %bitcast.87, f32[16,1,128]{2,1,0:T(1,128)S(1)} %reshape_reshape.11.gain_ref, bf16[2048,256]{1,0:T(8,128)(2,1)S(1)} %fusion.5.gu0_ref, bf16[128,2048]{1,0:T(8,128)(2,1)} %copy-done.3, bf16[2048,256]{1,0:T(8,128)(2,1)} %collective-permute-done.1.gu1_any, ...), custom_call_target="tpu_custom_call" | custom-call | tf_op jit(solution)/shard_map/experts/pallas_call | solution.py:183
  124.0 4.7 %all-to-all-start.5 = ((bf16[64,8,640]{2,1,0:T(8,128)(2,1)}), bf16[64,8,640]{2,1,0:T(8,128)(2,1)S(1)}, u32[]{:S(2)}, u32[]{:S(2)}) async-start(bf16[64,8,640]{2,1,0:T(8,128)(2,1)} %bitcast.35), calls=%async_computation.5 | async-start | bytes 1310720 | tf_op jit(solution)/shard_map/all_to_all | solution.py:21
  128.7 0.2 convert_reduce_fusion.2
  128.9 0.1 iota_compare_fusion.6
  129.0 0.1 select_reduce_fusion
  129.1 1.6 multiply_add_fusion
  130.7 11.9 %all-to-all-done.5 = bf16[64,8,640]{2,1,0:T(8,128)(2,1)S(1)} async-done(((bf16[64,8,640]{2,1,0:T(8,128)(2,1)}), bf16[64,8,640]{2,1,0:T(8,128)(2,1)S(1)}, u32[]{:S(2)}, u32[]{:S(2)}) %all-to-all-start.5) | async-done | bytes 655392 | tf_op jit(solution)/shard_map/all_to_all | solution.py:21
  142.7 0.1 slice.32
  142.8 0.1 reduce_sum.79
  142.9 0.6 copy.224
  143.5 3.3 %all-to-all-start.6 = ((bf16[8,2,512]{2,1,0:T(2,128)(2,1)}), bf16[8,2,512]{2,1,0:T(2,128)(2,1)S(1)}, u32[]{:S(2)}, u32[]{:S(2)}) async-start(bf16[8,2,512]{2,1,0:T(2,128)(2,1)} %bitcast.85), calls=%async_computation.6 | async-start | bytes 32768 | tf_op jit(solution)/shard_map/all_to_all | solution.py:21
  146.9 0.2 reshape.222
  147.1 0.2 reduce_sum.76
  147.3 0.1 reshape.227
  147.4 10.8 %all-to-all-done.6 = bf16[8,2,512]{2,1,0:T(2,128)(2,1)S(1)} async-done(((bf16[8,2,512]{2,1,0:T(2,128)(2,1)}), bf16[8,2,512]{2,1,0:T(2,128)(2,1)S(1)}, u32[]{:S(2)}, u32[]{:S(2)}) %all-to-all-start.6) | async-done | bytes 16416 | tf_op jit(solution)/shard_map/all_to_all | solution.py:21
  158.2 0.8 fusion.4
  (66 shorter events, 0.7 us)
Async XLA Ops:
  0.6 17.5 %copy-start.5 = (bf16[1,112,2048]{2,1,0:T(8,128)(2,1)S(1)}, bf16[1,112,2048]{2,1,0:T(8,128)(2,1)}, u32[]{:S(2)}) copy-start(bf16[1,112,2048]{2,1,0:T(8,128)(2,1)} %param.29) | copy-start | bytes 1376260
  2.3 18.7 %copy-start.9 = (s32[4,2]{0,1:T(2,128)S(1)}, s32[4,2]{0,1:T(2,128)}, u32[]{:S(2)}) copy-start(s32[4,2]{0,1:T(2,128)} %param.25) | copy-start | bytes 100
  2.3 18.8 %copy-start.8 = (bf16[4,512]{1,0:T(4,128)(2,1)S(1)}, bf16[4,512]{1,0:T(4,128)(2,1)}, u32[]{:S(2)}) copy-start(bf16[4,512]{1,0:T(4,128)(2,1)} %param.15) | copy-start | bytes 12292
  2.3 41.6 %all-to-all-start = ((bf16[8,64,512]{2,1,0:T(8,128)(2,1)}), bf16[8,64,512]{2,1,0:T(8,128)(2,1)S(1)}, u32[]{:S(2)}, u32[]{:S(2)}) async-start(bf16[8,64,512]{2,1,0:T(8,128)(2,1)} %broadcast_in_dim.27), calls=%async_computation | async-start | bytes 1048576 | tf_op jit(solution)/shard_map/all_to_all | solution.py:21
  18.1 24.5 %copy-start.10 = (bf16[512]{0:T(512)(128)(2,1)S(1)}, bf16[512]{0:T(512)(128)(2,1)}, u32[]{:S(2)}) copy-start(bf16[512]{0:T(512)(128)(2,1)} %param.16) | copy-start | bytes 3076
  18.1 24.6 %copy-start.11 = (bf16[512]{0:T(512)(128)(2,1)S(1)}, bf16[512]{0:T(512)(128)(2,1)}, u32[]{:S(2)}) copy-start(bf16[512]{0:T(512)(128)(2,1)} %param.24) | copy-start | bytes 3076
  18.1 26.1 %copy-start.3 = (bf16[128,2048]{1,0:T(8,128)(2,1)}, bf16[128,2048]{1,0:T(8,128)(2,1)S(1)}, u32[]{:S(2)}) copy-start(bf16[128,2048]{1,0:T(8,128)(2,1)S(1)} %pad.20.down0_any) | copy-start | bytes 1572868
  18.2 24.7 %collective-permute-start = (bf16[128,2048]{1,0:T(8,128)(2,1)S(1)}, bf16[128,2048]{1,0:T(8,128)(2,1)S(1)}, u32[]{:S(2)}, u32[]{:S(2)}) collective-permute-start(bf16[128,2048]{1,0:T(8,128)(2,1)S(1)} %pad.20.down0_any), channel_id=1, source_target_pairs={{0,4},{4,0},{1,5},{5,1},{2,6},{6,2},{3,7},{7,3},{8,12},{12,8},{9,1... | collective-permute-start | bytes 1572872 | tf_op jit(solution)/shard_map/ppermute | solution.py:246
  42.9 1.2 copy-start.4
  44.5 24.6 %copy-start = (f32[4,4,128,128]{3,2,1,0:T(8,128)S(1)}, f32[4,4,128,128]{3,2,1,0:T(8,128)}, u32[]{:S(2)}) copy-start(f32[4,4,128,128]{3,2,1,0:T(8,128)} %refs_1_.1) | copy-start | bytes 3145732
  44.6 24.6 %copy-start.1 = (f32[512]{0:T(512)S(1)}, f32[512]{0:T(512)}, u32[]{:S(2)}) copy-start(f32[512]{0:T(512)} %param.20) | copy-start | bytes 6148
  44.6 24.6 %copy-start.2 = (bf16[128]{0:T(256)(128)(2,1)S(1)}, bf16[128]{0:T(256)(128)(2,1)}, u32[]{:S(2)}) copy-start(bf16[128]{0:T(256)(128)(2,1)} %param.21) | copy-start | bytes 772
  45.6 23.6 %all-to-all-start.1 = ((f32[64,4,128]{2,1,0:T(4,128)}), f32[64,4,128]{2,1,0:T(4,128)S(1)}, u32[]{:S(2)}, u32[]{:S(2)}) async-start(f32[64,4,128]{2,1,0:T(4,128)} %copy.185), calls=%async_computation.1 | async-start | bytes 262144 | tf_op jit(solution)/shard_map/all_to_all | solution.py:21
  70.6 9.7 %all-to-all-start.2 = ((bf16[16,4,512]{2,1,0:T(4,128)(2,1)}), bf16[16,4,512]{2,1,0:T(4,128)(2,1)S(1)}, u32[]{:S(2)}, u32[]{:S(2)}) async-start(bf16[16,4,512]{2,1,0:T(4,128)(2,1)} %get-tuple-element.11), calls=%async_computation.2 | async-start | bytes 131072 | tf_op jit(solution)/shard_map/all_to_all | solution.py:21
  80.5 27.8 %copy-start.6 = (bf16[1,2048,112]{1,2,0:T(8,128)(2,1)S(1)}, bf16[1,2048,112]{1,2,0:T(8,128)(2,1)}, u32[]{:S(2)}) copy-start(bf16[1,2048,112]{1,2,0:T(8,128)(2,1)} %param.28) | copy-start | bytes 1376260
  102.2 18.5 %all-to-all-start.4 = ((bf16[64,32,128]{2,1,0:T(8,128)(2,1)}), bf16[64,32,128]{2,1,0:T(8,128)(2,1)S(1)}, u32[]{:S(2)}, u32[]{:S(2)}) async-start(bf16[64,32,128]{2,1,0:T(8,128)(2,1)} %bitcast.23), calls=%async_computation.4 | async-start | bytes 1048576 | tf_op jit(solution)/shard_map/all_to_all | solution.py:21
  108.5 1.0 copy-start.7
  110.1 4.8 %collective-permute-start.1 = (bf16[2048,256]{1,0:T(8,128)(2,1)S(1)}, bf16[2048,256]{1,0:T(8,128)(2,1)}, u32[]{:S(2)}, u32[]{:S(2)}) collective-permute-start(bf16[2048,256]{1,0:T(8,128)(2,1)S(1)} %fusion.5.gu0_ref), channel_id=1, source_target_pairs={{0,4},{4,0},{1,5},{5,1},{2,6},{6,2},{3,7},{7,3},{8,12},{12,8},{9,1... | collective-permute-start | bytes 3145736 | tf_op jit(solution)/shard_map/ppermute | solution.py:310
  124.0 5.1 %copy-start.12 = (f32[4,2]{0,1:T(2,128)S(1)}, f32[4,2]{0,1:T(2,128)}, u32[]{:S(2)}) copy-start(f32[4,2]{0,1:T(2,128)} %param.26) | copy-start | bytes 100
  124.0 18.7 %all-to-all-start.5 = ((bf16[64,8,640]{2,1,0:T(8,128)(2,1)}), bf16[64,8,640]{2,1,0:T(8,128)(2,1)S(1)}, u32[]{:S(2)}, u32[]{:S(2)}) async-start(bf16[64,8,640]{2,1,0:T(8,128)(2,1)} %bitcast.35), calls=%async_computation.5 | async-start | bytes 1310720 | tf_op jit(solution)/shard_map/all_to_all | solution.py:21
  143.5 14.7 %all-to-all-start.6 = ((bf16[8,2,512]{2,1,0:T(2,128)(2,1)}), bf16[8,2,512]{2,1,0:T(2,128)(2,1)S(1)}, u32[]{:S(2)}, u32[]{:S(2)}) async-start(bf16[8,2,512]{2,1,0:T(2,128)(2,1)} %bitcast.85), calls=%async_computation.6 | async-start | bytes 32768 | tf_op jit(solution)/shard_map/all_to_all | solution.py:21
